TPU v7x, 512 devices: a whole 4x8x8 slice. The times are simulated.
512 devices in a mesh: sp: 64 (over z, y), tp: 8 (over x, core).
Axes of the slice: x: 4, y: 8, z: 8, core: 2. Of those that a mesh axis runs over, the one named last changes fastest.
Arguments:
- resid: bfloat16 [32768, 2048], P('sp'), may hold values from -6 to 6
- queries: bfloat16 [32768, 2048], P('sp', 'tp'), may hold values from -6 to 6
- keys: bfloat16 [32768, 512], P('sp', 'tp'), may hold values from -6 to 6
- values: bfloat16 [32768, 512], P('sp', 'tp'), may hold values from -6 to 6
- documents: int32 [32768], P('sp'), may hold values from 0 to 31, never falling along the last dimension, each value on 1 to 2048 neighbouring positions
- q_gain: float32 [64], replicated, may hold values from 0.5 to 6.5
- k_gain: float32 [64], replicated, may hold values from 0.5 to 6.5
- sink: float32 [32], P('tp'), may hold values from -1 to 5
- w_out: bfloat16 [2048, 2048], P('tp'), may hold values from -0.5 to 0.5
- n_gain: float32 [2048], replicated, may hold values from 0.1 to 1.9
- w_up: bfloat16 [2048, 8192], P('sp', 'tp'), may hold values from -0.125 to 0.125
- w_down: bfloat16 [8192, 2048], P('tp', 'sp'), may hold values from -0.0625 to 0.0625
Outputs:
- layer_out: bfloat16 [32768, 2048], P('sp')
All inputs are finite; a program needn't handle non-finite values.
Results may differ from a plain program's by a relative error of at most 0.018.
The roundings to bfloat16 on the way count: a program that leaves them out, or rounds other values in their place, can miss the bound.
Values may be sent and summed in bfloat16 or wider, within the bound.
No kernel may reach another device: no remote copies, remote signals or barrier semaphores. Data moves between devices by JAX's collectives and lax.ppermute only.
A program may use at most 64 MiB of HBM per device.

v0:
```python
import jax
import jax.numpy as jnp
from jax import lax
from jax.experimental import pallas as pl
from jax.experimental.pallas import tpu as pltpu
from jax.sharding import Mesh
from jax.sharding import PartitionSpec as P

WINDOW = 128
EPS = 1e-06
SP = ("z", "y")
TP = ("x", "c")


def shift(x, axis, by):
    n = lax.axis_size(axis)
    return lax.ppermute(x, axis, [(i, (i + by) % n) for i in range(n)])


def swap(x):
    return lax.ppermute(x, "c", [(0, 1), (1, 0)])


def spread(x, axis):
    n = lax.axis_size(axis)
    tiles = lax.all_to_all(jnp.broadcast_to(x, (n, *x.shape)), axis, 0, 0, tiled=True)
    return tiles.reshape(n * x.shape[0], x.shape[1])


def tie(x, y):
    return lax.optimization_barrier((x, y))[0]


def down_body(z_ref, act_ref, *refs):
    *pieces, out_ref = refs
    act = act_ref[...]
    dims = (((1,), (1,)), ((), ()))
    blocks = out_ref.shape[1]
    for r in range(blocks):
        if r < blocks // 2:
            piece = pieces[r][...]
        elif r > blocks // 2:
            piece = pieces[r + 1][...]
        else:
            piece = jnp.concatenate([pieces[r][...], pieces[r + 1][...]], axis=0)
        done = lax.dot_general(act, piece, dims, preferred_element_type=jnp.float32)
        at = lax.rem(z_ref[0] + r, blocks)
        out_ref[:, at] = done.astype(out_ref.dtype).reshape(
            out_ref.shape[0], out_ref.shape[2], out_ref.shape[3]
        )


def down(z, act, pieces, share):
    size = pieces[0].shape[0]
    smem = pl.BlockSpec(memory_space=pltpu.SMEM)
    vmem = pl.BlockSpec(memory_space=pltpu.VMEM)
    return pl.pallas_call(
        down_body,
        in_specs=[smem] + [vmem] * (1 + len(pieces)),
        out_specs=vmem,
        out_shape=jax.ShapeDtypeStruct(
            (act.shape[0] // share, len(pieces) - 1, share, size), jnp.bfloat16
        ),
        cost_estimate=pl.CostEstimate(flops=1 << 30, transcendentals=0, bytes_accessed=1 << 23),
        compiler_params=pltpu.CompilerParams(vmem_limit_bytes=40 << 20),
        name="down",
    )(z, act, *pieces)


def rms_scale(field, gain):
    wide = field.astype(jnp.float32)
    return wide * lax.rsqrt(jnp.mean(wide * wide, axis=-1, keepdims=True) + EPS) * gain


def attention_body(
    core_ref, slope_ref, sink_ref, q_ref, kt_ref, vt_ref, doc_ref, before_ref, after_ref,
    qg_ref, kg_ref, other_ref, own_ref, kn_ref, vn_ref, dk_ref
):
    head = kt_ref.shape[0]
    heads = q_ref.shape[1] // head
    kg = kg_ref[...]
    for j in range(6):
        if j == 0:
            kt, vt, doc = before_ref[:head, :], before_ref[head : 2 * head, :], before_ref[2 * head : 2 * head + 8, :]
        elif j == 5:
            kt, vt, doc = after_ref[:head, :], after_ref[head : 2 * head, :], after_ref[2 * head : 2 * head + 8, :]
        else:
            lanes = slice((j - 1) * WINDOW, j * WINDOW)
            kt, vt, doc = kt_ref[:, lanes], vt_ref[:, lanes], doc_ref[:8, lanes]
        wide = kt.astype(jnp.float32)
        scale = lax.rsqrt(jnp.mean(wide * wide, axis=0, keepdims=True) + EPS)
        kn_ref[j] = (wide * scale * kg).astype(jnp.bfloat16)
        vn_ref[j] = vt
        dk_ref[j] = doc.astype(jnp.float32)
    row = lax.broadcasted_iota(jnp.int32, (WINDOW, 3 * WINDOW), 0)
    col = lax.broadcasted_iota(jnp.int32, (WINDOW, 3 * WINDOW), 1)
    distance = jnp.abs(col - WINDOW - row)
    near = distance <= WINDOW
    far = distance.astype(jnp.float32)
    core = core_ref[0]
    for half in range(2):
        side = 1 - core if half == 0 else core
        for j in range(2):
            block = 2 * side + j
            q = q_ref[pl.ds(pl.multiple_of(block * WINDOW, WINDOW), WINDOW), :]
            keys = jnp.concatenate([kn_ref[block], kn_ref[block + 1], kn_ref[block + 2]], axis=1)
            vals = jnp.concatenate([vn_ref[block], vn_ref[block + 1], vn_ref[block + 2]], axis=1)
            doc_k = jnp.concatenate(
                [jnp.broadcast_to(dk_ref[block + i][:1], (WINDOW, WINDOW)) for i in range(3)], axis=1
            )
            doc_q = jnp.broadcast_to(dk_ref[block + 1][:1], (WINDOW, WINDOW)).T
            allowed = near & (doc_k == jnp.concatenate([doc_q] * 3, axis=1))
            outs = []
            for h in range(heads):
                wide = q[:, h * head : (h + 1) * head].astype(jnp.float32)
                scale = lax.rsqrt(jnp.mean(wide * wide, axis=-1, keepdims=True) + EPS)
                qn = (wide * scale * qg_ref[...]).astype(jnp.bfloat16)
                s = jnp.dot(qn, keys, preferred_element_type=jnp.float32) * head ** (-0.5)
                s = jnp.where(allowed, s - slope_ref[h] * far, jnp.float32(-1e30))
                top = jnp.maximum(jnp.max(s, axis=-1, keepdims=True), sink_ref[h])
                p = jnp.exp(s - top)
                denom = jnp.sum(p, axis=-1, keepdims=True) + jnp.exp(sink_ref[h] - top)
                mixed = lax.dot_general(
                    p.astype(jnp.bfloat16), vals, (((1,), (1,)), ((), ())),
                    preferred_element_type=jnp.float32,
                )
                outs.append((mixed / denom).astype(jnp.bfloat16))
            target = other_ref if half == 0 else own_ref
            target[j * WINDOW : (j + 1) * WINDOW, :] = jnp.concatenate(outs, axis=1)


def attention(core, slopes, sink, q, kt, vt, doc, before, after, q_gain, k_gain):
    head, rows = kt.shape
    smem = pl.BlockSpec(memory_space=pltpu.SMEM)
    vmem = pl.BlockSpec(memory_space=pltpu.VMEM)
    out = jax.ShapeDtypeStruct((rows // 2, q.shape[1]), jnp.bfloat16)
    return pl.pallas_call(
        attention_body,
        in_specs=[smem] * 3 + [vmem] * 8,
        out_specs=[vmem, vmem],
        out_shape=[out, out],
        scratch_shapes=[
            pltpu.VMEM((6, head, WINDOW), jnp.bfloat16),
            pltpu.VMEM((6, head, WINDOW), jnp.bfloat16),
            pltpu.VMEM((6, 8, WINDOW), jnp.float32),
        ],
        cost_estimate=pl.CostEstimate(flops=1 << 31, transcendentals=1 << 20, bytes_accessed=1 << 20),
        name="attend",
    )(core, slopes, sink, q, kt, vt, doc, before, after, q_gain, k_gain)


def shards(
    resid, queries, keys, values, documents, q_gain, k_gain, sink, w_out, n_gain, w_up, w_down
):
    rows = resid.shape[0]
    heads_here = sink.shape[0]
    core = lax.axis_index("c")
    half = rows // 2
    share = rows // lax.axis_size(TP)
    nx = lax.axis_size("x")

    up = lax.all_gather(w_up, SP, axis=0, tiled=True)

    kt, vt = keys.T, values.T
    doc = jnp.broadcast_to((documents + 1).astype(jnp.bfloat16)[None, :], (16, rows))
    packed = jnp.concatenate([kt, vt, doc], axis=0)
    count = lax.axis_size(SP)
    onward = [(i, i + 1) for i in range(count - 1)]
    before = lax.ppermute(packed[:, rows - WINDOW :], SP, onward)
    after = lax.ppermute(packed[:, :WINDOW], SP, [(j, i) for i, j in onward])
    piece = spread(tie(w_down.T, packed), "y")
    w_out_other = swap(w_out)

    heads_all = heads_here * lax.axis_size(TP)
    first_head = (lax.axis_index(TP) * heads_here).astype(jnp.float32)
    slopes = jnp.exp2(
        -8.0 * (first_head + jnp.arange(heads_here, dtype=jnp.float32) + 1.0) / heads_all
    )
    att_send, att_own = attention(
        core.astype(jnp.int32).reshape(1), slopes, sink, queries, kt, vt, doc, before, after,
        q_gain[None, :], k_gain[:, None],
    )
    piece = tie(piece, att_send)
    cut = piece.shape[0] // 2
    up1, dn1 = shift(piece, "z", 1), shift(piece, "z", -1)
    up2, dn2 = shift(up1, "z", 1), shift(dn1, "z", -1)
    up3, dn3 = shift(up2, "z", 1), shift(dn2, "z", -1)
    up4, dn4 = shift(up3[:cut], "z", 1), shift(dn3[cut:], "z", -1)
    pieces = [piece, dn1, dn2, dn3, up4, dn4, up3, up2, up1]

    att_other = swap(att_send)
    partial = jnp.dot(att_own, w_out, preferred_element_type=jnp.float32) + jnp.dot(
        att_other, w_out_other, preferred_element_type=jnp.float32
    )
    tiles = lax.all_to_all(
        partial.astype(jnp.bfloat16).reshape(nx, share, -1), "x", 0, 0, tiled=True
    )
    head_mix = jnp.sum(tiles.astype(jnp.float32), axis=0)
    start = core * half + lax.axis_index("x") * share
    own_resid = lax.dynamic_slice_in_dim(resid, start, share, 0)
    middle = (own_resid.astype(jnp.float32) + head_mix).astype(jnp.bfloat16)
    normed = rms_scale(middle, n_gain).astype(jnp.bfloat16)
    mine = spread(normed, "x")
    normed_all = jnp.concatenate([swap(mine), mine], axis=0)

    upward = jnp.dot(normed_all, up, preferred_element_type=jnp.float32)
    active = jnp.square(jax.nn.relu(upward)).astype(jnp.bfloat16)
    z = lax.axis_index("z").astype(jnp.int32).reshape(1)
    sent = swap(down(z, active[:half], pieces, share))
    kept = down(z, active[half:], pieces, share)
    joined = (kept.astype(jnp.float32) + sent.astype(jnp.float32)).astype(jnp.bfloat16)
    tiles = lax.all_to_all(joined, "x", 0, 0, tiled=True)
    unit_mix = jnp.sum(tiles.astype(jnp.float32), axis=0).swapaxes(0, 1).reshape(share, -1)
    finished = spread((middle.astype(jnp.float32) + unit_mix).astype(jnp.bfloat16), "x")
    finished_other = swap(finished)
    low = jnp.where(core == 0, finished, finished_other)
    high = jnp.where(core == 0, finished_other, finished)
    return jnp.concatenate([low, high], axis=0)


def solution(mesh):
    fine = Mesh(mesh.devices.reshape(8, 8, 4, 2), ("z", "y", "x", "c"))
    placed = (
        P(SP, None),
        P(SP, TP),
        P(SP, TP),
        P(SP, TP),
        P(SP),
        P(),
        P(),
        P(TP),
        P(TP, None),
        P(),
        P(SP, TP),
        P(TP, SP),
    )
    return jax.shard_map(shards, mesh=fine, in_specs=placed, out_specs=P(SP, None), check_vma=False)
```

profile of v0, /device:TPU:1, one launch (start us, length us, event | category | flops | bytes accessed | tf_op | source)
XLA Modules:
  0.0 215.9 jit_solution(1662533588985810852)
XLA Ops:
  6.5 0.7 all-gather.2.cloned.1.call-update
  7.3 8.7 %collective-permute-start.3 = (bf16[256,2048]{1,0:T(8,128)(2,1)}, bf16[256,2048]{1,0:T(8,128)(2,1)S(1)}, u32[]{:S(2)}, u32[]{:S(2)}) collective-permute-start(bf16[256,2048]{1,0:T(8,128)(2,1)} %param.20), channel_id=1, source_target_pairs={{0,1},{1,0},{2,3},{3,2},{4,5},{5,4},{6,7},{7,6},{8,9},{9,8},{10,11... | collective-permute-start | bytes 3145736 | tf_op jit(solution)/shard_map/ppermute | solution.py:21
  16.0 0.7 add_convert_fusion.2
  16.7 0.9 pad_maximum_fusion.1
  17.6 1.3 collective-permute-start
  18.9 1.3 collective-permute-start.1
  20.2 0.6 multiply_exponential_fusion.slope_ref
  20.8 1.3 copy.15.kg_ref
  22.2 1.5 collective-permute-done.1.after_ref
  23.6 0.6 copy-done.8
  24.2 6.4 %attend.1 = (bf16[256,256]{1,0:T(8,128)(2,1)}, bf16[256,256]{1,0:T(8,128)(2,1)}) custom-call(s32[1]{0:T(128)} %bitcast.core_ref, f32[4]{0:T(128)} %multiply_exponential_fusion.slope_ref, f32[4]{0:T(128)} %sink_ref.1, bf16[512,256]{1,0:T(8,128)(2,1)} %q_ref.1, bf16[64,512]{1,0:T(8,128)(2,1)} %bitcast.30, bf16[64,512]{1,0:T(8,128)(2,1)} %bitcast.32, ...), custom_call_target="tpu_custom_call" | custom-call | flops 2147483648 | bytes 1048576 | tf_op jit(solution)/shard_map/attend/pallas_call | solution.py:137
  30.6 3.2 %collective-permute-start.2 = (bf16[256,256]{1,0:T(8,128)(2,1)}, bf16[256,256]{1,0:T(8,128)(2,1)S(1)}, u32[]{:S(2)}, u32[]{:S(2)}) collective-permute-start(bf16[256,256]{1,0:T(8,128)(2,1)} %get-tuple-element.10), channel_id=1, source_target_pairs={{0,1},{1,0},{2,3},{3,2},{4,5},{5,4},{6,7},{7,6},{8,9},{9,8},{10,11... | collective-permute-start | bytes 393224 | tf_op jit(solution)/shard_map/ppermute | solution.py:21
  33.8 1.2 collective-permute-done.2
  35.0 0.4 fusion.14
  35.5 1.4 fusion
  36.9 3.6 %all-to-all-start = ((bf16[4,64,2048]{2,1,0:T(8,128)(2,1)}), bf16[4,64,2048]{2,1,0:T(8,128)(2,1)S(1)}, u32[]{:S(2)}, u32[]{:S(2)}) async-start(bf16[4,64,2048]{2,1,0:T(8,128)(2,1)} %bitcast.5), calls=%async_computation | async-start | bytes 2097152 | tf_op jit(solution)/shard_map/all_to_all | solution.py:195
  40.5 0.0 copy-start.6
  40.6 14.8 %all-to-all-done = bf16[4,64,2048]{2,1,0:T(8,128)(2,1)S(1)} async-done(((bf16[4,64,2048]{2,1,0:T(8,128)(2,1)}), bf16[4,64,2048]{2,1,0:T(8,128)(2,1)S(1)}, u32[]{:S(2)}, u32[]{:S(2)}) %all-to-all-start) | async-done | bytes 1048608 | tf_op jit(solution)/shard_map/all_to_all | solution.py:195
  55.3 0.9 broadcast_in_dim.27
  56.2 4.1 %all-to-all-start.2 = ((bf16[8,32,1024]{2,1,0:T(8,128)(2,1)}), bf16[8,32,1024]{2,1,0:T(8,128)(2,1)S(1)}, u32[]{:S(2)}, u32[]{:S(2)}) async-start(bf16[8,32,1024]{2,1,0:T(8,128)(2,1)} %broadcast_in_dim.27), calls=%async_computation.2 | async-start | bytes 1048576 | tf_op jit(solution)/shard_map/all_to_all | solution.py:26
  60.3 0.2 convert_reduce_fusion.1
  60.5 1.1 fusion.7
  61.6 0.7 copy-done
  62.3 0.1 fusion.9
  62.5 14.3 %all-to-all-done.2 = bf16[8,32,1024]{2,1,0:T(8,128)(2,1)S(1)} async-done(((bf16[8,32,1024]{2,1,0:T(8,128)(2,1)}), bf16[8,32,1024]{2,1,0:T(8,128)(2,1)S(1)}, u32[]{:S(2)}, u32[]{:S(2)}) %all-to-all-start.2) | async-done | bytes 524320 | tf_op jit(solution)/shard_map/all_to_all | solution.py:26
  76.8 1.1 broadcast_in_dim.26
  77.9 4.2 %all-to-all-start.1 = ((bf16[4,64,2048]{2,1,0:T(8,128)(2,1)}), bf16[4,64,2048]{2,1,0:T(8,128)(2,1)}, u32[]{:S(2)}, u32[]{:S(2)}) async-start(bf16[4,64,2048]{2,1,0:T(8,128)(2,1)} %broadcast_in_dim.26), calls=%async_computation.1 | async-start | bytes 2097152 | tf_op jit(solution)/shard_map/all_to_all | solution.py:26
  82.1 4.3 %collective-permute-start.8 = (bf16[256,1024]{1,0:T(8,128)(2,1)S(1)}, bf16[256,1024]{1,0:T(8,128)(2,1)S(1)}, u32[]{:S(2)}, u32[]{:S(2)}) collective-permute-start(bf16[256,1024]{1,0:T(8,128)(2,1)S(1)} %bitcast.21), channel_id=1, source_target_pairs={{0,64},{64,128},{128,192},{192,256},{256,320},{320,384},{384,448},... | collective-permute-start | bytes 1572872 | tf_op jit(solution)/shard_map/ppermute | solution.py:17
  86.4 11.2 %collective-permute-start.5 = (bf16[256,1024]{1,0:T(8,128)(2,1)S(1)}, bf16[256,1024]{1,0:T(8,128)(2,1)S(1)}, u32[]{:S(2)}, u32[]{:S(2)}) collective-permute-start(bf16[256,1024]{1,0:T(8,128)(2,1)S(1)} %bitcast.22), channel_id=1, source_target_pairs={{0,448},{64,0},{128,64},{192,128},{256,192},{320,256},{384,320},{4... | collective-permute-start | bytes 1572872 | tf_op jit(solution)/shard_map/ppermute | solution.py:17
  97.6 16.0 %collective-permute-done.8.refs_8_ = bf16[256,1024]{1,0:T(8,128)(2,1)S(1)} collective-permute-done((bf16[256,1024]{1,0:T(8,128)(2,1)S(1)}, bf16[256,1024]{1,0:T(8,128)(2,1)S(1)}, u32[]{:S(2)}, u32[]{:S(2)}) %collective-permute-start.8) | collective-permute-done | bytes 524320 | tf_op jit(solution)/shard_map/ppermute | solution.py:17
  113.6 1.9 collective-permute-start.9
  115.5 0.0 collective-permute-done.5.refs_1_
  115.5 4.6 %collective-permute-start.6 = (bf16[256,1024]{1,0:T(8,128)(2,1)S(1)}, bf16[256,1024]{1,0:T(8,128)(2,1)}, u32[]{:S(2)}, u32[]{:S(2)}) collective-permute-start(bf16[256,1024]{1,0:T(8,128)(2,1)S(1)} %collective-permute-done.5.refs_1_), channel_id=1, source_target_pairs={{0,448},{64,0},{128,64},{192,128},{256,192},{320,256},{384,320},{4... | collective-permute-start | bytes 1572872 | tf_op jit(solution)/shard_map/ppermute | solution.py:17
  120.1 0.0 all-to-all-done.1
  120.1 4.3 %collective-permute-start.4 = (bf16[256,2048]{1,0:T(8,128)(2,1)}, bf16[256,2048]{1,0:T(8,128)(2,1)}, u32[]{:S(2)}, u32[]{:S(2)}) collective-permute-start(bf16[256,2048]{1,0:T(8,128)(2,1)} %bitcast.7), channel_id=1, source_target_pairs={{0,1},{1,0},{2,3},{3,2},{4,5},{5,4},{6,7},{7,6},{8,9},{9,8},{10,11... | collective-permute-start | bytes 3145736 | tf_op jit(solution)/shard_map/ppermute | solution.py:21
  124.4 4.0 %collective-permute-done.9.refs_7_ = bf16[256,1024]{1,0:T(8,128)(2,1)S(1)} collective-permute-done((bf16[256,1024]{1,0:T(8,128)(2,1)S(1)}, bf16[256,1024]{1,0:T(8,128)(2,1)S(1)}, u32[]{:S(2)}, u32[]{:S(2)}) %collective-permute-start.9) | collective-permute-done | bytes 524320 | tf_op jit(solution)/shard_map/ppermute | solution.py:17
  128.4 1.9 collective-permute-start.10
  130.3 0.0 collective-permute-done.6.refs_2_
  130.3 4.6 %collective-permute-start.7 = (bf16[256,1024]{1,0:T(8,128)(2,1)}, bf16[256,1024]{1,0:T(8,128)(2,1)S(1)}, u32[]{:S(2)}, u32[]{:S(2)}) collective-permute-start(bf16[256,1024]{1,0:T(8,128)(2,1)} %collective-permute-done.6.refs_2_), channel_id=1, source_target_pairs={{0,448},{64,0},{128,64},{192,128},{256,192},{320,256},{384,320},{4... | collective-permute-start | bytes 1572872 | tf_op jit(solution)/shard_map/ppermute | solution.py:17
  134.9 7.4 %collective-permute-done.10.refs_6_ = bf16[256,1024]{1,0:T(8,128)(2,1)S(1)} collective-permute-done((bf16[256,1024]{1,0:T(8,128)(2,1)S(1)}, bf16[256,1024]{1,0:T(8,128)(2,1)S(1)}, u32[]{:S(2)}, u32[]{:S(2)}) %collective-permute-start.10) | collective-permute-done | bytes 524320 | tf_op jit(solution)/shard_map/ppermute | solution.py:17
  142.3 0.7 slice.27
  143.0 1.9 collective-permute-start.11
  144.9 0.0 collective-permute-done.7.refs_3_
  144.9 0.7 slice.28
  145.6 4.6 %collective-permute-start.12 = (bf16[128,1024]{1,0:T(8,128)(2,1)}, bf16[128,1024]{1,0:T(8,128)(2,1)}, u32[]{:S(2)}, u32[]{:S(2)}) collective-permute-start(bf16[128,1024]{1,0:T(8,128)(2,1)} %slice.28), channel_id=1, source_target_pairs={{0,448},{64,0},{128,64},{192,128},{256,192},{320,256},{384,320},{4... | collective-permute-start | bytes 786440 | tf_op jit(solution)/shard_map/ppermute | solution.py:17
  150.2 0.0 collective-permute-done.4
  150.2 0.0 all-gather.2.cloned.1.call-done
  150.2 5.2 %multiply_convert_fusion = bf16[512,1024]{1,0:T(8,128)(2,1)S(1)} fusion(bf16[2048,1024]{1,0:T(8,128)(2,1)} %all-gather.2.cloned.1.call-done, bf16[256,2048]{1,0:T(8,128)(2,1)} %bitcast.7, bf16[256,2048]{1,0:T(8,128)(2,1)} %collective-permute-done.4), kind=kOutput, calls=%fused_computation.9 | convolution fusion | flops 2153250816 | bytes 7340032 | tf_op jit(solution)/shard_map/dot_general | solution.py:206
  155.4 0.1 fusion.12
  155.5 0.0 collective-permute-done.11.refs_4_
  155.5 0.0 collective-permute-done.12.refs_5_
  155.5 2.4 %down.3 = bf16[4,8,64,256]{3,2,1,0:T(8,128)(2,1)S(1)} custom-call(s32[1]{0:T(128)} %bitcast.6.z_ref, bf16[256,1024]{1,0:T(8,128)(2,1)S(1)} %get-tuple-element.18.act_ref, bf16[256,1024]{1,0:T(8,128)(2,1)S(1)} %bitcast.23, bf16[256,1024]{1,0:T(8,128)(2,1)S(1)} %collective-permute-done.5.refs_1_, bf16[256,1024]{1,0:T(8,128)(2,1)} %collective-permute-done.6.refs_2_, ...), custom_call_target="tpu_custom_call" | custom-call | flops 1073741824 | bytes 8388608 | tf_op jit(solution)/shard_map/down/pallas_call | solution.py:57
  157.9 6.0 %collective-permute-start.13 = (bf16[4,8,64,256]{3,2,1,0:T(8,128)(2,1)S(1)}, bf16[4,8,64,256]{3,2,1,0:T(8,128)(2,1)S(1)}, u32[]{:S(2)}, u32[]{:S(2)}) collective-permute-start(bf16[4,8,64,256]{3,2,1,0:T(8,128)(2,1)S(1)} %down.3), channel_id=1, source_target_pairs={{0,1},{1,0},{2,3},{3,2},{4,5},{5,4},{6,7},{7,6},{8,9},{9,8},{10,11... | collective-permute-start | bytes 3145736 | tf_op jit(solution)/shard_map/ppermute | solution.py:21
  163.9 2.4 %down.2 = bf16[4,8,64,256]{3,2,1,0:T(8,128)(2,1)S(1)} custom-call(s32[1]{0:T(128)} %bitcast.6.z_ref, bf16[256,1024]{1,0:T(8,128)(2,1)S(1)} %get-tuple-element.17.act_ref, bf16[256,1024]{1,0:T(8,128)(2,1)S(1)} %bitcast.24, bf16[256,1024]{1,0:T(8,128)(2,1)S(1)} %collective-permute-done.5.refs_1_, bf16[256,1024]{1,0:T(8,128)(2,1)} %collective-permute-done.6.refs_2_, ...), custom_call_target="tpu_custom_call" | custom-call | flops 1073741824 | bytes 8388608 | tf_op jit(solution)/shard_map/down/pallas_call | solution.py:57
  166.3 0.4 add_convert_fusion
  166.7 17.5 %all_to_all.25 = bf16[4,8,64,256]{3,2,1,0:T(8,128)(2,1)S(1)} all-to-all(bf16[4,8,64,256]{3,2,1,0:T(8,128)(2,1)S(1)} %add_convert_fusion), channel_id=1, replica_groups=mesh['z'=8,'y'=8,'x'=4,'c'=2] {'x'}, dimensions={0} | all-to-all | bytes 2097152 | tf_op jit(solution)/shard_map/all_to_all | solution.py:212
  184.2 0.2 convert_reduce_fusion
  184.4 0.1 fusion.10
  184.5 0.1 broadcast_in_dim.28
  184.6 16.5 %all_to_all.26 = bf16[4,64,2048]{2,1,0:T(8,128)(2,1)S(1)} all-to-all(bf16[4,64,2048]{2,1,0:T(8,128)(2,1)S(1)} %broadcast_in_dim.28), channel_id=1, replica_groups=mesh['z'=8,'y'=8,'x'=4,'c'=2] {'x'}, dimensions={0} | all-to-all | bytes 2097152 | tf_op jit(solution)/shard_map/all_to_all | solution.py:26
  201.1 3.9 %collective-permute-start.14 = (bf16[256,2048]{1,0:T(8,128)(2,1)S(1)}, bf16[256,2048]{1,0:T(8,128)(2,1)S(1)}, u32[]{:S(2)}, u32[]{:S(2)}) collective-permute-start(bf16[256,2048]{1,0:T(8,128)(2,1)S(1)} %bitcast.25), channel_id=1, source_target_pairs={{0,1},{1,0},{2,3},{3,2},{4,5},{5,4},{6,7},{7,6},{8,9},{9,8},{10,11... | collective-permute-start | bytes 3145736 | tf_op jit(solution)/shard_map/ppermute | solution.py:21
  205.0 2.3 %collective-permute-done.14 = bf16[256,2048]{1,0:T(8,128)(2,1)S(1)} collective-permute-done((bf16[256,2048]{1,0:T(8,128)(2,1)S(1)}, bf16[256,2048]{1,0:T(8,128)(2,1)S(1)}, u32[]{:S(2)}, u32[]{:S(2)}) %collective-permute-start.14) | collective-permute-done | bytes 1048608 | tf_op jit(solution)/shard_map/ppermute | solution.py:21
  207.3 0.2 broadcast_select_fusion.1
  207.5 1.6 pad_maximum_fusion
  (23 shorter events, 0.1 us)
Async XLA Ops:
  6.5 143.7 %all-gather.2.cloned.1.call-start = ((), (), s32[]{:S(2)}) async-start(), calls=%async_computation.5 | async-start | bytes 4259840 | tf_op jit(solution)/shard_map/all_gather | solution.py:162
  7.3 27.7 %collective-permute-start.3 = (bf16[256,2048]{1,0:T(8,128)(2,1)}, bf16[256,2048]{1,0:T(8,128)(2,1)S(1)}, u32[]{:S(2)}, u32[]{:S(2)}) collective-permute-start(bf16[256,2048]{1,0:T(8,128)(2,1)} %param.20), channel_id=1, source_target_pairs={{0,1},{1,0},{2,3},{3,2},{4,5},{5,4},{6,7},{7,6},{8,9},{9,8},{10,11... | collective-permute-start | bytes 3145736 | tf_op jit(solution)/shard_map/ppermute | solution.py:21
  16.7 6.9 %copy-start.5 = (bf16[16,512]{1,0:T(8,128)(2,1)}, bf16[16,512]{1,0:T(8,128)(2,1)S(1)}, u32[]{:S(2)}) copy-start(bf16[16,512]{1,0:T(8,128)(2,1)S(1)} %broadcast_in_dim.23.doc_ref) | copy-start | bytes 49156
  17.6 4.5 %collective-permute-start = (bf16[144,128]{1,0:T(8,128)(2,1)S(1)}, bf16[144,128]{1,0:T(8,128)(2,1)S(1)}, u32[]{:S(2)}, u32[]{:S(2)}) collective-permute-start(bf16[144,128]{1,0:T(8,128)(2,1)S(1)} %get-tuple-element.20), channel_id=1, source_target_pairs={{0,8},{8,16},{16,24},{24,32},{32,40},{40,48},{48,56},{56,64},{64,7... | collective-permute-start | bytes 110600 | tf_op jit(solution)/shard_map/ppermute | solution.py:169
  18.9 4.7 %collective-permute-start.1 = (bf16[144,128]{1,0:T(8,128)(2,1)S(1)}, bf16[144,128]{1,0:T(8,128)(2,1)S(1)}, u32[]{:S(2)}, u32[]{:S(2)}) collective-permute-start(bf16[144,128]{1,0:T(8,128)(2,1)S(1)} %get-tuple-element.19), channel_id=1, source_target_pairs={{8,0},{16,8},{24,16},{32,24},{40,32},{48,40},{56,48},{64,56},{72,6... | collective-permute-start | bytes 110600 | tf_op jit(solution)/shard_map/ppermute | solution.py:170
  22.2 1.5 copy-start.7
  23.6 0.6 copy-start.8
  30.6 4.8 %copy-start.2 = (bf16[256,2048]{1,0:T(8,128)(2,1)S(1)}, bf16[256,2048]{1,0:T(8,128)(2,1)}, u32[]{:S(2)}) copy-start(bf16[256,2048]{1,0:T(8,128)(2,1)} %param.20) | copy-start | bytes 3145732
  30.6 4.8 %copy-start.3 = (bf16[256,256]{1,0:T(8,128)(2,1)S(1)}, bf16[256,256]{1,0:T(8,128)(2,1)}, u32[]{:S(2)}) copy-start(bf16[256,256]{1,0:T(8,128)(2,1)} %get-tuple-element.9) | copy-start | bytes 393220
  30.6 4.4 %collective-permute-start.2 = (bf16[256,256]{1,0:T(8,128)(2,1)}, bf16[256,256]{1,0:T(8,128)(2,1)S(1)}, u32[]{:S(2)}, u32[]{:S(2)}) collective-permute-start(bf16[256,256]{1,0:T(8,128)(2,1)} %get-tuple-element.10), channel_id=1, source_target_pairs={{0,1},{1,0},{2,3},{3,2},{4,5},{5,4},{6,7},{7,6},{8,9},{9,8},{10,11... | collective-permute-start | bytes 393224 | tf_op jit(solution)/shard_map/ppermute | solution.py:21
  36.9 18.5 %copy-start.4 = (bf16[1024,32]{0,1:T(8,128)(2,1)S(1)}, bf16[1024,32]{0,1:T(8,128)(2,1)}, u32[]{:S(2)}) copy-start(bf16[1024,32]{0,1:T(8,128)(2,1)} %param.23) | copy-start | bytes 196612
  36.9 18.5 %all-to-all-start = ((bf16[4,64,2048]{2,1,0:T(8,128)(2,1)}), bf16[4,64,2048]{2,1,0:T(8,128)(2,1)S(1)}, u32[]{:S(2)}, u32[]{:S(2)}) async-start(bf16[4,64,2048]{2,1,0:T(8,128)(2,1)} %bitcast.5), calls=%async_computation | async-start | bytes 2097152 | tf_op jit(solution)/shard_map/all_to_all | solution.py:195
  40.5 21.8 %copy-start.6 = (f32[2048]{0:T(1024)S(1)}, f32[2048]{0:T(1024)}, u32[]{:S(2)}) copy-start(f32[2048]{0:T(1024)} %param.21) | copy-start | bytes 24580
  56.2 20.6 %all-to-all-start.2 = ((bf16[8,32,1024]{2,1,0:T(8,128)(2,1)}), bf16[8,32,1024]{2,1,0:T(8,128)(2,1)S(1)}, u32[]{:S(2)}, u32[]{:S(2)}) async-start(bf16[8,32,1024]{2,1,0:T(8,128)(2,1)} %broadcast_in_dim.27), calls=%async_computation.2 | async-start | bytes 1048576 | tf_op jit(solution)/shard_map/all_to_all | solution.py:26
  61.6 0.7 copy-start
  77.9 42.2 %all-to-all-start.1 = ((bf16[4,64,2048]{2,1,0:T(8,128)(2,1)}), bf16[4,64,2048]{2,1,0:T(8,128)(2,1)}, u32[]{:S(2)}, u32[]{:S(2)}) async-start(bf16[4,64,2048]{2,1,0:T(8,128)(2,1)} %broadcast_in_dim.26), calls=%async_computation.1 | async-start | bytes 2097152 | tf_op jit(solution)/shard_map/all_to_all | solution.py:26
  82.1 31.5 %collective-permute-start.8 = (bf16[256,1024]{1,0:T(8,128)(2,1)S(1)}, bf16[256,1024]{1,0:T(8,128)(2,1)S(1)}, u32[]{:S(2)}, u32[]{:S(2)}) collective-permute-start(bf16[256,1024]{1,0:T(8,128)(2,1)S(1)} %bitcast.21), channel_id=1, source_target_pairs={{0,64},{64,128},{128,192},{192,256},{256,320},{320,384},{384,448},... | collective-permute-start | bytes 1572872 | tf_op jit(solution)/shard_map/ppermute | solution.py:17
  86.4 29.1 %collective-permute-start.5 = (bf16[256,1024]{1,0:T(8,128)(2,1)S(1)}, bf16[256,1024]{1,0:T(8,128)(2,1)S(1)}, u32[]{:S(2)}, u32[]{:S(2)}) collective-permute-start(bf16[256,1024]{1,0:T(8,128)(2,1)S(1)} %bitcast.22), channel_id=1, source_target_pairs={{0,448},{64,0},{128,64},{192,128},{256,192},{320,256},{384,320},{4... | collective-permute-start | bytes 1572872 | tf_op jit(solution)/shard_map/ppermute | solution.py:17
  113.6 14.8 %collective-permute-start.9 = (bf16[256,1024]{1,0:T(8,128)(2,1)S(1)}, bf16[256,1024]{1,0:T(8,128)(2,1)S(1)}, u32[]{:S(2)}, u32[]{:S(2)}) collective-permute-start(bf16[256,1024]{1,0:T(8,128)(2,1)S(1)} %collective-permute-done.8.refs_8_), channel_id=1, source_target_pairs={{0,64},{64,128},{128,192},{192,256},{256,320},{320,384},{384,448},... | collective-permute-start | bytes 1572872 | tf_op jit(solution)/shard_map/ppermute | solution.py:17
  115.5 14.8 %collective-permute-start.6 = (bf16[256,1024]{1,0:T(8,128)(2,1)S(1)}, bf16[256,1024]{1,0:T(8,128)(2,1)}, u32[]{:S(2)}, u32[]{:S(2)}) collective-permute-start(bf16[256,1024]{1,0:T(8,128)(2,1)S(1)} %collective-permute-done.5.refs_1_), channel_id=1, source_target_pairs={{0,448},{64,0},{128,64},{192,128},{256,192},{320,256},{384,320},{4... | collective-permute-start | bytes 1572872 | tf_op jit(solution)/shard_map/ppermute | solution.py:17
  120.1 30.1 %collective-permute-start.4 = (bf16[256,2048]{1,0:T(8,128)(2,1)}, bf16[256,2048]{1,0:T(8,128)(2,1)}, u32[]{:S(2)}, u32[]{:S(2)}) collective-permute-start(bf16[256,2048]{1,0:T(8,128)(2,1)} %bitcast.7), channel_id=1, source_target_pairs={{0,1},{1,0},{2,3},{3,2},{4,5},{5,4},{6,7},{7,6},{8,9},{9,8},{10,11... | collective-permute-start | bytes 3145736 | tf_op jit(solution)/shard_map/ppermute | solution.py:21
  128.4 13.9 %collective-permute-start.10 = (bf16[256,1024]{1,0:T(8,128)(2,1)S(1)}, bf16[256,1024]{1,0:T(8,128)(2,1)S(1)}, u32[]{:S(2)}, u32[]{:S(2)}) collective-permute-start(bf16[256,1024]{1,0:T(8,128)(2,1)S(1)} %collective-permute-done.9.refs_7_), channel_id=1, source_target_pairs={{0,64},{64,128},{128,192},{192,256},{256,320},{320,384},{384,448},... | collective-permute-start | bytes 1572872 | tf_op jit(solution)/shard_map/ppermute | solution.py:17
  130.3 14.6 %collective-permute-start.7 = (bf16[256,1024]{1,0:T(8,128)(2,1)}, bf16[256,1024]{1,0:T(8,128)(2,1)S(1)}, u32[]{:S(2)}, u32[]{:S(2)}) collective-permute-start(bf16[256,1024]{1,0:T(8,128)(2,1)} %collective-permute-done.6.refs_2_), channel_id=1, source_target_pairs={{0,448},{64,0},{128,64},{192,128},{256,192},{320,256},{384,320},{4... | collective-permute-start | bytes 1572872 | tf_op jit(solution)/shard_map/ppermute | solution.py:17
  143.0 12.5 %collective-permute-start.11 = (bf16[128,1024]{1,0:T(8,128)(2,1)}, bf16[128,1024]{1,0:T(8,128)(2,1)S(1)}, u32[]{:S(2)}, u32[]{:S(2)}) collective-permute-start(bf16[128,1024]{1,0:T(8,128)(2,1)} %slice.27), channel_id=1, source_target_pairs={{0,64},{64,128},{128,192},{192,256},{256,320},{320,384},{384,448},... | collective-permute-start | bytes 786440 | tf_op jit(solution)/shard_map/ppermute | solution.py:17
  145.6 9.9 %collective-permute-start.12 = (bf16[128,1024]{1,0:T(8,128)(2,1)}, bf16[128,1024]{1,0:T(8,128)(2,1)}, u32[]{:S(2)}, u32[]{:S(2)}) collective-permute-start(bf16[128,1024]{1,0:T(8,128)(2,1)} %slice.28), channel_id=1, source_target_pairs={{0,448},{64,0},{128,64},{192,128},{256,192},{320,256},{384,320},{4... | collective-permute-start | bytes 786440 | tf_op jit(solution)/shard_map/ppermute | solution.py:17
  157.9 8.4 %collective-permute-start.13 = (bf16[4,8,64,256]{3,2,1,0:T(8,128)(2,1)S(1)}, bf16[4,8,64,256]{3,2,1,0:T(8,128)(2,1)S(1)}, u32[]{:S(2)}, u32[]{:S(2)}) collective-permute-start(bf16[4,8,64,256]{3,2,1,0:T(8,128)(2,1)S(1)} %down.3), channel_id=1, source_target_pairs={{0,1},{1,0},{2,3},{3,2},{4,5},{5,4},{6,7},{7,6},{8,9},{9,8},{10,11... | collective-permute-start | bytes 3145736 | tf_op jit(solution)/shard_map/ppermute | solution.py:21
  166.7 17.7 %copy-start.1 = (bf16[64,2048]{1,0:T(8,128)(2,1)S(1)}, bf16[64,2048]{1,0:T(8,128)(2,1)}, u32[]{:S(2)}) copy-start(bf16[64,2048]{1,0:T(8,128)(2,1)} %copy-done) | copy-start | bytes 786436
  201.1 6.2 %collective-permute-start.14 = (bf16[256,2048]{1,0:T(8,128)(2,1)S(1)}, bf16[256,2048]{1,0:T(8,128)(2,1)S(1)}, u32[]{:S(2)}, u32[]{:S(2)}) collective-permute-start(bf16[256,2048]{1,0:T(8,128)(2,1)S(1)} %bitcast.25), channel_id=1, source_target_pairs={{0,1},{1,0},{2,3},{3,2},{4,5},{5,4},{6,7},{7,6},{8,9},{9,8},{10,11... | collective-permute-start | bytes 3145736 | tf_op jit(solution)/shard_map/ppermute | solution.py:21
Sparse Core Ops, SparseCore 0:
  10.4 98.5 all-gather.1
where the time goes:
time: 217 us; the launch traced here: 216 us
  starting transfers between devices  75.6 us (35%)
  waiting for transfers between devices  62.1 us (29%)
  blocking collectives  34 us (16%)
  between operations  13.8 us (6%)
  Pallas kernels  11.2 us (5%)
  matrix products  7.02 us (3%)
  local copies, waits for them, and re-layouts  6.28 us (3%)
  other arithmetic  5.97 us (3%)
    ppermute x8, starting transfers between devices, shift(): return lax.ppermute(x, axis, [(i, (i + by) % n) for i in range(n)])  34.9 us
    ppermute x8, waiting for transfers between devices, shift(): return lax.ppermute(x, axis, [(i, (i + by) % n) for i in range(n)])  27.4 us
    ppermute x5, starting transfers between devices, swap(): return lax.ppermute(x, 'c', [(0, 1), (1, 0)])  26.1 us
    all_to_all x1, blocking collectives, shards(): tiles = lax.all_to_all(joined, 'x', 0, 0, tiled=True)  17.5 us
    all_to_all x1, blocking collectives, spread(): lax.all_to_all(jnp.broadcast_to(x, (n, *x.shape)), axis, 0, 0, tiled=True)  16.5 us
    all_to_all x1, waiting for transfers between devices, shards(): lax.all_to_all(partial.astype(jnp.bfloat16).reshape(nx, share, -1), 'x',...  14.8 us
    all_to_all x2, waiting for transfers between devices, spread(): lax.all_to_all(jnp.broadcast_to(x, (n, *x.shape)), axis, 0, 0, tiled=True)  14.3 us
    all_to_all x2, starting transfers between devices, spread(): lax.all_to_all(jnp.broadcast_to(x, (n, *x.shape)), axis, 0, 0, tiled=True)  8.37 us
  transfers between devices with their start and end apart: 19, of which 8 were waited for; matrix products, arithmetic and copies ran while one was open for 7% of the time, Pallas kernels for 4%

commit v1 on v0

--- a/solution.py
+++ b/solution.py
@@ -12,9 +12,26 @@
 TP = ("x", "c")
 
 
-def shift(x, axis, by):
-    n = lax.axis_size(axis)
-    return lax.ppermute(x, axis, [(i, (i + by) % n) for i in range(n)])
+def along(x, by):
+    nz, ny = lax.axis_size("z"), lax.axis_size("y")
+    pairs = []
+    for z in range(nz):
+        for y in range(ny):
+            here = 2 * (z * ny + y)
+            pairs.append((here, 2 * (z * ny + (y + by) % ny)))
+            pairs.append((here + 1, 2 * ((z + by) % nz * ny + y) + 1))
+    return lax.ppermute(x, ("z", "y", "c"), pairs)
+
+
+def across(x):
+    nz, ny = lax.axis_size("z"), lax.axis_size("y")
+    groups = [[2 * (z * ny + y) for z in range(nz)] for y in range(ny)]
+    groups += [[2 * (z * ny + y) + 1 for y in range(ny)] for z in range(nz)]
+    tiles = lax.all_to_all(
+        jnp.broadcast_to(x, (nz, *x.shape)),
+        ("z", "y", "c"), 0, 0, tiled=True, axis_index_groups=groups,
+    )
+    return tiles.reshape(nz * x.shape[0], x.shape[1])
 
 
 def swap(x):
@@ -31,45 +48,66 @@
     return lax.optimization_barrier((x, y))[0]
 
 
-def down_body(z_ref, act_ref, *refs):
-    *pieces, out_ref = refs
-    act = act_ref[...]
-    dims = (((1,), (1,)), ((), ()))
-    blocks = out_ref.shape[1]
-    for r in range(blocks):
-        if r < blocks // 2:
-            piece = pieces[r][...]
-        elif r > blocks // 2:
-            piece = pieces[r + 1][...]
-        else:
-            piece = jnp.concatenate([pieces[r][...], pieces[r + 1][...]], axis=0)
-        done = lax.dot_general(act, piece, dims, preferred_element_type=jnp.float32)
-        at = lax.rem(z_ref[0] + r, blocks)
-        out_ref[:, at] = done.astype(out_ref.dtype).reshape(
-            out_ref.shape[0], out_ref.shape[2], out_ref.shape[3]
-        )
-
-
-def down(z, act, pieces, share):
-    size = pieces[0].shape[0]
+def scatter_x(x):
+    n = lax.axis_size("x")
+    tiles = lax.all_to_all(x.reshape(n, x.shape[0] // n, x.shape[1]), "x", 0, 0, tiled=True)
+    return jnp.sum(tiles.astype(jnp.float32), axis=0)
+
+
+def rms_scale(field, gain):
+    wide = field.astype(jnp.float32)
+    return wide * lax.rsqrt(jnp.mean(wide * wide, axis=-1, keepdims=True) + EPS) * gain
+
+
+def mixer_body(at_ref, theirs_ref, mine_ref, *refs):
+    *pieces, down_ref, act_ref, out_ref, up_ref = refs
+    count = len(pieces) - 1
+    units = act_ref.shape[1]
+    cut = pieces[count // 2].shape[0]
+    chunk = 2 * cut // count
+    for r in range(count):
+        index = lax.rem(at_ref[0] + r, count)
+        for j in range(count):
+            if r < count // 2:
+                source, low = pieces[r], j * chunk
+            elif r > count // 2:
+                source, low = pieces[r + 1], j * chunk
+            else:
+                source, low = pieces[r + j * chunk // cut], j * chunk % cut
+            to = pl.multiple_of(j * at_ref[1] + index * at_ref[2], chunk)
+            up_ref[pl.ds(to, chunk), :] = source[low : low + chunk, :units]
+            down_ref[pl.ds(to, chunk), :] = source[low : low + chunk, units:]
+
+    def hidden(rows):
+        wide = jnp.dot(rows, up_ref[...], preferred_element_type=jnp.float32)
+        return jnp.square(jnp.maximum(wide, 0.0)).astype(jnp.bfloat16)
+
+    first = hidden(theirs_ref[...])
+    act_ref[...] = hidden(mine_ref[...])
+    out_ref[...] = lax.dot_general(
+        first, down_ref[...], (((1,), (1,)), ((), ())), preferred_element_type=jnp.float32
+    ).astype(out_ref.dtype)
+
+
+def mixer(at, theirs, mine, pieces):
+    height, width = mine.shape
+    units = pieces[0].shape[1] // 2
     smem = pl.BlockSpec(memory_space=pltpu.SMEM)
     vmem = pl.BlockSpec(memory_space=pltpu.VMEM)
     return pl.pallas_call(
-        down_body,
-        in_specs=[smem] + [vmem] * (1 + len(pieces)),
-        out_specs=vmem,
-        out_shape=jax.ShapeDtypeStruct(
-            (act.shape[0] // share, len(pieces) - 1, share, size), jnp.bfloat16
-        ),
-        cost_estimate=pl.CostEstimate(flops=1 << 30, transcendentals=0, bytes_accessed=1 << 23),
+        mixer_body,
+        in_specs=[smem] + [vmem] * (2 + len(pieces)),
+        out_specs=[vmem] * 3,
+        out_shape=[
+            jax.ShapeDtypeStruct((width, units), jnp.bfloat16),
+            jax.ShapeDtypeStruct((height, units), jnp.bfloat16),
+            jax.ShapeDtypeStruct((height, width), jnp.bfloat16),
+        ],
+        scratch_shapes=[pltpu.VMEM((width, units), jnp.bfloat16)],
+        cost_estimate=pl.CostEstimate(flops=1 << 31, transcendentals=0, bytes_accessed=1 << 23),
         compiler_params=pltpu.CompilerParams(vmem_limit_bytes=40 << 20),
-        name="down",
-    )(z, act, *pieces)
-
-
-def rms_scale(field, gain):
-    wide = field.astype(jnp.float32)
-    return wide * lax.rsqrt(jnp.mean(wide * wide, axis=-1, keepdims=True) + EPS) * gain
+        name="mixer",
+    )(at, theirs, mine, *pieces)
 
 
 def attention_body(
@@ -159,8 +197,6 @@
     share = rows // lax.axis_size(TP)
     nx = lax.axis_size("x")
 
-    up = lax.all_gather(w_up, SP, axis=0, tiled=True)
-
     kt, vt = keys.T, values.T
     doc = jnp.broadcast_to((documents + 1).astype(jnp.bfloat16)[None, :], (16, rows))
     packed = jnp.concatenate([kt, vt, doc], axis=0)
@@ -168,7 +204,7 @@
     onward = [(i, i + 1) for i in range(count - 1)]
     before = lax.ppermute(packed[:, rows - WINDOW :], SP, onward)
     after = lax.ppermute(packed[:, :WINDOW], SP, [(j, i) for i, j in onward])
-    piece = spread(tie(w_down.T, packed), "y")
+    piece = across(tie(jnp.concatenate([w_up, w_down.T], axis=1), packed))
     w_out_other = swap(w_out)
 
     heads_all = heads_here * lax.axis_size(TP)
@@ -182,10 +218,10 @@
     )
     piece = tie(piece, att_send)
     cut = piece.shape[0] // 2
-    up1, dn1 = shift(piece, "z", 1), shift(piece, "z", -1)
-    up2, dn2 = shift(up1, "z", 1), shift(dn1, "z", -1)
-    up3, dn3 = shift(up2, "z", 1), shift(dn2, "z", -1)
-    up4, dn4 = shift(up3[:cut], "z", 1), shift(dn3[cut:], "z", -1)
+    up1, dn1 = along(piece, 1), along(piece, -1)
+    up2, dn2 = along(up1, 1), along(dn1, -1)
+    up3, dn3 = along(up2, 1), along(dn2, -1)
+    up4, dn4 = along(up3[:cut], 1), along(dn3[cut:], -1)
     pieces = [piece, dn1, dn2, dn3, up4, dn4, up3, up2, up1]
 
     att_other = swap(att_send)
@@ -201,16 +237,21 @@
     middle = (own_resid.astype(jnp.float32) + head_mix).astype(jnp.bfloat16)
     normed = rms_scale(middle, n_gain).astype(jnp.bfloat16)
     mine = spread(normed, "x")
-    normed_all = jnp.concatenate([swap(mine), mine], axis=0)
-
-    upward = jnp.dot(normed_all, up, preferred_element_type=jnp.float32)
-    active = jnp.square(jax.nn.relu(upward)).astype(jnp.bfloat16)
-    z = lax.axis_index("z").astype(jnp.int32).reshape(1)
-    sent = swap(down(z, active[:half], pieces, share))
-    kept = down(z, active[half:], pieces, share)
-    joined = (kept.astype(jnp.float32) + sent.astype(jnp.float32)).astype(jnp.bfloat16)
-    tiles = lax.all_to_all(joined, "x", 0, 0, tiled=True)
-    unit_mix = jnp.sum(tiles.astype(jnp.float32), axis=0).swapaxes(0, 1).reshape(share, -1)
+    theirs = swap(mine)
+    z, y = lax.axis_index("z"), lax.axis_index("y")
+    chunk, block = w_up.shape[0], w_up.shape[0] * lax.axis_size("y")
+    at = jnp.stack(
+        [jnp.where(core == 0, y, z), jnp.where(core == 0, block, chunk), jnp.where(core == 0, chunk, block)]
+    ).astype(jnp.int32)
+    down_t, active, out = mixer(at, theirs, mine, pieces)
+    sent = swap(out)
+    kept = lax.optimization_barrier(
+        lax.dot_general(
+            active, down_t, (((1,), (1,)), ((), ())), preferred_element_type=jnp.float32
+        )
+    )
+    joined = (kept + sent.astype(jnp.float32)).astype(jnp.bfloat16)
+    unit_mix = scatter_x(joined)
     finished = spread((middle.astype(jnp.float32) + unit_mix).astype(jnp.bfloat16), "x")
     finished_other = swap(finished)
     low = jnp.where(core == 0, finished, finished_other)

time: 217 us -> 182 us (0.84); the launches traced: 216 us -> 178 us
  waiting for transfers between devices: 62.1 us -> 36.9 us
  between operations: 13.8 us -> 0.34 us
  starting transfers between devices: 75.6 us -> 70.5 us
  Pallas kernels: 11.2 us -> 13.9 us
    all_to_all x2 -> x1, waiting for transfers between devices: 14.3 us -> 2.48 us  [spread(): lax.all_to_all(jnp.broadcast_to(x, (n, *x.shape)), axis, 0, 0, tiled=True)]
    ppermute x8, waiting for transfers between devices: 27.4 us -> 16.7 us  [along(): return lax.ppermute(x, ('z', 'y', 'c'), pairs)]
    ppermute x5, starting transfers between devices: 26.1 us -> 16.6 us  [swap(): return lax.ppermute(x, 'c', [(0, 1), (1, 0)])]
    all_to_all x0 -> x1, starting transfers between devices: none -> 7.64 us  [across(): lax.all_to_all(jnp.broadcast_to(x, (nz, *x.shape)), ('z', 'y', 'c'), 0, 0...]
    all_to_all x2 -> x1, starting transfers between devices: 8.37 us -> 3.52 us  [spread(): lax.all_to_all(jnp.broadcast_to(x, (n, *x.shape)), axis, 0, 0, tiled=True)]
    all_to_all x1, waiting for transfers between devices: 14.8 us -> 11.7 us  [shards(): lax.all_to_all(partial.astype(jnp.bfloat16).reshape(nx, share, -1), 'x',...]
    ppermute x1, starting transfers between devices: 1.29 us -> 3.99 us  [shards(): before = lax.ppermute(packed[:, rows - WINDOW:], SP, onward)]
    pallas_call x2 -> x1, Pallas kernels: 4.81 us -> 7.5 us  [mixer(): pl.pallas_call(mixer_body, in_specs=[smem] + [vmem] * (2 + len(pieces)),...]
  transfers between devices with their start and end apart: 19 -> 18, of which waited for: 8 -> 9; matrix products, arithmetic and copies ran while one was open for 7% -> 9% of each run, Pallas kernels for 4% -> 4%
where the time goes in v1:
time: 182 us; the launch traced here: 178 us
  starting transfers between devices  70.5 us (39%)
  waiting for transfers between devices  36.9 us (20%)
  blocking collectives  33.8 us (19%)
  Pallas kernels  13.9 us (8%)
  matrix products  8.61 us (5%)
  local copies, waits for them, and re-layouts  7.67 us (4%)
  other arithmetic  6.87 us (4%)
    ppermute x8, starting transfers between devices, along(): return lax.ppermute(x, ('z', 'y', 'c'), pairs)  33.2 us
    all_to_all x1, blocking collectives, scatter_x(): lax.all_to_all(x.reshape(n, x.shape[0] // n, x.shape[1]), 'x', 0, 0, tile...  17.3 us
    ppermute x8, waiting for transfers between devices, along(): return lax.ppermute(x, ('z', 'y', 'c'), pairs)  16.7 us
    ppermute x5, starting transfers between devices, swap(): return lax.ppermute(x, 'c', [(0, 1), (1, 0)])  16.6 us
    all_to_all x1, blocking collectives, spread(): lax.all_to_all(jnp.broadcast_to(x, (n, *x.shape)), axis, 0, 0, tiled=True)  16.5 us
    all_to_all x1, waiting for transfers between devices, shards(): lax.all_to_all(partial.astype(jnp.bfloat16).reshape(nx, share, -1), 'x',...  11.7 us
    all_to_all x1, starting transfers between devices, across(): lax.all_to_all(jnp.broadcast_to(x, (nz, *x.shape)), ('z', 'y', 'c'), 0, 0...  7.64 us
    pallas_call x1, Pallas kernels, mixer(): pl.pallas_call(mixer_body, in_specs=[smem] + [vmem] * (2 + len(pieces)),...  7.5 us
  transfers between devices with their start and end apart: 18, of which 9 were waited for; matrix products, arithmetic and copies ran while one was open for 9% of the time, Pallas kernels for 4%

profile of v1, /device:TPU:1, one launch (start us, length us, event | category | flops | bytes accessed | tf_op | source)
XLA Modules:
  0.0 178.5 jit_solution(6988535454321645988)
XLA Ops:
  0.0 0.8 add_convert_fusion.2
  0.8 0.9 pad_maximum_fusion.2
  1.7 0.9 pad_maximum_fusion.1
  2.6 1.1 broadcast_in_dim.27
  3.7 7.6 %all-to-all-start.2 = ((bf16[8,32,2048]{2,1,0:T(8,128)(2,1)}), bf16[8,32,2048]{2,1,0:T(8,128)(2,1)S(1)}, u32[]{:S(2)}, u32[]{:S(2)}) async-start(bf16[8,32,2048]{2,1,0:T(8,128)(2,1)} %broadcast_in_dim.27), calls=%async_computation.2 | async-start | bytes 2097152 | tf_op jit(solution)/shard_map/all_to_all | solution.py:30
  11.4 6.1 %collective-permute-start.3 = (bf16[256,2048]{1,0:T(8,128)(2,1)S(1)}, bf16[256,2048]{1,0:T(8,128)(2,1)S(1)}, u32[]{:S(2)}, u32[]{:S(2)}) collective-permute-start(bf16[256,2048]{1,0:T(8,128)(2,1)S(1)} %copy-done.2), channel_id=1, source_target_pairs={{0,1},{1,0},{2,3},{3,2},{4,5},{5,4},{6,7},{7,6},{8,9},{9,8},{10,11... | collective-permute-start | bytes 3145736 | tf_op jit(solution)/shard_map/ppermute | solution.py:38
  17.5 1.3 collective-permute-start.1
  18.8 4.0 %collective-permute-start = (bf16[144,128]{1,0:T(8,128)(2,1)S(1)}, bf16[144,128]{1,0:T(8,128)(2,1)S(1)}, u32[]{:S(2)}, u32[]{:S(2)}) collective-permute-start(bf16[144,128]{1,0:T(8,128)(2,1)S(1)} %get-tuple-element.24), channel_id=1, source_target_pairs={{0,8},{8,16},{16,24},{24,32},{32,40},{40,48},{48,56},{56,64},{64,7... | collective-permute-start | bytes 110600 | tf_op jit(solution)/shard_map/ppermute | solution.py:205
  22.8 0.6 multiply_exponential_fusion.slope_ref
  23.3 0.7 copy.13.kg_ref
  24.0 2.3 %collective-permute-done.1.after_ref = bf16[144,128]{1,0:T(8,128)(2,1)S(1)} collective-permute-done((bf16[144,128]{1,0:T(8,128)(2,1)S(1)}, bf16[144,128]{1,0:T(8,128)(2,1)S(1)}, u32[]{:S(2)}, u32[]{:S(2)}) %collective-permute-start.1) | collective-permute-done | bytes 36896 | tf_op jit(solution)/shard_map/ppermute | solution.py:206
  26.3 0.0 collective-permute-done.before_ref
  26.3 0.6 copy-done.7
  26.9 0.0 copy-done.8
  26.9 6.4 %attend.1 = (bf16[256,256]{1,0:T(8,128)(2,1)}, bf16[256,256]{1,0:T(8,128)(2,1)}) custom-call(s32[1]{0:T(128)} %bitcast.core_ref, f32[4]{0:T(128)} %multiply_exponential_fusion.slope_ref, f32[4]{0:T(128)} %sink_ref.1, bf16[512,256]{1,0:T(8,128)(2,1)} %q_ref.1, bf16[64,512]{1,0:T(8,128)(2,1)} %bitcast.32, bf16[64,512]{1,0:T(8,128)(2,1)} %bitcast.34, ...), custom_call_target="tpu_custom_call" | custom-call | flops 2147483648 | bytes 1048576 | tf_op jit(solution)/shard_map/attend/pallas_call | solution.py:175
  33.3 2.0 %collective-permute-start.2 = (bf16[256,256]{1,0:T(8,128)(2,1)}, bf16[256,256]{1,0:T(8,128)(2,1)S(1)}, u32[]{:S(2)}, u32[]{:S(2)}) collective-permute-start(bf16[256,256]{1,0:T(8,128)(2,1)} %get-tuple-element.13), channel_id=1, source_target_pairs={{0,1},{1,0},{2,3},{3,2},{4,5},{5,4},{6,7},{7,6},{8,9},{9,8},{10,11... | collective-permute-start | bytes 393224 | tf_op jit(solution)/shard_map/ppermute | solution.py:38
  35.3 1.5 collective-permute-done.2
  36.9 0.0 collective-permute-done.3
  36.9 1.8 fusion.6
  38.6 0.0 all-to-all-done.2
  38.6 7.8 %collective-permute-start.8 = (bf16[256,2048]{1,0:T(8,128)(2,1)S(1)}, bf16[256,2048]{1,0:T(8,128)(2,1)S(1)}, u32[]{:S(2)}, u32[]{:S(2)}) collective-permute-start(bf16[256,2048]{1,0:T(8,128)(2,1)S(1)} %bitcast.22), channel_id=1, source_target_pairs={{0,8},{1,65},{8,16},{9,73},{16,24},{17,81},{24,32},{25,89},{32,40}... | collective-permute-start | bytes 3145736 | tf_op jit(solution)/shard_map/ppermute | solution.py:23
  46.4 5.7 %collective-permute-start.5 = (bf16[256,2048]{1,0:T(8,128)(2,1)S(1)}, bf16[256,2048]{1,0:T(8,128)(2,1)}, u32[]{:S(2)}, u32[]{:S(2)}) collective-permute-start(bf16[256,2048]{1,0:T(8,128)(2,1)S(1)} %bitcast.23), channel_id=1, source_target_pairs={{0,56},{1,449},{8,0},{9,457},{16,8},{17,465},{24,16},{25,473},{32,... | collective-permute-start | bytes 3145736 | tf_op jit(solution)/shard_map/ppermute | solution.py:23
  52.1 3.4 %fusion = bf16[256,2048]{1,0:T(8,128)(2,1)} fusion(f32[256,2048]{1,0:T(8,128)} %fusion.6, bf16[256,256]{1,0:T(8,128)(2,1)S(1)} %copy-done.3, bf16[256,2048]{1,0:T(8,128)(2,1)} %param.20), kind=kOutput, calls=%fused_computation.1 | convolution fusion | flops 269484032 | bytes 4325376 | tf_op jit(solution)/shard_map/dot_general | solution.py:228
  55.5 4.1 %all-to-all-start = ((bf16[4,64,2048]{2,1,0:T(8,128)(2,1)}), bf16[4,64,2048]{2,1,0:T(8,128)(2,1)S(1)}, u32[]{:S(2)}, u32[]{:S(2)}) async-start(bf16[4,64,2048]{2,1,0:T(8,128)(2,1)} %bitcast.28), calls=%async_computation | async-start | bytes 2097152 | tf_op jit(solution)/shard_map/all_to_all | solution.py:231
  59.6 11.7 %all-to-all-done = bf16[4,64,2048]{2,1,0:T(8,128)(2,1)S(1)} async-done(((bf16[4,64,2048]{2,1,0:T(8,128)(2,1)}), bf16[4,64,2048]{2,1,0:T(8,128)(2,1)S(1)}, u32[]{:S(2)}, u32[]{:S(2)}) %all-to-all-start) | async-done | bytes 1048608 | tf_op jit(solution)/shard_map/all_to_all | solution.py:231
  71.3 0.2 convert_reduce_fusion.1
  71.5 0.0 collective-permute-done.8.refs_8_
  71.5 1.9 %collective-permute-start.9 = (bf16[256,2048]{1,0:T(8,128)(2,1)S(1)}, bf16[256,2048]{1,0:T(8,128)(2,1)}, u32[]{:S(2)}, u32[]{:S(2)}) collective-permute-start(bf16[256,2048]{1,0:T(8,128)(2,1)S(1)} %collective-permute-done.8.refs_8_), channel_id=1, source_target_pairs={{0,8},{1,65},{8,16},{9,73},{16,24},{17,81},{24,32},{25,89},{32,40}... | collective-permute-start | bytes 3145736 | tf_op jit(solution)/shard_map/ppermute | solution.py:23
  73.4 0.0 collective-permute-done.5.refs_1_
  73.5 4.6 %collective-permute-start.6 = (bf16[256,2048]{1,0:T(8,128)(2,1)}, bf16[256,2048]{1,0:T(8,128)(2,1)}, u32[]{:S(2)}, u32[]{:S(2)}) collective-permute-start(bf16[256,2048]{1,0:T(8,128)(2,1)} %collective-permute-done.5.refs_1_), channel_id=1, source_target_pairs={{0,56},{1,449},{8,0},{9,457},{16,8},{17,465},{24,16},{25,473},{32,... | collective-permute-start | bytes 3145736 | tf_op jit(solution)/shard_map/ppermute | solution.py:23
  78.0 1.1 fusion.1
  79.2 0.1 fusion.3
  79.3 1.1 broadcast_in_dim.26
  80.4 3.5 %all-to-all-start.1 = ((bf16[4,64,2048]{2,1,0:T(8,128)(2,1)}), bf16[4,64,2048]{2,1,0:T(8,128)(2,1)S(1)}, u32[]{:S(2)}, u32[]{:S(2)}) async-start(bf16[4,64,2048]{2,1,0:T(8,128)(2,1)} %broadcast_in_dim.26), calls=%async_computation.1 | async-start | bytes 2097152 | tf_op jit(solution)/shard_map/all_to_all | solution.py:43
  84.0 4.6 %collective-permute-done.9.refs_7_ = bf16[256,2048]{1,0:T(8,128)(2,1)} collective-permute-done((bf16[256,2048]{1,0:T(8,128)(2,1)S(1)}, bf16[256,2048]{1,0:T(8,128)(2,1)}, u32[]{:S(2)}, u32[]{:S(2)}) %collective-permute-start.9) | collective-permute-done | bytes 1048608 | tf_op jit(solution)/shard_map/ppermute | solution.py:23
  88.6 1.9 %collective-permute-start.10 = (bf16[256,2048]{1,0:T(8,128)(2,1)}, bf16[256,2048]{1,0:T(8,128)(2,1)S(1)}, u32[]{:S(2)}, u32[]{:S(2)}) collective-permute-start(bf16[256,2048]{1,0:T(8,128)(2,1)} %collective-permute-done.9.refs_7_), channel_id=1, source_target_pairs={{0,8},{1,65},{8,16},{9,73},{16,24},{17,81},{24,32},{25,89},{32,40}... | collective-permute-start | bytes 3145736 | tf_op jit(solution)/shard_map/ppermute | solution.py:23
  90.5 0.0 collective-permute-done.6.refs_2_
  90.5 4.9 %collective-permute-start.7 = (bf16[256,2048]{1,0:T(8,128)(2,1)}, bf16[256,2048]{1,0:T(8,128)(2,1)}, u32[]{:S(2)}, u32[]{:S(2)}) collective-permute-start(bf16[256,2048]{1,0:T(8,128)(2,1)} %collective-permute-done.6.refs_2_), channel_id=1, source_target_pairs={{0,56},{1,449},{8,0},{9,457},{16,8},{17,465},{24,16},{25,473},{32,... | collective-permute-start | bytes 3145736 | tf_op jit(solution)/shard_map/ppermute | solution.py:23
  95.4 2.5 %all-to-all-done.1 = bf16[4,64,2048]{2,1,0:T(8,128)(2,1)S(1)} async-done(((bf16[4,64,2048]{2,1,0:T(8,128)(2,1)}), bf16[4,64,2048]{2,1,0:T(8,128)(2,1)S(1)}, u32[]{:S(2)}, u32[]{:S(2)}) %all-to-all-start.1) | async-done | bytes 1048608 | tf_op jit(solution)/shard_map/all_to_all | solution.py:43
  97.9 1.9 %collective-permute-start.4 = (bf16[256,2048]{1,0:T(8,128)(2,1)S(1)}, bf16[256,2048]{1,0:T(8,128)(2,1)}, u32[]{:S(2)}, u32[]{:S(2)}) collective-permute-start(bf16[256,2048]{1,0:T(8,128)(2,1)S(1)} %bitcast.25), channel_id=1, source_target_pairs={{0,1},{1,0},{2,3},{3,2},{4,5},{5,4},{6,7},{7,6},{8,9},{9,8},{10,11... | collective-permute-start | bytes 3145736 | tf_op jit(solution)/shard_map/ppermute | solution.py:38
  99.8 5.7 %collective-permute-done.10.refs_6_ = bf16[256,2048]{1,0:T(8,128)(2,1)S(1)} collective-permute-done((bf16[256,2048]{1,0:T(8,128)(2,1)}, bf16[256,2048]{1,0:T(8,128)(2,1)S(1)}, u32[]{:S(2)}, u32[]{:S(2)}) %collective-permute-start.10) | collective-permute-done | bytes 1048608 | tf_op jit(solution)/shard_map/ppermute | solution.py:23
  105.5 0.8 slice.18
  106.3 1.9 %collective-permute-start.11 = (bf16[128,2048]{1,0:T(8,128)(2,1)}, bf16[128,2048]{1,0:T(8,128)(2,1)}, u32[]{:S(2)}, u32[]{:S(2)}) collective-permute-start(bf16[128,2048]{1,0:T(8,128)(2,1)} %slice.18), channel_id=1, source_target_pairs={{0,8},{1,65},{8,16},{9,73},{16,24},{17,81},{24,32},{25,89},{32,40}... | collective-permute-start | bytes 1572872 | tf_op jit(solution)/shard_map/ppermute | solution.py:23
  108.3 0.0 collective-permute-done.7.refs_3_
  108.3 1.9 %slice.19 = bf16[128,2048]{1,0:T(8,128)(2,1)} slice(bf16[256,2048]{1,0:T(8,128)(2,1)} %collective-permute-done.7.refs_3_), slice={[128:256], [0:2048]} | slice | bytes 1048576 | tf_op jit(solution)/shard_map/slice | solution.py:224
  110.2 4.6 %collective-permute-start.12 = (bf16[128,2048]{1,0:T(8,128)(2,1)}, bf16[128,2048]{1,0:T(8,128)(2,1)}, u32[]{:S(2)}, u32[]{:S(2)}) collective-permute-start(bf16[128,2048]{1,0:T(8,128)(2,1)} %slice.19), channel_id=1, source_target_pairs={{0,56},{1,449},{8,0},{9,457},{16,8},{17,465},{24,16},{25,473},{32,... | collective-permute-start | bytes 1572872 | tf_op jit(solution)/shard_map/ppermute | solution.py:23
  114.8 0.1 pad_add_fusion.at_ref
  114.8 0.0 collective-permute-done.4.theirs_ref
  114.8 3.2 %collective-permute-done.11.refs_4_ = bf16[128,2048]{1,0:T(8,128)(2,1)} collective-permute-done((bf16[128,2048]{1,0:T(8,128)(2,1)}, bf16[128,2048]{1,0:T(8,128)(2,1)}, u32[]{:S(2)}, u32[]{:S(2)}) %collective-permute-start.11) | collective-permute-done | bytes 524320 | tf_op jit(solution)/shard_map/ppermute | solution.py:23
  118.1 3.1 %collective-permute-done.12.refs_5_ = bf16[128,2048]{1,0:T(8,128)(2,1)} collective-permute-done((bf16[128,2048]{1,0:T(8,128)(2,1)}, bf16[128,2048]{1,0:T(8,128)(2,1)}, u32[]{:S(2)}, u32[]{:S(2)}) %collective-permute-start.12) | collective-permute-done | bytes 524320 | tf_op jit(solution)/shard_map/ppermute | solution.py:23
  121.2 1.2 copy-done.1
  122.4 7.5 %mixer.1 = (bf16[2048,1024]{1,0:T(8,128)(2,1)}, bf16[256,1024]{1,0:T(8,128)(2,1)S(1)}, bf16[256,2048]{1,0:T(8,128)(2,1)S(1)}) custom-call(s32[3]{0:T(128)S(1)} %pad_add_fusion.at_ref, bf16[256,2048]{1,0:T(8,128)(2,1)} %collective-permute-done.4.theirs_ref, bf16[256,2048]{1,0:T(8,128)(2,1)S(1)} %bitcast.26, bf16[256,2048]{1,0:T(8,128)(2,1)S(1)} %bitcast.24, ...), custom_call_target="tpu_custom_call" | custom-call | flops 2147483648 | bytes 8388608 | tf_op jit(solution)/shard_map/mixer/pallas_call | solution.py:97
  129.9 2.7 %collective-permute-start.13 = (bf16[256,2048]{1,0:T(8,128)(2,1)S(1)}, bf16[256,2048]{1,0:T(8,128)(2,1)S(1)}, u32[]{:S(2)}, u32[]{:S(2)}) collective-permute-start(bf16[256,2048]{1,0:T(8,128)(2,1)S(1)} %get-tuple-element.18), channel_id=1, source_target_pairs={{0,1},{1,0},{2,3},{3,2},{4,5},{5,4},{6,7},{7,6},{8,9},{9,8},{10,11... | collective-permute-start | bytes 3145736 | tf_op jit(solution)/shard_map/ppermute | solution.py:38
  132.6 3.5 %fusion.7 = f32[256,2048]{1,0:T(8,128)S(1)} fusion(bf16[256,1024]{1,0:T(8,128)(2,1)S(1)} %get-tuple-element.16, bf16[2048,1024]{1,0:T(8,128)(2,1)} %get-tuple-element.17), kind=kOutput, calls=%fused_computation.24 | convolution fusion | flops 1073741824 | bytes 6815744 | tf_op jit(solution)/shard_map/dot_general | solution.py:249
  136.1 0.0 collective-permute-done.13
  136.1 0.3 add_convert_fusion
  136.4 17.3 %all_to_all.25 = bf16[4,64,2048]{2,1,0:T(8,128)(2,1)S(1)} all-to-all(bf16[4,64,2048]{2,1,0:T(8,128)(2,1)S(1)} %bitcast.29), channel_id=1, replica_groups=mesh['z'=8,'y'=8,'x'=4,'c'=2] {'x'}, dimensions={0} | all-to-all | bytes 2097152 | tf_op jit(solution)/shard_map/all_to_all | solution.py:53
  153.7 0.2 convert_reduce_fusion
  153.9 0.1 broadcast_in_dim.28
  154.0 16.5 %all_to_all.26 = bf16[4,64,2048]{2,1,0:T(8,128)(2,1)S(1)} all-to-all(bf16[4,64,2048]{2,1,0:T(8,128)(2,1)S(1)} %broadcast_in_dim.28), channel_id=1, replica_groups=mesh['z'=8,'y'=8,'x'=4,'c'=2] {'x'}, dimensions={0} | all-to-all | bytes 2097152 | tf_op jit(solution)/shard_map/all_to_all | solution.py:43
  170.5 3.9 %collective-permute-start.14 = (bf16[256,2048]{1,0:T(8,128)(2,1)S(1)}, bf16[256,2048]{1,0:T(8,128)(2,1)S(1)}, u32[]{:S(2)}, u32[]{:S(2)}) collective-permute-start(bf16[256,2048]{1,0:T(8,128)(2,1)S(1)} %bitcast.27), channel_id=1, source_target_pairs={{0,1},{1,0},{2,3},{3,2},{4,5},{5,4},{6,7},{7,6},{8,9},{9,8},{10,11... | collective-permute-start | bytes 3145736 | tf_op jit(solution)/shard_map/ppermute | solution.py:38
  174.4 2.3 %collective-permute-done.14 = bf16[256,2048]{1,0:T(8,128)(2,1)S(1)} collective-permute-done((bf16[256,2048]{1,0:T(8,128)(2,1)S(1)}, bf16[256,2048]{1,0:T(8,128)(2,1)S(1)}, u32[]{:S(2)}, u32[]{:S(2)}) %collective-permute-start.14) | collective-permute-done | bytes 1048608 | tf_op jit(solution)/shard_map/ppermute | solution.py:38
  176.7 0.2 broadcast_select_fusion.1
  176.9 1.6 pad_maximum_fusion
  (19 shorter events, 0.1 us)
Async XLA Ops:
  0.0 11.4 %copy-start.2 = (bf16[256,2048]{1,0:T(8,128)(2,1)S(1)}, bf16[256,2048]{1,0:T(8,128)(2,1)}, u32[]{:S(2)}) copy-start(bf16[256,2048]{1,0:T(8,128)(2,1)} %param.20) | copy-start | bytes 3145732
  0.0 23.3 %copy-start.6 = (f32[64]{0:T(128)S(1)}, f32[64]{0:T(128)}, u32[]{:S(2)}) copy-start(f32[64]{0:T(128)} %param.18) | copy-start | bytes 772
  1.7 24.6 %copy-start.4 = (bf16[16,512]{1,0:T(8,128)(2,1)}, bf16[16,512]{1,0:T(8,128)(2,1)S(1)}, u32[]{:S(2)}) copy-start(bf16[16,512]{1,0:T(8,128)(2,1)S(1)} %broadcast_in_dim.23.doc_ref) | copy-start | bytes 49156
  3.7 34.9 %all-to-all-start.2 = ((bf16[8,32,2048]{2,1,0:T(8,128)(2,1)}), bf16[8,32,2048]{2,1,0:T(8,128)(2,1)S(1)}, u32[]{:S(2)}, u32[]{:S(2)}) async-start(bf16[8,32,2048]{2,1,0:T(8,128)(2,1)} %broadcast_in_dim.27), calls=%async_computation.2 | async-start | bytes 2097152 | tf_op jit(solution)/shard_map/all_to_all | solution.py:30
  11.4 25.5 %collective-permute-start.3 = (bf16[256,2048]{1,0:T(8,128)(2,1)S(1)}, bf16[256,2048]{1,0:T(8,128)(2,1)S(1)}, u32[]{:S(2)}, u32[]{:S(2)}) collective-permute-start(bf16[256,2048]{1,0:T(8,128)(2,1)S(1)} %copy-done.2), channel_id=1, source_target_pairs={{0,1},{1,0},{2,3},{3,2},{4,5},{5,4},{6,7},{7,6},{8,9},{9,8},{10,11... | collective-permute-start | bytes 3145736 | tf_op jit(solution)/shard_map/ppermute | solution.py:38
  17.5 8.8 %collective-permute-start.1 = (bf16[144,128]{1,0:T(8,128)(2,1)S(1)}, bf16[144,128]{1,0:T(8,128)(2,1)S(1)}, u32[]{:S(2)}, u32[]{:S(2)}) collective-permute-start(bf16[144,128]{1,0:T(8,128)(2,1)S(1)} %get-tuple-element.23), channel_id=1, source_target_pairs={{8,0},{16,8},{24,16},{32,24},{40,32},{48,40},{56,48},{64,56},{72,6... | collective-permute-start | bytes 110600 | tf_op jit(solution)/shard_map/ppermute | solution.py:206
  18.8 7.5 %collective-permute-start = (bf16[144,128]{1,0:T(8,128)(2,1)S(1)}, bf16[144,128]{1,0:T(8,128)(2,1)S(1)}, u32[]{:S(2)}, u32[]{:S(2)}) collective-permute-start(bf16[144,128]{1,0:T(8,128)(2,1)S(1)} %get-tuple-element.24), channel_id=1, source_target_pairs={{0,8},{8,16},{16,24},{24,32},{32,40},{40,48},{48,56},{56,64},{64,7... | collective-permute-start | bytes 110600 | tf_op jit(solution)/shard_map/ppermute | solution.py:205
  26.3 0.6 copy-start.7
  26.3 0.6 copy-start.8
  33.3 18.8 %copy-start.3 = (bf16[256,256]{1,0:T(8,128)(2,1)S(1)}, bf16[256,256]{1,0:T(8,128)(2,1)}, u32[]{:S(2)}) copy-start(bf16[256,256]{1,0:T(8,128)(2,1)} %get-tuple-element.12) | copy-start | bytes 393220
  33.3 3.6 %collective-permute-start.2 = (bf16[256,256]{1,0:T(8,128)(2,1)}, bf16[256,256]{1,0:T(8,128)(2,1)S(1)}, u32[]{:S(2)}, u32[]{:S(2)}) collective-permute-start(bf16[256,256]{1,0:T(8,128)(2,1)} %get-tuple-element.13), channel_id=1, source_target_pairs={{0,1},{1,0},{2,3},{3,2},{4,5},{5,4},{6,7},{7,6},{8,9},{9,8},{10,11... | collective-permute-start | bytes 393224 | tf_op jit(solution)/shard_map/ppermute | solution.py:38
  38.6 32.9 %collective-permute-start.8 = (bf16[256,2048]{1,0:T(8,128)(2,1)S(1)}, bf16[256,2048]{1,0:T(8,128)(2,1)S(1)}, u32[]{:S(2)}, u32[]{:S(2)}) collective-permute-start(bf16[256,2048]{1,0:T(8,128)(2,1)S(1)} %bitcast.22), channel_id=1, source_target_pairs={{0,8},{1,65},{8,16},{9,73},{16,24},{17,81},{24,32},{25,89},{32,40}... | collective-permute-start | bytes 3145736 | tf_op jit(solution)/shard_map/ppermute | solution.py:23
  46.4 27.0 %collective-permute-start.5 = (bf16[256,2048]{1,0:T(8,128)(2,1)S(1)}, bf16[256,2048]{1,0:T(8,128)(2,1)}, u32[]{:S(2)}, u32[]{:S(2)}) collective-permute-start(bf16[256,2048]{1,0:T(8,128)(2,1)S(1)} %bitcast.23), channel_id=1, source_target_pairs={{0,56},{1,449},{8,0},{9,457},{16,8},{17,465},{24,16},{25,473},{32,... | collective-permute-start | bytes 3145736 | tf_op jit(solution)/shard_map/ppermute | solution.py:23
  55.5 23.7 %copy-start.5 = (f32[2048]{0:T(1024)S(1)}, f32[2048]{0:T(1024)}, u32[]{:S(2)}) copy-start(f32[2048]{0:T(1024)} %param.21) | copy-start | bytes 24580
  55.5 15.8 %all-to-all-start = ((bf16[4,64,2048]{2,1,0:T(8,128)(2,1)}), bf16[4,64,2048]{2,1,0:T(8,128)(2,1)S(1)}, u32[]{:S(2)}, u32[]{:S(2)}) async-start(bf16[4,64,2048]{2,1,0:T(8,128)(2,1)} %bitcast.28), calls=%async_computation | async-start | bytes 2097152 | tf_op jit(solution)/shard_map/all_to_all | solution.py:231
  71.5 8.9 %copy-start = (bf16[256,2048]{1,0:T(8,128)(2,1)}, bf16[256,2048]{1,0:T(8,128)(2,1)S(1)}, u32[]{:S(2)}) copy-start(bf16[256,2048]{1,0:T(8,128)(2,1)S(1)} %collective-permute-done.8.refs_8_) | copy-start | bytes 3145732
  71.5 17.0 %collective-permute-start.9 = (bf16[256,2048]{1,0:T(8,128)(2,1)S(1)}, bf16[256,2048]{1,0:T(8,128)(2,1)}, u32[]{:S(2)}, u32[]{:S(2)}) collective-permute-start(bf16[256,2048]{1,0:T(8,128)(2,1)S(1)} %collective-permute-done.8.refs_8_), channel_id=1, source_target_pairs={{0,8},{1,65},{8,16},{9,73},{16,24},{17,81},{24,32},{25,89},{32,40}... | collective-permute-start | bytes 3145736 | tf_op jit(solution)/shard_map/ppermute | solution.py:23
  73.5 17.0 %collective-permute-start.6 = (bf16[256,2048]{1,0:T(8,128)(2,1)}, bf16[256,2048]{1,0:T(8,128)(2,1)}, u32[]{:S(2)}, u32[]{:S(2)}) collective-permute-start(bf16[256,2048]{1,0:T(8,128)(2,1)} %collective-permute-done.5.refs_1_), channel_id=1, source_target_pairs={{0,56},{1,449},{8,0},{9,457},{16,8},{17,465},{24,16},{25,473},{32,... | collective-permute-start | bytes 3145736 | tf_op jit(solution)/shard_map/ppermute | solution.py:23
  80.4 17.4 %all-to-all-start.1 = ((bf16[4,64,2048]{2,1,0:T(8,128)(2,1)}), bf16[4,64,2048]{2,1,0:T(8,128)(2,1)S(1)}, u32[]{:S(2)}, u32[]{:S(2)}) async-start(bf16[4,64,2048]{2,1,0:T(8,128)(2,1)} %broadcast_in_dim.26), calls=%async_computation.1 | async-start | bytes 2097152 | tf_op jit(solution)/shard_map/all_to_all | solution.py:43
  88.6 17.0 %collective-permute-start.10 = (bf16[256,2048]{1,0:T(8,128)(2,1)}, bf16[256,2048]{1,0:T(8,128)(2,1)S(1)}, u32[]{:S(2)}, u32[]{:S(2)}) collective-permute-start(bf16[256,2048]{1,0:T(8,128)(2,1)} %collective-permute-done.9.refs_7_), channel_id=1, source_target_pairs={{0,8},{1,65},{8,16},{9,73},{16,24},{17,81},{24,32},{25,89},{32,40}... | collective-permute-start | bytes 3145736 | tf_op jit(solution)/shard_map/ppermute | solution.py:23
  90.5 17.8 %collective-permute-start.7 = (bf16[256,2048]{1,0:T(8,128)(2,1)}, bf16[256,2048]{1,0:T(8,128)(2,1)}, u32[]{:S(2)}, u32[]{:S(2)}) collective-permute-start(bf16[256,2048]{1,0:T(8,128)(2,1)} %collective-permute-done.6.refs_2_), channel_id=1, source_target_pairs={{0,56},{1,449},{8,0},{9,457},{16,8},{17,465},{24,16},{25,473},{32,... | collective-permute-start | bytes 3145736 | tf_op jit(solution)/shard_map/ppermute | solution.py:23
  97.9 17.0 %collective-permute-start.4 = (bf16[256,2048]{1,0:T(8,128)(2,1)S(1)}, bf16[256,2048]{1,0:T(8,128)(2,1)}, u32[]{:S(2)}, u32[]{:S(2)}) collective-permute-start(bf16[256,2048]{1,0:T(8,128)(2,1)S(1)} %bitcast.25), channel_id=1, source_target_pairs={{0,1},{1,0},{2,3},{3,2},{4,5},{5,4},{6,7},{7,6},{8,9},{9,8},{10,11... | collective-permute-start | bytes 3145736 | tf_op jit(solution)/shard_map/ppermute | solution.py:38
  106.3 11.7 %collective-permute-start.11 = (bf16[128,2048]{1,0:T(8,128)(2,1)}, bf16[128,2048]{1,0:T(8,128)(2,1)}, u32[]{:S(2)}, u32[]{:S(2)}) collective-permute-start(bf16[128,2048]{1,0:T(8,128)(2,1)} %slice.18), channel_id=1, source_target_pairs={{0,8},{1,65},{8,16},{9,73},{16,24},{17,81},{24,32},{25,89},{32,40}... | collective-permute-start | bytes 1572872 | tf_op jit(solution)/shard_map/ppermute | solution.py:23
  110.2 11.0 %collective-permute-start.12 = (bf16[128,2048]{1,0:T(8,128)(2,1)}, bf16[128,2048]{1,0:T(8,128)(2,1)}, u32[]{:S(2)}, u32[]{:S(2)}) collective-permute-start(bf16[128,2048]{1,0:T(8,128)(2,1)} %slice.19), channel_id=1, source_target_pairs={{0,56},{1,449},{8,0},{9,457},{16,8},{17,465},{24,16},{25,473},{32,... | collective-permute-start | bytes 1572872 | tf_op jit(solution)/shard_map/ppermute | solution.py:23
  121.2 1.2 copy-start.1
  129.9 6.2 %collective-permute-start.13 = (bf16[256,2048]{1,0:T(8,128)(2,1)S(1)}, bf16[256,2048]{1,0:T(8,128)(2,1)S(1)}, u32[]{:S(2)}, u32[]{:S(2)}) collective-permute-start(bf16[256,2048]{1,0:T(8,128)(2,1)S(1)} %get-tuple-element.18), channel_id=1, source_target_pairs={{0,1},{1,0},{2,3},{3,2},{4,5},{5,4},{6,7},{7,6},{8,9},{9,8},{10,11... | collective-permute-start | bytes 3145736 | tf_op jit(solution)/shard_map/ppermute | solution.py:38
  170.5 6.2 %collective-permute-start.14 = (bf16[256,2048]{1,0:T(8,128)(2,1)S(1)}, bf16[256,2048]{1,0:T(8,128)(2,1)S(1)}, u32[]{:S(2)}, u32[]{:S(2)}) collective-permute-start(bf16[256,2048]{1,0:T(8,128)(2,1)S(1)} %bitcast.27), channel_id=1, source_target_pairs={{0,1},{1,0},{2,3},{3,2},{4,5},{5,4},{6,7},{7,6},{8,9},{9,8},{10,11... | collective-permute-start | bytes 3145736 | tf_op jit(solution)/shard_map/ppermute | solution.py:38

commit v2 on v1

--- a/solution.py
+++ b/solution.py
@@ -23,15 +23,14 @@
     return lax.ppermute(x, ("z", "y", "c"), pairs)
 
 
-def across(x):
+def across(copies):
     nz, ny = lax.axis_size("z"), lax.axis_size("y")
     groups = [[2 * (z * ny + y) for z in range(nz)] for y in range(ny)]
     groups += [[2 * (z * ny + y) + 1 for y in range(ny)] for z in range(nz)]
     tiles = lax.all_to_all(
-        jnp.broadcast_to(x, (nz, *x.shape)),
-        ("z", "y", "c"), 0, 0, tiled=True, axis_index_groups=groups,
-    )
-    return tiles.reshape(nz * x.shape[0], x.shape[1])
+        copies, ("z", "y", "c"), 0, 0, tiled=True, axis_index_groups=groups
+    )
+    return tiles.reshape(-1, tiles.shape[2])
 
 
 def swap(x):
@@ -61,22 +60,16 @@
 
 def mixer_body(at_ref, theirs_ref, mine_ref, *refs):
     *pieces, down_ref, act_ref, out_ref, up_ref = refs
-    count = len(pieces) - 1
+    count = len(pieces)
     units = act_ref.shape[1]
-    cut = pieces[count // 2].shape[0]
-    chunk = 2 * cut // count
+    chunk = pieces[0].shape[0] // count
     for r in range(count):
         index = lax.rem(at_ref[0] + r, count)
         for j in range(count):
-            if r < count // 2:
-                source, low = pieces[r], j * chunk
-            elif r > count // 2:
-                source, low = pieces[r + 1], j * chunk
-            else:
-                source, low = pieces[r + j * chunk // cut], j * chunk % cut
+            rows = slice(j * chunk, (j + 1) * chunk)
             to = pl.multiple_of(j * at_ref[1] + index * at_ref[2], chunk)
-            up_ref[pl.ds(to, chunk), :] = source[low : low + chunk, :units]
-            down_ref[pl.ds(to, chunk), :] = source[low : low + chunk, units:]
+            up_ref[pl.ds(to, chunk), :] = pieces[r][rows, :units]
+            down_ref[pl.ds(to, chunk), :] = pieces[r][rows, units:]
 
     def hidden(rows):
         wide = jnp.dot(rows, up_ref[...], preferred_element_type=jnp.float32)
@@ -204,7 +197,8 @@
     onward = [(i, i + 1) for i in range(count - 1)]
     before = lax.ppermute(packed[:, rows - WINDOW :], SP, onward)
     after = lax.ppermute(packed[:, :WINDOW], SP, [(j, i) for i, j in onward])
-    piece = across(tie(jnp.concatenate([w_up, w_down.T], axis=1), packed))
+    both = tie(jnp.concatenate([w_up, w_down.T], axis=1), packed)
+    piece = across(jnp.broadcast_to(both, (lax.axis_size("z"), *both.shape)))
     w_out_other = swap(w_out)
 
     heads_all = heads_here * lax.axis_size(TP)
@@ -217,12 +211,11 @@
         q_gain[None, :], k_gain[:, None],
     )
     piece = tie(piece, att_send)
-    cut = piece.shape[0] // 2
     up1, dn1 = along(piece, 1), along(piece, -1)
     up2, dn2 = along(up1, 1), along(dn1, -1)
     up3, dn3 = along(up2, 1), along(dn2, -1)
-    up4, dn4 = along(up3[:cut], 1), along(dn3[cut:], -1)
-    pieces = [piece, dn1, dn2, dn3, up4, dn4, up3, up2, up1]
+    up4 = along(up3, 1)
+    pieces = [piece, dn1, dn2, dn3, up4, up3, up2, up1]
 
     att_other = swap(att_send)
     partial = jnp.dot(att_own, w_out, preferred_element_type=jnp.float32) + jnp.dot(
@@ -254,9 +247,11 @@
     unit_mix = scatter_x(joined)
     finished = spread((middle.astype(jnp.float32) + unit_mix).astype(jnp.bfloat16), "x")
     finished_other = swap(finished)
-    low = jnp.where(core == 0, finished, finished_other)
-    high = jnp.where(core == 0, finished_other, finished)
-    return jnp.concatenate([low, high], axis=0)
+    out = lax.dynamic_update_slice_in_dim(
+        jnp.zeros(resid.shape, resid.dtype), finished, core * half, 0
+    )
+    out = lax.optimization_barrier(out)
+    return lax.dynamic_update_slice_in_dim(out, finished_other, (1 - core) * half, 0)
 
 
 def solution(mesh):

time: 182 us -> 177 us (0.973); the launches traced: 178 us -> 176 us
  blocking collectives: 33.8 us -> 49.7 us
  waiting for transfers between devices: 36.9 us -> 30.7 us
  starting transfers between devices: 70.5 us -> 65.9 us
  local copies, waits for them, and re-layouts: 7.67 us -> 4.04 us
  matrix products: 8.61 us -> 6.58 us
    all_to_all x1 -> x2, blocking collectives: 16.5 us -> 32.6 us  [spread(): lax.all_to_all(jnp.broadcast_to(x, (n, *x.shape)), axis, 0, 0, tiled=True)]
    all_to_all x1, waiting for transfers between devices: 11.7 us -> 1.17 us  [shards(): lax.all_to_all(partial.astype(jnp.bfloat16).reshape(nx, share, -1), 'x',...]
    ppermute x8 -> x7, waiting for transfers between devices: 16.7 us -> 25.3 us  [along(): return lax.ppermute(x, ('z', 'y', 'c'), pairs)]
    all_to_all x2 -> x1, starting transfers between devices: 11.2 us -> 7.64 us  [across(): lax.all_to_all(copies, ('z', 'y', 'c'), 0, 0, tiled=True, axis_index_grou...]
    slice x2 -> x0, local copies, waits for them, and re-layouts: 2.74 us -> none  [shards(): up4, dn4 = (along(up3[:cut], 1), along(dn3[cut:], -1))]
    all_to_all x2 -> x1, waiting for transfers between devices: 2.48 us -> 0.01 us  [across(): lax.all_to_all(copies, ('z', 'y', 'c'), 0, 0, tiled=True, axis_index_grou...]
    ppermute x5, waiting for transfers between devices: 3.8 us -> 1.9 us  [swap(): return lax.ppermute(x, 'c', [(0, 1), (1, 0)])]
    ppermute x8 -> x7, starting transfers between devices: 33.2 us -> 32.5 us  [along(): return lax.ppermute(x, ('z', 'y', 'c'), pairs)]
  transfers between devices with their start and end apart: 18 -> 16, of which waited for: 9 -> 8; matrix products, arithmetic and copies ran while one was open for 9% -> 6% of each run, Pallas kernels for 4% -> 4%
where the time goes in v2:
time: 177 us; the launch traced here: 176 us
  starting transfers between devices  65.9 us (37%)
  blocking collectives  49.7 us (28%)
  waiting for transfers between devices  30.7 us (17%)
  Pallas kernels  14.2 us (8%)
  matrix products  6.58 us (4%)
  other arithmetic  5.08 us (3%)
  local copies, waits for them, and re-layouts  4.04 us (2%)
    all_to_all x2, blocking collectives, spread(): lax.all_to_all(jnp.broadcast_to(x, (n, *x.shape)), axis, 0, 0, tiled=True)  32.6 us
    ppermute x7, starting transfers between devices, along(): return lax.ppermute(x, ('z', 'y', 'c'), pairs)  32.5 us
    ppermute x7, waiting for transfers between devices, along(): return lax.ppermute(x, ('z', 'y', 'c'), pairs)  25.3 us
    all_to_all x1, blocking collectives, scatter_x(): lax.all_to_all(x.reshape(n, x.shape[0] // n, x.shape[1]), 'x', 0, 0, tile...  17.1 us
    ppermute x5, starting transfers between devices, swap(): return lax.ppermute(x, 'c', [(0, 1), (1, 0)])  16.3 us
    pallas_call x1, Pallas kernels, mixer(): pl.pallas_call(mixer_body, in_specs=[smem] + [vmem] * (2 + len(pieces)),...  7.8 us
    all_to_all x1, starting transfers between devices, across(): lax.all_to_all(copies, ('z', 'y', 'c'), 0, 0, tiled=True, axis_index_grou...  7.64 us
    pallas_call x1, Pallas kernels, attention(): pl.pallas_call(attention_body, in_specs=[smem] * 3 + [vmem] * 8, out_spec...  6.38 us
  transfers between devices with their start and end apart: 16, of which 8 were waited for; matrix products, arithmetic and copies ran while one was open for 6% of the time, Pallas kernels for 4%

profile of v2, /device:TPU:1, one launch (start us, length us, event | category | flops | bytes accessed | tf_op | source)
XLA Modules:
  0.0 176.5 jit_solution(17161448608581202490)
XLA Ops:
  0.0 0.7 add_convert_fusion.2
  0.7 0.9 pad_maximum_fusion.1
  1.6 0.0 copy-start.2
  1.6 0.9 pad_maximum_fusion
  2.5 1.1 broadcast_in_dim.31
  3.6 7.6 %all-to-all-start.2 = ((bf16[8,32,2048]{2,1,0:T(8,128)(2,1)}), bf16[8,32,2048]{2,1,0:T(8,128)(2,1)S(1)}, u32[]{:S(2)}, u32[]{:S(2)}) async-start(bf16[8,32,2048]{2,1,0:T(8,128)(2,1)} %broadcast_in_dim.31), calls=%async_computation.2 | async-start | bytes 2097152 | tf_op jit(solution)/shard_map/all_to_all | solution.py:30
  11.2 6.1 %collective-permute-start.3 = (bf16[256,2048]{1,0:T(8,128)(2,1)}, bf16[256,2048]{1,0:T(8,128)(2,1)S(1)}, u32[]{:S(2)}, u32[]{:S(2)}) collective-permute-start(bf16[256,2048]{1,0:T(8,128)(2,1)} %param.20), channel_id=1, source_target_pairs={{0,1},{1,0},{2,3},{3,2},{4,5},{5,4},{6,7},{7,6},{8,9},{9,8},{10,11... | collective-permute-start | bytes 3145736 | tf_op jit(solution)/shard_map/ppermute | solution.py:37
  17.3 1.3 collective-permute-start.1
  18.6 4.0 %collective-permute-start = (bf16[144,128]{1,0:T(8,128)(2,1)S(1)}, bf16[144,128]{1,0:T(8,128)(2,1)S(1)}, u32[]{:S(2)}, u32[]{:S(2)}) collective-permute-start(bf16[144,128]{1,0:T(8,128)(2,1)S(1)} %get-tuple-element.22), channel_id=1, source_target_pairs={{0,8},{8,16},{16,24},{24,32},{32,40},{40,48},{48,56},{56,64},{64,7... | collective-permute-start | bytes 110600 | tf_op jit(solution)/shard_map/ppermute | solution.py:198
  22.6 0.6 multiply_exponential_fusion.slope_ref
  23.2 0.0 copy-done.4
  23.2 0.7 copy.13.kg_ref
  23.9 2.2 %collective-permute-done.1.after_ref = bf16[144,128]{1,0:T(8,128)(2,1)S(1)} collective-permute-done((bf16[144,128]{1,0:T(8,128)(2,1)S(1)}, bf16[144,128]{1,0:T(8,128)(2,1)S(1)}, u32[]{:S(2)}, u32[]{:S(2)}) %collective-permute-start.1) | collective-permute-done | bytes 36896 | tf_op jit(solution)/shard_map/ppermute | solution.py:199
  26.2 0.0 collective-permute-done.before_ref
  26.2 0.0 copy-done.2
  26.2 0.6 copy-done.5
  26.8 0.0 copy-done.6
  26.8 6.4 %attend.1 = (bf16[256,256]{1,0:T(8,128)(2,1)}, bf16[256,256]{1,0:T(8,128)(2,1)}) custom-call(s32[1]{0:T(128)} %bitcast.core_ref, f32[4]{0:T(128)} %multiply_exponential_fusion.slope_ref, f32[4]{0:T(128)} %sink_ref.1, bf16[512,256]{1,0:T(8,128)(2,1)} %q_ref.1, bf16[64,512]{1,0:T(8,128)(2,1)} %bitcast.31, bf16[64,512]{1,0:T(8,128)(2,1)} %bitcast.33, ...), custom_call_target="tpu_custom_call" | custom-call | flops 2147483648 | bytes 1048576 | tf_op jit(solution)/shard_map/attend/pallas_call | solution.py:168
  33.2 2.0 %collective-permute-start.2 = (bf16[256,256]{1,0:T(8,128)(2,1)}, bf16[256,256]{1,0:T(8,128)(2,1)S(1)}, u32[]{:S(2)}, u32[]{:S(2)}) collective-permute-start(bf16[256,256]{1,0:T(8,128)(2,1)} %get-tuple-element.13), channel_id=1, source_target_pairs={{0,1},{1,0},{2,3},{3,2},{4,5},{5,4},{6,7},{7,6},{8,9},{9,8},{10,11... | collective-permute-start | bytes 393224 | tf_op jit(solution)/shard_map/ppermute | solution.py:37
  35.2 0.0 all-to-all-done.2
  35.2 8.1 %collective-permute-start.8 = (bf16[256,2048]{1,0:T(8,128)(2,1)S(1)}, bf16[256,2048]{1,0:T(8,128)(2,1)S(1)}, u32[]{:S(2)}, u32[]{:S(2)}) collective-permute-start(bf16[256,2048]{1,0:T(8,128)(2,1)S(1)} %bitcast.20), channel_id=1, source_target_pairs={{0,8},{1,65},{8,16},{9,73},{16,24},{17,81},{24,32},{25,89},{32,40}... | collective-permute-start | bytes 3145736 | tf_op jit(solution)/shard_map/ppermute | solution.py:23
  43.4 0.0 collective-permute-done.2
  43.4 0.0 collective-permute-done.3
  43.4 0.4 fusion.6
  43.8 0.0 copy-done.1
  43.8 2.7 %fusion = bf16[256,2048]{1,0:T(8,128)(2,1)} fusion(f32[256,2048]{1,0:T(8,128)S(1)} %fusion.6, bf16[256,256]{1,0:T(8,128)(2,1)S(1)} %copy-done.1, bf16[256,2048]{1,0:T(8,128)(2,1)} %param.20), kind=kOutput, calls=%fused_computation.1 | convolution fusion | flops 269484032 | bytes 4325376 | tf_op jit(solution)/shard_map/dot_general | solution.py:221
  46.5 4.1 %all-to-all-start = ((bf16[4,64,2048]{2,1,0:T(8,128)(2,1)}), bf16[4,64,2048]{2,1,0:T(8,128)(2,1)S(1)}, u32[]{:S(2)}, u32[]{:S(2)}) async-start(bf16[4,64,2048]{2,1,0:T(8,128)(2,1)} %bitcast.27), calls=%async_computation | async-start | bytes 2097152 | tf_op jit(solution)/shard_map/all_to_all | solution.py:224
  50.7 5.7 %collective-permute-start.5 = (bf16[256,2048]{1,0:T(8,128)(2,1)S(1)}, bf16[256,2048]{1,0:T(8,128)(2,1)}, u32[]{:S(2)}, u32[]{:S(2)}) collective-permute-start(bf16[256,2048]{1,0:T(8,128)(2,1)S(1)} %bitcast.21), channel_id=1, source_target_pairs={{0,56},{1,449},{8,0},{9,457},{16,8},{17,465},{24,16},{25,473},{32,... | collective-permute-start | bytes 3145736 | tf_op jit(solution)/shard_map/ppermute | solution.py:23
  56.4 3.3 %collective-permute-done.8.refs_7_ = bf16[256,2048]{1,0:T(8,128)(2,1)S(1)} collective-permute-done((bf16[256,2048]{1,0:T(8,128)(2,1)S(1)}, bf16[256,2048]{1,0:T(8,128)(2,1)S(1)}, u32[]{:S(2)}, u32[]{:S(2)}) %collective-permute-start.8) | collective-permute-done | bytes 1048608 | tf_op jit(solution)/shard_map/ppermute | solution.py:23
  59.6 1.9 %collective-permute-start.9 = (bf16[256,2048]{1,0:T(8,128)(2,1)S(1)}, bf16[256,2048]{1,0:T(8,128)(2,1)}, u32[]{:S(2)}, u32[]{:S(2)}) collective-permute-start(bf16[256,2048]{1,0:T(8,128)(2,1)S(1)} %collective-permute-done.8.refs_7_), channel_id=1, source_target_pairs={{0,8},{1,65},{8,16},{9,73},{16,24},{17,81},{24,32},{25,89},{32,40}... | collective-permute-start | bytes 3145736 | tf_op jit(solution)/shard_map/ppermute | solution.py:23
  61.6 1.2 all-to-all-done
  62.7 0.2 convert_reduce_fusion.1
  62.9 1.1 fusion.1
  64.1 4.1 %collective-permute-done.5.refs_1_ = bf16[256,2048]{1,0:T(8,128)(2,1)} collective-permute-done((bf16[256,2048]{1,0:T(8,128)(2,1)S(1)}, bf16[256,2048]{1,0:T(8,128)(2,1)}, u32[]{:S(2)}, u32[]{:S(2)}) %collective-permute-start.5) | collective-permute-done | bytes 1048608 | tf_op jit(solution)/shard_map/ppermute | solution.py:23
  68.1 5.4 %collective-permute-start.6 = (bf16[256,2048]{1,0:T(8,128)(2,1)}, bf16[256,2048]{1,0:T(8,128)(2,1)}, u32[]{:S(2)}, u32[]{:S(2)}) collective-permute-start(bf16[256,2048]{1,0:T(8,128)(2,1)} %collective-permute-done.5.refs_1_), channel_id=1, source_target_pairs={{0,56},{1,449},{8,0},{9,457},{16,8},{17,465},{24,16},{25,473},{32,... | collective-permute-start | bytes 3145736 | tf_op jit(solution)/shard_map/ppermute | solution.py:23
  73.5 3.0 %collective-permute-done.9.refs_6_ = bf16[256,2048]{1,0:T(8,128)(2,1)} collective-permute-done((bf16[256,2048]{1,0:T(8,128)(2,1)S(1)}, bf16[256,2048]{1,0:T(8,128)(2,1)}, u32[]{:S(2)}, u32[]{:S(2)}) %collective-permute-start.9) | collective-permute-done | bytes 1048608 | tf_op jit(solution)/shard_map/ppermute | solution.py:23
  76.5 1.9 %collective-permute-start.10 = (bf16[256,2048]{1,0:T(8,128)(2,1)}, bf16[256,2048]{1,0:T(8,128)(2,1)}, u32[]{:S(2)}, u32[]{:S(2)}) collective-permute-start(bf16[256,2048]{1,0:T(8,128)(2,1)} %collective-permute-done.9.refs_6_), channel_id=1, source_target_pairs={{0,8},{1,65},{8,16},{9,73},{16,24},{17,81},{24,32},{25,89},{32,40}... | collective-permute-start | bytes 3145736 | tf_op jit(solution)/shard_map/ppermute | solution.py:23
  78.4 0.1 fusion.3
  78.6 0.1 broadcast_in_dim.30
  78.7 16.6 %all_to_all.25 = bf16[4,64,2048]{2,1,0:T(8,128)(2,1)S(1)} all-to-all(bf16[4,64,2048]{2,1,0:T(8,128)(2,1)S(1)} %broadcast_in_dim.30), channel_id=1, replica_groups=mesh['z'=8,'y'=8,'x'=4,'c'=2] {'x'}, dimensions={0} | all-to-all | bytes 2097152 | tf_op jit(solution)/shard_map/all_to_all | solution.py:42
  95.3 1.9 %collective-permute-start.4 = (bf16[256,2048]{1,0:T(8,128)(2,1)S(1)}, bf16[256,2048]{1,0:T(8,128)(2,1)}, u32[]{:S(2)}, u32[]{:S(2)}) collective-permute-start(bf16[256,2048]{1,0:T(8,128)(2,1)S(1)} %bitcast.23), channel_id=1, source_target_pairs={{0,1},{1,0},{2,3},{3,2},{4,5},{5,4},{6,7},{7,6},{8,9},{9,8},{10,11... | collective-permute-start | bytes 3145736 | tf_op jit(solution)/shard_map/ppermute | solution.py:37
  97.2 0.0 collective-permute-done.6.refs_2_
  97.3 7.5 %collective-permute-start.7 = (bf16[256,2048]{1,0:T(8,128)(2,1)}, bf16[256,2048]{1,0:T(8,128)(2,1)}, u32[]{:S(2)}, u32[]{:S(2)}) collective-permute-start(bf16[256,2048]{1,0:T(8,128)(2,1)} %collective-permute-done.6.refs_2_), channel_id=1, source_target_pairs={{0,56},{1,449},{8,0},{9,457},{16,8},{17,465},{24,16},{25,473},{32,... | collective-permute-start | bytes 3145736 | tf_op jit(solution)/shard_map/ppermute | solution.py:23
  104.7 0.0 collective-permute-done.10.refs_5_
  104.8 1.9 %collective-permute-start.11 = (bf16[256,2048]{1,0:T(8,128)(2,1)}, bf16[256,2048]{1,0:T(8,128)(2,1)}, u32[]{:S(2)}, u32[]{:S(2)}) collective-permute-start(bf16[256,2048]{1,0:T(8,128)(2,1)} %collective-permute-done.10.refs_5_), channel_id=1, source_target_pairs={{0,8},{1,65},{8,16},{9,73},{16,24},{17,81},{24,32},{25,89},{32,40}... | collective-permute-start | bytes 3145736 | tf_op jit(solution)/shard_map/ppermute | solution.py:23
  106.7 0.1 pad_add_fusion.at_ref
  106.8 0.0 collective-permute-done.4.theirs_ref
  106.8 10.0 %collective-permute-done.7.refs_3_ = bf16[256,2048]{1,0:T(8,128)(2,1)} collective-permute-done((bf16[256,2048]{1,0:T(8,128)(2,1)}, bf16[256,2048]{1,0:T(8,128)(2,1)}, u32[]{:S(2)}, u32[]{:S(2)}) %collective-permute-start.7) | collective-permute-done | bytes 1048608 | tf_op jit(solution)/shard_map/ppermute | solution.py:23
  116.8 5.0 %collective-permute-done.11.refs_4_ = bf16[256,2048]{1,0:T(8,128)(2,1)} collective-permute-done((bf16[256,2048]{1,0:T(8,128)(2,1)}, bf16[256,2048]{1,0:T(8,128)(2,1)}, u32[]{:S(2)}, u32[]{:S(2)}) %collective-permute-start.11) | collective-permute-done | bytes 1048608 | tf_op jit(solution)/shard_map/ppermute | solution.py:23
  121.8 7.8 %mixer.1 = (bf16[2048,1024]{1,0:T(8,128)(2,1)}, bf16[256,1024]{1,0:T(8,128)(2,1)S(1)}, bf16[256,2048]{1,0:T(8,128)(2,1)S(1)}) custom-call(s32[3]{0:T(128)S(1)} %pad_add_fusion.at_ref, bf16[256,2048]{1,0:T(8,128)(2,1)} %collective-permute-done.4.theirs_ref, bf16[256,2048]{1,0:T(8,128)(2,1)S(1)} %bitcast.24, bf16[256,2048]{1,0:T(8,128)(2,1)S(1)} %bitcast.22, ...), custom_call_target="tpu_custom_call" | custom-call | flops 2147483648 | bytes 8388608 | tf_op jit(solution)/shard_map/mixer/pallas_call | solution.py:90
  129.6 1.9 %collective-permute-start.12 = (bf16[256,2048]{1,0:T(8,128)(2,1)S(1)}, bf16[256,2048]{1,0:T(8,128)(2,1)S(1)}, u32[]{:S(2)}, u32[]{:S(2)}) collective-permute-start(bf16[256,2048]{1,0:T(8,128)(2,1)S(1)} %get-tuple-element.18), channel_id=1, source_target_pairs={{0,1},{1,0},{2,3},{3,2},{4,5},{5,4},{6,7},{7,6},{8,9},{9,8},{10,11... | collective-permute-start | bytes 3145736 | tf_op jit(solution)/shard_map/ppermute | solution.py:37
  131.5 3.5 %fusion.7 = f32[256,2048]{1,0:T(8,128)S(1)} fusion(bf16[256,1024]{1,0:T(8,128)(2,1)S(1)} %get-tuple-element.16, bf16[2048,1024]{1,0:T(8,128)(2,1)} %get-tuple-element.17), kind=kOutput, calls=%fused_computation.23 | convolution fusion | flops 1073741824 | bytes 6815744 | tf_op jit(solution)/shard_map/dot_general | solution.py:242
  135.0 0.0 collective-permute-done.12
  135.0 0.3 add_convert_fusion
  135.4 17.1 %all_to_all.26 = bf16[4,64,2048]{2,1,0:T(8,128)(2,1)S(1)} all-to-all(bf16[4,64,2048]{2,1,0:T(8,128)(2,1)S(1)} %bitcast.28), channel_id=1, replica_groups=mesh['z'=8,'y'=8,'x'=4,'c'=2] {'x'}, dimensions={0} | all-to-all | bytes 2097152 | tf_op jit(solution)/shard_map/all_to_all | solution.py:52
  152.5 0.2 convert_reduce_fusion
  152.7 0.1 broadcast_in_dim.32
  152.8 16.0 %all_to_all.27 = bf16[4,64,2048]{2,1,0:T(8,128)(2,1)S(1)} all-to-all(bf16[4,64,2048]{2,1,0:T(8,128)(2,1)S(1)} %broadcast_in_dim.32), channel_id=1, replica_groups=mesh['z'=8,'y'=8,'x'=4,'c'=2] {'x'}, dimensions={0} | all-to-all | bytes 2097152 | tf_op jit(solution)/shard_map/all_to_all | solution.py:42
  168.8 4.4 %collective-permute-start.13 = (bf16[256,2048]{1,0:T(8,128)(2,1)S(1)}, bf16[256,2048]{1,0:T(8,128)(2,1)S(1)}, u32[]{:S(2)}, u32[]{:S(2)}) collective-permute-start(bf16[256,2048]{1,0:T(8,128)(2,1)S(1)} %bitcast.25), channel_id=1, source_target_pairs={{0,1},{1,0},{2,3},{3,2},{4,5},{5,4},{6,7},{7,6},{8,9},{9,8},{10,11... | collective-permute-start | bytes 3145736 | tf_op jit(solution)/shard_map/ppermute | solution.py:37
  173.2 0.2 broadcast_in_dim.26
  173.4 0.1 constant_dynamic-update-slice_fusion.1
  173.5 0.0 copy-start
  173.6 1.9 %collective-permute-done.13 = bf16[256,2048]{1,0:T(8,128)(2,1)S(1)} collective-permute-done((bf16[256,2048]{1,0:T(8,128)(2,1)S(1)}, bf16[256,2048]{1,0:T(8,128)(2,1)S(1)}, u32[]{:S(2)}, u32[]{:S(2)}) %collective-permute-start.13) | collective-permute-done | bytes 1048608 | tf_op jit(solution)/shard_map/ppermute | solution.py:37
  175.4 1.0 constant_dynamic-update-slice_fusion
  (11 shorter events, 0.1 us)
Async XLA Ops:
  0.0 23.2 %copy-start.4 = (f32[64]{0:T(128)S(1)}, f32[64]{0:T(128)}, u32[]{:S(2)}) copy-start(f32[64]{0:T(128)} %param.18) | copy-start | bytes 772
  1.6 24.6 %copy-start.2 = (bf16[16,512]{1,0:T(8,128)(2,1)}, bf16[16,512]{1,0:T(8,128)(2,1)S(1)}, u32[]{:S(2)}) copy-start(bf16[16,512]{1,0:T(8,128)(2,1)S(1)} %broadcast_in_dim.27.doc_ref) | copy-start | bytes 49156
  3.6 31.6 %all-to-all-start.2 = ((bf16[8,32,2048]{2,1,0:T(8,128)(2,1)}), bf16[8,32,2048]{2,1,0:T(8,128)(2,1)S(1)}, u32[]{:S(2)}, u32[]{:S(2)}) async-start(bf16[8,32,2048]{2,1,0:T(8,128)(2,1)} %broadcast_in_dim.31), calls=%async_computation.2 | async-start | bytes 2097152 | tf_op jit(solution)/shard_map/all_to_all | solution.py:30
  11.2 32.2 %collective-permute-start.3 = (bf16[256,2048]{1,0:T(8,128)(2,1)}, bf16[256,2048]{1,0:T(8,128)(2,1)S(1)}, u32[]{:S(2)}, u32[]{:S(2)}) collective-permute-start(bf16[256,2048]{1,0:T(8,128)(2,1)} %param.20), channel_id=1, source_target_pairs={{0,1},{1,0},{2,3},{3,2},{4,5},{5,4},{6,7},{7,6},{8,9},{9,8},{10,11... | collective-permute-start | bytes 3145736 | tf_op jit(solution)/shard_map/ppermute | solution.py:37
  17.3 8.8 %collective-permute-start.1 = (bf16[144,128]{1,0:T(8,128)(2,1)S(1)}, bf16[144,128]{1,0:T(8,128)(2,1)S(1)}, u32[]{:S(2)}, u32[]{:S(2)}) collective-permute-start(bf16[144,128]{1,0:T(8,128)(2,1)S(1)} %get-tuple-element.21), channel_id=1, source_target_pairs={{8,0},{16,8},{24,16},{32,24},{40,32},{48,40},{56,48},{64,56},{72,6... | collective-permute-start | bytes 110600 | tf_op jit(solution)/shard_map/ppermute | solution.py:199
  18.6 7.5 %collective-permute-start = (bf16[144,128]{1,0:T(8,128)(2,1)S(1)}, bf16[144,128]{1,0:T(8,128)(2,1)S(1)}, u32[]{:S(2)}, u32[]{:S(2)}) collective-permute-start(bf16[144,128]{1,0:T(8,128)(2,1)S(1)} %get-tuple-element.22), channel_id=1, source_target_pairs={{0,8},{8,16},{16,24},{24,32},{32,40},{40,48},{48,56},{56,64},{64,7... | collective-permute-start | bytes 110600 | tf_op jit(solution)/shard_map/ppermute | solution.py:198
  26.2 0.6 copy-start.5
  26.2 0.6 copy-start.6
  33.2 10.7 %copy-start.1 = (bf16[256,256]{1,0:T(8,128)(2,1)S(1)}, bf16[256,256]{1,0:T(8,128)(2,1)}, u32[]{:S(2)}) copy-start(bf16[256,256]{1,0:T(8,128)(2,1)} %get-tuple-element.12) | copy-start | bytes 393220
  33.2 10.2 %collective-permute-start.2 = (bf16[256,256]{1,0:T(8,128)(2,1)}, bf16[256,256]{1,0:T(8,128)(2,1)S(1)}, u32[]{:S(2)}, u32[]{:S(2)}) collective-permute-start(bf16[256,256]{1,0:T(8,128)(2,1)} %get-tuple-element.13), channel_id=1, source_target_pairs={{0,1},{1,0},{2,3},{3,2},{4,5},{5,4},{6,7},{7,6},{8,9},{9,8},{10,11... | collective-permute-start | bytes 393224 | tf_op jit(solution)/shard_map/ppermute | solution.py:37
  35.2 24.4 %collective-permute-start.8 = (bf16[256,2048]{1,0:T(8,128)(2,1)S(1)}, bf16[256,2048]{1,0:T(8,128)(2,1)S(1)}, u32[]{:S(2)}, u32[]{:S(2)}) collective-permute-start(bf16[256,2048]{1,0:T(8,128)(2,1)S(1)} %bitcast.20), channel_id=1, source_target_pairs={{0,8},{1,65},{8,16},{9,73},{16,24},{17,81},{24,32},{25,89},{32,40}... | collective-permute-start | bytes 3145736 | tf_op jit(solution)/shard_map/ppermute | solution.py:23
  46.5 31.9 %copy-start.3 = (f32[2048]{0:T(1024)S(1)}, f32[2048]{0:T(1024)}, u32[]{:S(2)}) copy-start(f32[2048]{0:T(1024)} %param.21) | copy-start | bytes 24580
  46.5 16.2 %all-to-all-start = ((bf16[4,64,2048]{2,1,0:T(8,128)(2,1)}), bf16[4,64,2048]{2,1,0:T(8,128)(2,1)S(1)}, u32[]{:S(2)}, u32[]{:S(2)}) async-start(bf16[4,64,2048]{2,1,0:T(8,128)(2,1)} %bitcast.27), calls=%async_computation | async-start | bytes 2097152 | tf_op jit(solution)/shard_map/all_to_all | solution.py:224
  50.7 17.4 %collective-permute-start.5 = (bf16[256,2048]{1,0:T(8,128)(2,1)S(1)}, bf16[256,2048]{1,0:T(8,128)(2,1)}, u32[]{:S(2)}, u32[]{:S(2)}) collective-permute-start(bf16[256,2048]{1,0:T(8,128)(2,1)S(1)} %bitcast.21), channel_id=1, source_target_pairs={{0,56},{1,449},{8,0},{9,457},{16,8},{17,465},{24,16},{25,473},{32,... | collective-permute-start | bytes 3145736 | tf_op jit(solution)/shard_map/ppermute | solution.py:23
  59.6 16.8 %collective-permute-start.9 = (bf16[256,2048]{1,0:T(8,128)(2,1)S(1)}, bf16[256,2048]{1,0:T(8,128)(2,1)}, u32[]{:S(2)}, u32[]{:S(2)}) collective-permute-start(bf16[256,2048]{1,0:T(8,128)(2,1)S(1)} %collective-permute-done.8.refs_7_), channel_id=1, source_target_pairs={{0,8},{1,65},{8,16},{9,73},{16,24},{17,81},{24,32},{25,89},{32,40}... | collective-permute-start | bytes 3145736 | tf_op jit(solution)/shard_map/ppermute | solution.py:23
  68.1 29.1 %collective-permute-start.6 = (bf16[256,2048]{1,0:T(8,128)(2,1)}, bf16[256,2048]{1,0:T(8,128)(2,1)}, u32[]{:S(2)}, u32[]{:S(2)}) collective-permute-start(bf16[256,2048]{1,0:T(8,128)(2,1)} %collective-permute-done.5.refs_1_), channel_id=1, source_target_pairs={{0,56},{1,449},{8,0},{9,457},{16,8},{17,465},{24,16},{25,473},{32,... | collective-permute-start | bytes 3145736 | tf_op jit(solution)/shard_map/ppermute | solution.py:23
  76.5 28.2 %collective-permute-start.10 = (bf16[256,2048]{1,0:T(8,128)(2,1)}, bf16[256,2048]{1,0:T(8,128)(2,1)}, u32[]{:S(2)}, u32[]{:S(2)}) collective-permute-start(bf16[256,2048]{1,0:T(8,128)(2,1)} %collective-permute-done.9.refs_6_), channel_id=1, source_target_pairs={{0,8},{1,65},{8,16},{9,73},{16,24},{17,81},{24,32},{25,89},{32,40}... | collective-permute-start | bytes 3145736 | tf_op jit(solution)/shard_map/ppermute | solution.py:23
  95.3 11.5 %collective-permute-start.4 = (bf16[256,2048]{1,0:T(8,128)(2,1)S(1)}, bf16[256,2048]{1,0:T(8,128)(2,1)}, u32[]{:S(2)}, u32[]{:S(2)}) collective-permute-start(bf16[256,2048]{1,0:T(8,128)(2,1)S(1)} %bitcast.23), channel_id=1, source_target_pairs={{0,1},{1,0},{2,3},{3,2},{4,5},{5,4},{6,7},{7,6},{8,9},{9,8},{10,11... | collective-permute-start | bytes 3145736 | tf_op jit(solution)/shard_map/ppermute | solution.py:37
  97.3 19.5 %collective-permute-start.7 = (bf16[256,2048]{1,0:T(8,128)(2,1)}, bf16[256,2048]{1,0:T(8,128)(2,1)}, u32[]{:S(2)}, u32[]{:S(2)}) collective-permute-start(bf16[256,2048]{1,0:T(8,128)(2,1)} %collective-permute-done.6.refs_2_), channel_id=1, source_target_pairs={{0,56},{1,449},{8,0},{9,457},{16,8},{17,465},{24,16},{25,473},{32,... | collective-permute-start | bytes 3145736 | tf_op jit(solution)/shard_map/ppermute | solution.py:23
  104.8 17.1 %collective-permute-start.11 = (bf16[256,2048]{1,0:T(8,128)(2,1)}, bf16[256,2048]{1,0:T(8,128)(2,1)}, u32[]{:S(2)}, u32[]{:S(2)}) collective-permute-start(bf16[256,2048]{1,0:T(8,128)(2,1)} %collective-permute-done.10.refs_5_), channel_id=1, source_target_pairs={{0,8},{1,65},{8,16},{9,73},{16,24},{17,81},{24,32},{25,89},{32,40}... | collective-permute-start | bytes 3145736 | tf_op jit(solution)/shard_map/ppermute | solution.py:23
  129.6 5.4 %collective-permute-start.12 = (bf16[256,2048]{1,0:T(8,128)(2,1)S(1)}, bf16[256,2048]{1,0:T(8,128)(2,1)S(1)}, u32[]{:S(2)}, u32[]{:S(2)}) collective-permute-start(bf16[256,2048]{1,0:T(8,128)(2,1)S(1)} %get-tuple-element.18), channel_id=1, source_target_pairs={{0,1},{1,0},{2,3},{3,2},{4,5},{5,4},{6,7},{7,6},{8,9},{9,8},{10,11... | collective-permute-start | bytes 3145736 | tf_op jit(solution)/shard_map/ppermute | solution.py:37
  168.8 6.7 %collective-permute-start.13 = (bf16[256,2048]{1,0:T(8,128)(2,1)S(1)}, bf16[256,2048]{1,0:T(8,128)(2,1)S(1)}, u32[]{:S(2)}, u32[]{:S(2)}) collective-permute-start(bf16[256,2048]{1,0:T(8,128)(2,1)S(1)} %bitcast.25), channel_id=1, source_target_pairs={{0,1},{1,0},{2,3},{3,2},{4,5},{5,4},{6,7},{7,6},{8,9},{9,8},{10,11... | collective-permute-start | bytes 3145736 | tf_op jit(solution)/shard_map/ppermute | solution.py:37
  173.5 1.9 %copy-start = (bf16[512,2048]{1,0:T(8,128)(2,1)}, bf16[512,2048]{1,0:T(8,128)(2,1)S(1)}, u32[]{:S(2)}) copy-start(bf16[512,2048]{1,0:T(8,128)(2,1)S(1)} %constant_dynamic-update-slice_fusion.1) | copy-start | bytes 6291460

commit v3 on v1

--- a/solution.py
+++ b/solution.py
@@ -23,15 +23,14 @@
     return lax.ppermute(x, ("z", "y", "c"), pairs)
 
 
-def across(x):
+def across(copies):
     nz, ny = lax.axis_size("z"), lax.axis_size("y")
     groups = [[2 * (z * ny + y) for z in range(nz)] for y in range(ny)]
     groups += [[2 * (z * ny + y) + 1 for y in range(ny)] for z in range(nz)]
     tiles = lax.all_to_all(
-        jnp.broadcast_to(x, (nz, *x.shape)),
-        ("z", "y", "c"), 0, 0, tiled=True, axis_index_groups=groups,
-    )
-    return tiles.reshape(nz * x.shape[0], x.shape[1])
+        copies, ("z", "y", "c"), 0, 0, tiled=True, axis_index_groups=groups
+    )
+    return tiles.reshape(-1, tiles.shape[2])
 
 
 def swap(x):
@@ -42,10 +41,6 @@
     n = lax.axis_size(axis)
     tiles = lax.all_to_all(jnp.broadcast_to(x, (n, *x.shape)), axis, 0, 0, tiled=True)
     return tiles.reshape(n * x.shape[0], x.shape[1])
-
-
-def tie(x, y):
-    return lax.optimization_barrier((x, y))[0]
 
 
 def scatter_x(x):
@@ -204,7 +199,8 @@
     onward = [(i, i + 1) for i in range(count - 1)]
     before = lax.ppermute(packed[:, rows - WINDOW :], SP, onward)
     after = lax.ppermute(packed[:, :WINDOW], SP, [(j, i) for i, j in onward])
-    piece = across(tie(jnp.concatenate([w_up, w_down.T], axis=1), packed))
+    both = jnp.concatenate([w_up, w_down.T], axis=1)
+    piece = across(jnp.broadcast_to(both, (lax.axis_size("z"), *both.shape)))
     w_out_other = swap(w_out)
 
     heads_all = heads_here * lax.axis_size(TP)
@@ -216,7 +212,6 @@
         core.astype(jnp.int32).reshape(1), slopes, sink, queries, kt, vt, doc, before, after,
         q_gain[None, :], k_gain[:, None],
     )
-    piece = tie(piece, att_send)
     cut = piece.shape[0] // 2
     up1, dn1 = along(piece, 1), along(piece, -1)
     up2, dn2 = along(up1, 1), along(dn1, -1)
@@ -254,9 +249,11 @@
     unit_mix = scatter_x(joined)
     finished = spread((middle.astype(jnp.float32) + unit_mix).astype(jnp.bfloat16), "x")
     finished_other = swap(finished)
-    low = jnp.where(core == 0, finished, finished_other)
-    high = jnp.where(core == 0, finished_other, finished)
-    return jnp.concatenate([low, high], axis=0)
+    out = lax.dynamic_update_slice_in_dim(
+        jnp.zeros(resid.shape, resid.dtype), finished, core * half, 0
+    )
+    out = lax.optimization_barrier(out)
+    return lax.dynamic_update_slice_in_dim(out, finished_other, (1 - core) * half, 0)
 
 
 def solution(mesh):

time: 182 us -> 179 us (0.984)
  other arithmetic: 6.87 us -> 3.52 us
where the time goes in v3:
time: 179 us; the launch traced here: 176 us
  starting transfers between devices  70.5 us (39%)
  waiting for transfers between devices  36.5 us (20%)
  blocking collectives  33.8 us (19%)
  Pallas kernels  13.9 us (8%)
  local copies, waits for them, and re-layouts  8.99 us (5%)
  matrix products  8.59 us (5%)
  other arithmetic  3.52 us (2%)
    ppermute x8, starting transfers between devices, along(): return lax.ppermute(x, ('z', 'y', 'c'), pairs)  33.3 us
    all_to_all x1, blocking collectives, scatter_x(): lax.all_to_all(x.reshape(n, x.shape[0] // n, x.shape[1]), 'x', 0, 0, tile...  17.3 us
    ppermute x5, starting transfers between devices, swap(): return lax.ppermute(x, 'c', [(0, 1), (1, 0)])  16.7 us
    ppermute x8, waiting for transfers between devices, along(): return lax.ppermute(x, ('z', 'y', 'c'), pairs)  16.6 us
    all_to_all x1, blocking collectives, spread(): lax.all_to_all(jnp.broadcast_to(x, (n, *x.shape)), axis, 0, 0, tiled=True)  16.5 us
    all_to_all x1, waiting for transfers between devices, shards(): lax.all_to_all(partial.astype(jnp.bfloat16).reshape(nx, share, -1), 'x',...  11.7 us
    all_to_all x1, starting transfers between devices, across(): lax.all_to_all(copies, ('z', 'y', 'c'), 0, 0, tiled=True, axis_index_grou...  7.64 us
    pallas_call x1, Pallas kernels, mixer(): pl.pallas_call(mixer_body, in_specs=[smem] + [vmem] * (2 + len(pieces)),...  7.52 us
  transfers between devices with their start and end apart: 18, of which 9 were waited for; matrix products, arithmetic and copies ran while one was open for 9% of the time, Pallas kernels for 4%

profile of v3, /device:TPU:1, one launch (start us, length us, event | category | flops | bytes accessed | tf_op | source)
XLA Modules:
  0.0 176.2 jit_solution(8845007323994954004)
XLA Ops:
  0.0 0.0 copy-start.5
  0.0 1.0 pad_maximum_fusion
  1.0 1.1 broadcast_in_dim.31
  2.1 7.6 %all-to-all-start.2 = ((bf16[8,32,2048]{2,1,0:T(8,128)(2,1)}), bf16[8,32,2048]{2,1,0:T(8,128)(2,1)S(1)}, u32[]{:S(2)}, u32[]{:S(2)}) async-start(bf16[8,32,2048]{2,1,0:T(8,128)(2,1)} %broadcast_in_dim.31), calls=%async_computation.2 | async-start | bytes 2097152 | tf_op jit(solution)/shard_map/all_to_all | solution.py:30
  9.8 6.1 %collective-permute-start.3 = (bf16[256,2048]{1,0:T(8,128)(2,1)S(1)}, bf16[256,2048]{1,0:T(8,128)(2,1)S(1)}, u32[]{:S(2)}, u32[]{:S(2)}) collective-permute-start(bf16[256,2048]{1,0:T(8,128)(2,1)S(1)} %copy-done.3), channel_id=1, source_target_pairs={{0,1},{1,0},{2,3},{3,2},{4,5},{5,4},{6,7},{7,6},{8,9},{9,8},{10,11... | collective-permute-start | bytes 3145736 | tf_op jit(solution)/shard_map/ppermute | solution.py:37
  15.9 1.3 collective-permute-start.1
  17.2 4.0 %collective-permute-start = (bf16[144,128]{1,0:T(8,128)(2,1)S(1)}, bf16[144,128]{1,0:T(8,128)(2,1)S(1)}, u32[]{:S(2)}, u32[]{:S(2)}) collective-permute-start(bf16[144,128]{1,0:T(8,128)(2,1)S(1)} %get-tuple-element.18), channel_id=1, source_target_pairs={{0,8},{8,16},{16,24},{24,32},{32,40},{40,48},{48,56},{56,64},{64,7... | collective-permute-start | bytes 110600 | tf_op jit(solution)/shard_map/ppermute | solution.py:200
  21.2 0.5 multiply_exponential_fusion.slope_ref
  21.8 0.7 copy.13.kg_ref
  22.5 2.2 %collective-permute-done.1.after_ref = bf16[144,128]{1,0:T(8,128)(2,1)S(1)} collective-permute-done((bf16[144,128]{1,0:T(8,128)(2,1)S(1)}, bf16[144,128]{1,0:T(8,128)(2,1)S(1)}, u32[]{:S(2)}, u32[]{:S(2)}) %collective-permute-start.1) | collective-permute-done | bytes 36896 | tf_op jit(solution)/shard_map/ppermute | solution.py:201
  24.7 0.0 collective-permute-done.before_ref
  24.7 0.6 copy-done.11
  25.3 0.0 copy-done.12
  25.3 6.4 %attend.1 = (bf16[256,256]{1,0:T(8,128)(2,1)}, bf16[256,256]{1,0:T(8,128)(2,1)}) custom-call(s32[1]{0:T(128)} %bitcast.core_ref, f32[4]{0:T(128)} %multiply_exponential_fusion.slope_ref, f32[4]{0:T(128)} %sink_ref.1, bf16[512,256]{1,0:T(8,128)(2,1)} %q_ref.1, bf16[64,512]{1,0:T(8,128)(2,1)} %bitcast.29, bf16[64,512]{1,0:T(8,128)(2,1)} %bitcast.31, ...), custom_call_target="tpu_custom_call" | custom-call | flops 2147483648 | bytes 1048576 | tf_op jit(solution)/shard_map/attend/pallas_call | solution.py:170
  31.7 2.0 %collective-permute-start.2 = (bf16[256,256]{1,0:T(8,128)(2,1)}, bf16[256,256]{1,0:T(8,128)(2,1)S(1)}, u32[]{:S(2)}, u32[]{:S(2)}) collective-permute-start(bf16[256,256]{1,0:T(8,128)(2,1)} %get-tuple-element.11), channel_id=1, source_target_pairs={{0,1},{1,0},{2,3},{3,2},{4,5},{5,4},{6,7},{7,6},{8,9},{9,8},{10,11... | collective-permute-start | bytes 393224 | tf_op jit(solution)/shard_map/ppermute | solution.py:37
  33.7 1.5 collective-permute-done.2
  35.3 0.0 collective-permute-done.3
  35.3 1.8 fusion.5
  37.0 0.0 all-to-all-done.2
  37.0 7.9 %collective-permute-start.8 = (bf16[256,2048]{1,0:T(8,128)(2,1)S(1)}, bf16[256,2048]{1,0:T(8,128)(2,1)S(1)}, u32[]{:S(2)}, u32[]{:S(2)}) collective-permute-start(bf16[256,2048]{1,0:T(8,128)(2,1)S(1)} %bitcast.20), channel_id=1, source_target_pairs={{0,8},{1,65},{8,16},{9,73},{16,24},{17,81},{24,32},{25,89},{32,40}... | collective-permute-start | bytes 3145736 | tf_op jit(solution)/shard_map/ppermute | solution.py:23
  45.0 5.6 %collective-permute-start.5 = (bf16[256,2048]{1,0:T(8,128)(2,1)S(1)}, bf16[256,2048]{1,0:T(8,128)(2,1)}, u32[]{:S(2)}, u32[]{:S(2)}) collective-permute-start(bf16[256,2048]{1,0:T(8,128)(2,1)S(1)} %bitcast.21), channel_id=1, source_target_pairs={{0,56},{1,449},{8,0},{9,457},{16,8},{17,465},{24,16},{25,473},{32,... | collective-permute-start | bytes 3145736 | tf_op jit(solution)/shard_map/ppermute | solution.py:23
  50.6 3.4 %fusion = bf16[256,2048]{1,0:T(8,128)(2,1)} fusion(f32[256,2048]{1,0:T(8,128)} %fusion.5, bf16[256,256]{1,0:T(8,128)(2,1)S(1)} %copy-done.4, bf16[256,2048]{1,0:T(8,128)(2,1)} %param.20), kind=kOutput, calls=%fused_computation.1 | convolution fusion | flops 269484032 | bytes 4325376 | tf_op jit(solution)/shard_map/dot_general | solution.py:223
  53.9 4.1 %all-to-all-start = ((bf16[4,64,2048]{2,1,0:T(8,128)(2,1)}), bf16[4,64,2048]{2,1,0:T(8,128)(2,1)S(1)}, u32[]{:S(2)}, u32[]{:S(2)}) async-start(bf16[4,64,2048]{2,1,0:T(8,128)(2,1)} %bitcast.27), calls=%async_computation | async-start | bytes 2097152 | tf_op jit(solution)/shard_map/all_to_all | solution.py:226
  58.1 11.7 %all-to-all-done = bf16[4,64,2048]{2,1,0:T(8,128)(2,1)S(1)} async-done(((bf16[4,64,2048]{2,1,0:T(8,128)(2,1)}), bf16[4,64,2048]{2,1,0:T(8,128)(2,1)S(1)}, u32[]{:S(2)}, u32[]{:S(2)}) %all-to-all-start) | async-done | bytes 1048608 | tf_op jit(solution)/shard_map/all_to_all | solution.py:226
  69.8 0.2 convert_reduce_fusion.1
  69.9 0.0 collective-permute-done.8.refs_8_
  70.0 1.9 %collective-permute-start.9 = (bf16[256,2048]{1,0:T(8,128)(2,1)S(1)}, bf16[256,2048]{1,0:T(8,128)(2,1)}, u32[]{:S(2)}, u32[]{:S(2)}) collective-permute-start(bf16[256,2048]{1,0:T(8,128)(2,1)S(1)} %collective-permute-done.8.refs_8_), channel_id=1, source_target_pairs={{0,8},{1,65},{8,16},{9,73},{16,24},{17,81},{24,32},{25,89},{32,40}... | collective-permute-start | bytes 3145736 | tf_op jit(solution)/shard_map/ppermute | solution.py:23
  71.9 0.0 collective-permute-done.5.refs_1_
  71.9 4.6 %collective-permute-start.6 = (bf16[256,2048]{1,0:T(8,128)(2,1)}, bf16[256,2048]{1,0:T(8,128)(2,1)}, u32[]{:S(2)}, u32[]{:S(2)}) collective-permute-start(bf16[256,2048]{1,0:T(8,128)(2,1)} %collective-permute-done.5.refs_1_), channel_id=1, source_target_pairs={{0,56},{1,449},{8,0},{9,457},{16,8},{17,465},{24,16},{25,473},{32,... | collective-permute-start | bytes 3145736 | tf_op jit(solution)/shard_map/ppermute | solution.py:23
  76.5 1.1 fusion.1
  77.6 0.1 fusion.3
  77.8 1.1 broadcast_in_dim.30
  78.9 3.5 %all-to-all-start.1 = ((bf16[4,64,2048]{2,1,0:T(8,128)(2,1)}), bf16[4,64,2048]{2,1,0:T(8,128)(2,1)S(1)}, u32[]{:S(2)}, u32[]{:S(2)}) async-start(bf16[4,64,2048]{2,1,0:T(8,128)(2,1)} %broadcast_in_dim.30), calls=%async_computation.1 | async-start | bytes 2097152 | tf_op jit(solution)/shard_map/all_to_all | solution.py:42
  82.4 4.6 %collective-permute-done.9.refs_7_ = bf16[256,2048]{1,0:T(8,128)(2,1)} collective-permute-done((bf16[256,2048]{1,0:T(8,128)(2,1)S(1)}, bf16[256,2048]{1,0:T(8,128)(2,1)}, u32[]{:S(2)}, u32[]{:S(2)}) %collective-permute-start.9) | collective-permute-done | bytes 1048608 | tf_op jit(solution)/shard_map/ppermute | solution.py:23
  87.0 1.9 %collective-permute-start.10 = (bf16[256,2048]{1,0:T(8,128)(2,1)}, bf16[256,2048]{1,0:T(8,128)(2,1)S(1)}, u32[]{:S(2)}, u32[]{:S(2)}) collective-permute-start(bf16[256,2048]{1,0:T(8,128)(2,1)} %collective-permute-done.9.refs_7_), channel_id=1, source_target_pairs={{0,8},{1,65},{8,16},{9,73},{16,24},{17,81},{24,32},{25,89},{32,40}... | collective-permute-start | bytes 3145736 | tf_op jit(solution)/shard_map/ppermute | solution.py:23
  88.9 0.0 collective-permute-done.6.refs_2_
  88.9 4.9 %collective-permute-start.7 = (bf16[256,2048]{1,0:T(8,128)(2,1)}, bf16[256,2048]{1,0:T(8,128)(2,1)}, u32[]{:S(2)}, u32[]{:S(2)}) collective-permute-start(bf16[256,2048]{1,0:T(8,128)(2,1)} %collective-permute-done.6.refs_2_), channel_id=1, source_target_pairs={{0,56},{1,449},{8,0},{9,457},{16,8},{17,465},{24,16},{25,473},{32,... | collective-permute-start | bytes 3145736 | tf_op jit(solution)/shard_map/ppermute | solution.py:23
  93.8 2.5 %all-to-all-done.1 = bf16[4,64,2048]{2,1,0:T(8,128)(2,1)S(1)} async-done(((bf16[4,64,2048]{2,1,0:T(8,128)(2,1)}), bf16[4,64,2048]{2,1,0:T(8,128)(2,1)S(1)}, u32[]{:S(2)}, u32[]{:S(2)}) %all-to-all-start.1) | async-done | bytes 1048608 | tf_op jit(solution)/shard_map/all_to_all | solution.py:42
  96.3 1.9 %collective-permute-start.4 = (bf16[256,2048]{1,0:T(8,128)(2,1)S(1)}, bf16[256,2048]{1,0:T(8,128)(2,1)}, u32[]{:S(2)}, u32[]{:S(2)}) collective-permute-start(bf16[256,2048]{1,0:T(8,128)(2,1)S(1)} %bitcast.23), channel_id=1, source_target_pairs={{0,1},{1,0},{2,3},{3,2},{4,5},{5,4},{6,7},{7,6},{8,9},{9,8},{10,11... | collective-permute-start | bytes 3145736 | tf_op jit(solution)/shard_map/ppermute | solution.py:37
  98.3 5.7 %collective-permute-done.10.refs_6_ = bf16[256,2048]{1,0:T(8,128)(2,1)S(1)} collective-permute-done((bf16[256,2048]{1,0:T(8,128)(2,1)}, bf16[256,2048]{1,0:T(8,128)(2,1)S(1)}, u32[]{:S(2)}, u32[]{:S(2)}) %collective-permute-start.10) | collective-permute-done | bytes 1048608 | tf_op jit(solution)/shard_map/ppermute | solution.py:23
  104.0 0.8 slice.16
  104.8 1.9 %collective-permute-start.11 = (bf16[128,2048]{1,0:T(8,128)(2,1)}, bf16[128,2048]{1,0:T(8,128)(2,1)}, u32[]{:S(2)}, u32[]{:S(2)}) collective-permute-start(bf16[128,2048]{1,0:T(8,128)(2,1)} %slice.16), channel_id=1, source_target_pairs={{0,8},{1,65},{8,16},{9,73},{16,24},{17,81},{24,32},{25,89},{32,40}... | collective-permute-start | bytes 1572872 | tf_op jit(solution)/shard_map/ppermute | solution.py:23
  106.7 0.0 collective-permute-done.7.refs_3_
  106.7 1.9 %slice.17 = bf16[128,2048]{1,0:T(8,128)(2,1)} slice(bf16[256,2048]{1,0:T(8,128)(2,1)} %collective-permute-done.7.refs_3_), slice={[128:256], [0:2048]} | slice | bytes 1048576 | tf_op jit(solution)/shard_map/slice | solution.py:219
  108.6 4.6 %collective-permute-start.12 = (bf16[128,2048]{1,0:T(8,128)(2,1)}, bf16[128,2048]{1,0:T(8,128)(2,1)}, u32[]{:S(2)}, u32[]{:S(2)}) collective-permute-start(bf16[128,2048]{1,0:T(8,128)(2,1)} %slice.17), channel_id=1, source_target_pairs={{0,56},{1,449},{8,0},{9,457},{16,8},{17,465},{24,16},{25,473},{32,... | collective-permute-start | bytes 1572872 | tf_op jit(solution)/shard_map/ppermute | solution.py:23
  113.2 0.1 pad_add_fusion.at_ref
  113.3 3.2 %collective-permute-done.11.refs_4_ = bf16[128,2048]{1,0:T(8,128)(2,1)} collective-permute-done((bf16[128,2048]{1,0:T(8,128)(2,1)}, bf16[128,2048]{1,0:T(8,128)(2,1)}, u32[]{:S(2)}, u32[]{:S(2)}) %collective-permute-start.11) | collective-permute-done | bytes 524320 | tf_op jit(solution)/shard_map/ppermute | solution.py:23
  116.5 3.1 %collective-permute-done.12.refs_5_ = bf16[128,2048]{1,0:T(8,128)(2,1)} collective-permute-done((bf16[128,2048]{1,0:T(8,128)(2,1)}, bf16[128,2048]{1,0:T(8,128)(2,1)}, u32[]{:S(2)}, u32[]{:S(2)}) %collective-permute-start.12) | collective-permute-done | bytes 524320 | tf_op jit(solution)/shard_map/ppermute | solution.py:23
  119.6 1.2 copy-done.1
  120.8 7.5 %mixer.1 = (bf16[2048,1024]{1,0:T(8,128)(2,1)}, bf16[256,1024]{1,0:T(8,128)(2,1)S(1)}, bf16[256,2048]{1,0:T(8,128)(2,1)S(1)}) custom-call(s32[3]{0:T(128)S(1)} %pad_add_fusion.at_ref, bf16[256,2048]{1,0:T(8,128)(2,1)} %collective-permute-done.4.theirs_ref, bf16[256,2048]{1,0:T(8,128)(2,1)S(1)} %bitcast.24, bf16[256,2048]{1,0:T(8,128)(2,1)S(1)} %bitcast.22, ...), custom_call_target="tpu_custom_call" | custom-call | flops 2147483648 | bytes 8388608 | tf_op jit(solution)/shard_map/mixer/pallas_call | solution.py:92
  128.3 2.7 %collective-permute-start.13 = (bf16[256,2048]{1,0:T(8,128)(2,1)S(1)}, bf16[256,2048]{1,0:T(8,128)(2,1)S(1)}, u32[]{:S(2)}, u32[]{:S(2)}) collective-permute-start(bf16[256,2048]{1,0:T(8,128)(2,1)S(1)} %get-tuple-element.14), channel_id=1, source_target_pairs={{0,1},{1,0},{2,3},{3,2},{4,5},{5,4},{6,7},{7,6},{8,9},{9,8},{10,11... | collective-permute-start | bytes 3145736 | tf_op jit(solution)/shard_map/ppermute | solution.py:37
  131.1 3.5 %fusion.6 = f32[256,2048]{1,0:T(8,128)S(1)} fusion(bf16[256,1024]{1,0:T(8,128)(2,1)S(1)} %get-tuple-element.12, bf16[2048,1024]{1,0:T(8,128)(2,1)} %get-tuple-element.13), kind=kOutput, calls=%fused_computation.24 | convolution fusion | flops 1073741824 | bytes 6815744 | tf_op jit(solution)/shard_map/dot_general | solution.py:244
  134.6 0.0 collective-permute-done.13
  134.6 0.3 add_convert_fusion
  134.9 17.3 %all_to_all.25 = bf16[4,64,2048]{2,1,0:T(8,128)(2,1)S(1)} all-to-all(bf16[4,64,2048]{2,1,0:T(8,128)(2,1)S(1)} %bitcast.28), channel_id=1, replica_groups=mesh['z'=8,'y'=8,'x'=4,'c'=2] {'x'}, dimensions={0} | all-to-all | bytes 2097152 | tf_op jit(solution)/shard_map/all_to_all | solution.py:48
  152.2 0.2 convert_reduce_fusion
  152.4 0.1 broadcast_in_dim.32
  152.5 16.5 %all_to_all.26 = bf16[4,64,2048]{2,1,0:T(8,128)(2,1)S(1)} all-to-all(bf16[4,64,2048]{2,1,0:T(8,128)(2,1)S(1)} %broadcast_in_dim.32), channel_id=1, replica_groups=mesh['z'=8,'y'=8,'x'=4,'c'=2] {'x'}, dimensions={0} | all-to-all | bytes 2097152 | tf_op jit(solution)/shard_map/all_to_all | solution.py:42
  169.0 3.9 %collective-permute-start.14 = (bf16[256,2048]{1,0:T(8,128)(2,1)S(1)}, bf16[256,2048]{1,0:T(8,128)(2,1)S(1)}, u32[]{:S(2)}, u32[]{:S(2)}) collective-permute-start(bf16[256,2048]{1,0:T(8,128)(2,1)S(1)} %bitcast.25), channel_id=1, source_target_pairs={{0,1},{1,0},{2,3},{3,2},{4,5},{5,4},{6,7},{7,6},{8,9},{9,8},{10,11... | collective-permute-start | bytes 3145736 | tf_op jit(solution)/shard_map/ppermute | solution.py:37
  172.9 0.2 broadcast_in_dim.26
  173.2 0.1 constant_dynamic-update-slice_fusion.1
  173.3 0.0 copy-start.2
  173.3 1.9 %collective-permute-done.14 = bf16[256,2048]{1,0:T(8,128)(2,1)S(1)} collective-permute-done((bf16[256,2048]{1,0:T(8,128)(2,1)S(1)}, bf16[256,2048]{1,0:T(8,128)(2,1)S(1)}, u32[]{:S(2)}, u32[]{:S(2)}) %collective-permute-start.14) | collective-permute-done | bytes 1048608 | tf_op jit(solution)/shard_map/ppermute | solution.py:37
  175.2 1.0 constant_dynamic-update-slice_fusion
  (27 shorter events, 0.1 us)
Async XLA Ops:
  0.0 9.8 %copy-start.3 = (bf16[256,2048]{1,0:T(8,128)(2,1)S(1)}, bf16[256,2048]{1,0:T(8,128)(2,1)}, u32[]{:S(2)}) copy-start(bf16[256,2048]{1,0:T(8,128)(2,1)} %param.20) | copy-start | bytes 3145732
  0.0 15.8 %copy-start.9 = (s32[512]{0:T(512)S(1)}, s32[512]{0:T(512)}, u32[]{:S(2)}) copy-start(s32[512]{0:T(512)} %param.16) | copy-start | bytes 6148
  0.0 15.9 %copy-start.6 = (bf16[512,64]{0,1:T(8,128)(2,1)S(1)}, bf16[512,64]{0,1:T(8,128)(2,1)}, u32[]{:S(2)}) copy-start(bf16[512,64]{0,1:T(8,128)(2,1)} %param.15) | copy-start | bytes 196612
  0.0 15.9 %copy-start.5 = (bf16[512,64]{0,1:T(8,128)(2,1)S(1)}, bf16[512,64]{0,1:T(8,128)(2,1)}, u32[]{:S(2)}) copy-start(bf16[512,64]{0,1:T(8,128)(2,1)} %param.14) | copy-start | bytes 196612
  0.0 21.7 %copy-start.10 = (f32[64]{0:T(128)S(1)}, f32[64]{0:T(128)}, u32[]{:S(2)}) copy-start(f32[64]{0:T(128)} %param.18) | copy-start | bytes 772
  2.1 34.9 %all-to-all-start.2 = ((bf16[8,32,2048]{2,1,0:T(8,128)(2,1)}), bf16[8,32,2048]{2,1,0:T(8,128)(2,1)S(1)}, u32[]{:S(2)}, u32[]{:S(2)}) async-start(bf16[8,32,2048]{2,1,0:T(8,128)(2,1)} %broadcast_in_dim.31), calls=%async_computation.2 | async-start | bytes 2097152 | tf_op jit(solution)/shard_map/all_to_all | solution.py:30
  9.8 25.5 %collective-permute-start.3 = (bf16[256,2048]{1,0:T(8,128)(2,1)S(1)}, bf16[256,2048]{1,0:T(8,128)(2,1)S(1)}, u32[]{:S(2)}, u32[]{:S(2)}) collective-permute-start(bf16[256,2048]{1,0:T(8,128)(2,1)S(1)} %copy-done.3), channel_id=1, source_target_pairs={{0,1},{1,0},{2,3},{3,2},{4,5},{5,4},{6,7},{7,6},{8,9},{9,8},{10,11... | collective-permute-start | bytes 3145736 | tf_op jit(solution)/shard_map/ppermute | solution.py:37
  15.9 8.8 %copy-start.7 = (bf16[16,512]{1,0:T(8,128)(2,1)}, bf16[16,512]{1,0:T(8,128)(2,1)S(1)}, u32[]{:S(2)}) copy-start(bf16[16,512]{1,0:T(8,128)(2,1)S(1)} %broadcast_in_dim.27.doc_ref) | copy-start | bytes 49156
  15.9 8.8 %collective-permute-start.1 = (bf16[144,128]{1,0:T(8,128)(2,1)S(1)}, bf16[144,128]{1,0:T(8,128)(2,1)S(1)}, u32[]{:S(2)}, u32[]{:S(2)}) collective-permute-start(bf16[144,128]{1,0:T(8,128)(2,1)S(1)} %get-tuple-element.17), channel_id=1, source_target_pairs={{8,0},{16,8},{24,16},{32,24},{40,32},{48,40},{56,48},{64,56},{72,6... | collective-permute-start | bytes 110600 | tf_op jit(solution)/shard_map/ppermute | solution.py:201
  17.2 7.5 %collective-permute-start = (bf16[144,128]{1,0:T(8,128)(2,1)S(1)}, bf16[144,128]{1,0:T(8,128)(2,1)S(1)}, u32[]{:S(2)}, u32[]{:S(2)}) collective-permute-start(bf16[144,128]{1,0:T(8,128)(2,1)S(1)} %get-tuple-element.18), channel_id=1, source_target_pairs={{0,8},{8,16},{16,24},{24,32},{32,40},{40,48},{48,56},{56,64},{64,7... | collective-permute-start | bytes 110600 | tf_op jit(solution)/shard_map/ppermute | solution.py:200
  24.7 0.6 copy-start.11
  24.7 0.6 copy-start.12
  31.7 18.9 %copy-start.4 = (bf16[256,256]{1,0:T(8,128)(2,1)S(1)}, bf16[256,256]{1,0:T(8,128)(2,1)}, u32[]{:S(2)}) copy-start(bf16[256,256]{1,0:T(8,128)(2,1)} %get-tuple-element.10) | copy-start | bytes 393220
  31.7 3.6 %collective-permute-start.2 = (bf16[256,256]{1,0:T(8,128)(2,1)}, bf16[256,256]{1,0:T(8,128)(2,1)S(1)}, u32[]{:S(2)}, u32[]{:S(2)}) collective-permute-start(bf16[256,256]{1,0:T(8,128)(2,1)} %get-tuple-element.11), channel_id=1, source_target_pairs={{0,1},{1,0},{2,3},{3,2},{4,5},{5,4},{6,7},{7,6},{8,9},{9,8},{10,11... | collective-permute-start | bytes 393224 | tf_op jit(solution)/shard_map/ppermute | solution.py:37
  37.0 32.9 %collective-permute-start.8 = (bf16[256,2048]{1,0:T(8,128)(2,1)S(1)}, bf16[256,2048]{1,0:T(8,128)(2,1)S(1)}, u32[]{:S(2)}, u32[]{:S(2)}) collective-permute-start(bf16[256,2048]{1,0:T(8,128)(2,1)S(1)} %bitcast.20), channel_id=1, source_target_pairs={{0,8},{1,65},{8,16},{9,73},{16,24},{17,81},{24,32},{25,89},{32,40}... | collective-permute-start | bytes 3145736 | tf_op jit(solution)/shard_map/ppermute | solution.py:23
  45.0 26.9 %collective-permute-start.5 = (bf16[256,2048]{1,0:T(8,128)(2,1)S(1)}, bf16[256,2048]{1,0:T(8,128)(2,1)}, u32[]{:S(2)}, u32[]{:S(2)}) collective-permute-start(bf16[256,2048]{1,0:T(8,128)(2,1)S(1)} %bitcast.21), channel_id=1, source_target_pairs={{0,56},{1,449},{8,0},{9,457},{16,8},{17,465},{24,16},{25,473},{32,... | collective-permute-start | bytes 3145736 | tf_op jit(solution)/shard_map/ppermute | solution.py:23
  53.9 23.7 %copy-start.8 = (f32[2048]{0:T(1024)S(1)}, f32[2048]{0:T(1024)}, u32[]{:S(2)}) copy-start(f32[2048]{0:T(1024)} %param.21) | copy-start | bytes 24580
  53.9 15.8 %all-to-all-start = ((bf16[4,64,2048]{2,1,0:T(8,128)(2,1)}), bf16[4,64,2048]{2,1,0:T(8,128)(2,1)S(1)}, u32[]{:S(2)}, u32[]{:S(2)}) async-start(bf16[4,64,2048]{2,1,0:T(8,128)(2,1)} %bitcast.27), calls=%async_computation | async-start | bytes 2097152 | tf_op jit(solution)/shard_map/all_to_all | solution.py:226
  70.0 8.9 %copy-start = (bf16[256,2048]{1,0:T(8,128)(2,1)}, bf16[256,2048]{1,0:T(8,128)(2,1)S(1)}, u32[]{:S(2)}) copy-start(bf16[256,2048]{1,0:T(8,128)(2,1)S(1)} %collective-permute-done.8.refs_8_) | copy-start | bytes 3145732
  70.0 17.0 %collective-permute-start.9 = (bf16[256,2048]{1,0:T(8,128)(2,1)S(1)}, bf16[256,2048]{1,0:T(8,128)(2,1)}, u32[]{:S(2)}, u32[]{:S(2)}) collective-permute-start(bf16[256,2048]{1,0:T(8,128)(2,1)S(1)} %collective-permute-done.8.refs_8_), channel_id=1, source_target_pairs={{0,8},{1,65},{8,16},{9,73},{16,24},{17,81},{24,32},{25,89},{32,40}... | collective-permute-start | bytes 3145736 | tf_op jit(solution)/shard_map/ppermute | solution.py:23
  71.9 17.0 %collective-permute-start.6 = (bf16[256,2048]{1,0:T(8,128)(2,1)}, bf16[256,2048]{1,0:T(8,128)(2,1)}, u32[]{:S(2)}, u32[]{:S(2)}) collective-permute-start(bf16[256,2048]{1,0:T(8,128)(2,1)} %collective-permute-done.5.refs_1_), channel_id=1, source_target_pairs={{0,56},{1,449},{8,0},{9,457},{16,8},{17,465},{24,16},{25,473},{32,... | collective-permute-start | bytes 3145736 | tf_op jit(solution)/shard_map/ppermute | solution.py:23
  78.9 17.5 %all-to-all-start.1 = ((bf16[4,64,2048]{2,1,0:T(8,128)(2,1)}), bf16[4,64,2048]{2,1,0:T(8,128)(2,1)S(1)}, u32[]{:S(2)}, u32[]{:S(2)}) async-start(bf16[4,64,2048]{2,1,0:T(8,128)(2,1)} %broadcast_in_dim.30), calls=%async_computation.1 | async-start | bytes 2097152 | tf_op jit(solution)/shard_map/all_to_all | solution.py:42
  87.0 17.0 %collective-permute-start.10 = (bf16[256,2048]{1,0:T(8,128)(2,1)}, bf16[256,2048]{1,0:T(8,128)(2,1)S(1)}, u32[]{:S(2)}, u32[]{:S(2)}) collective-permute-start(bf16[256,2048]{1,0:T(8,128)(2,1)} %collective-permute-done.9.refs_7_), channel_id=1, source_target_pairs={{0,8},{1,65},{8,16},{9,73},{16,24},{17,81},{24,32},{25,89},{32,40}... | collective-permute-start | bytes 3145736 | tf_op jit(solution)/shard_map/ppermute | solution.py:23
  88.9 17.8 %collective-permute-start.7 = (bf16[256,2048]{1,0:T(8,128)(2,1)}, bf16[256,2048]{1,0:T(8,128)(2,1)}, u32[]{:S(2)}, u32[]{:S(2)}) collective-permute-start(bf16[256,2048]{1,0:T(8,128)(2,1)} %collective-permute-done.6.refs_2_), channel_id=1, source_target_pairs={{0,56},{1,449},{8,0},{9,457},{16,8},{17,465},{24,16},{25,473},{32,... | collective-permute-start | bytes 3145736 | tf_op jit(solution)/shard_map/ppermute | solution.py:23
  96.3 16.9 %collective-permute-start.4 = (bf16[256,2048]{1,0:T(8,128)(2,1)S(1)}, bf16[256,2048]{1,0:T(8,128)(2,1)}, u32[]{:S(2)}, u32[]{:S(2)}) collective-permute-start(bf16[256,2048]{1,0:T(8,128)(2,1)S(1)} %bitcast.23), channel_id=1, source_target_pairs={{0,1},{1,0},{2,3},{3,2},{4,5},{5,4},{6,7},{7,6},{8,9},{9,8},{10,11... | collective-permute-start | bytes 3145736 | tf_op jit(solution)/shard_map/ppermute | solution.py:37
  104.8 11.7 %collective-permute-start.11 = (bf16[128,2048]{1,0:T(8,128)(2,1)}, bf16[128,2048]{1,0:T(8,128)(2,1)}, u32[]{:S(2)}, u32[]{:S(2)}) collective-permute-start(bf16[128,2048]{1,0:T(8,128)(2,1)} %slice.16), channel_id=1, source_target_pairs={{0,8},{1,65},{8,16},{9,73},{16,24},{17,81},{24,32},{25,89},{32,40}... | collective-permute-start | bytes 1572872 | tf_op jit(solution)/shard_map/ppermute | solution.py:23
  108.6 11.0 %collective-permute-start.12 = (bf16[128,2048]{1,0:T(8,128)(2,1)}, bf16[128,2048]{1,0:T(8,128)(2,1)}, u32[]{:S(2)}, u32[]{:S(2)}) collective-permute-start(bf16[128,2048]{1,0:T(8,128)(2,1)} %slice.17), channel_id=1, source_target_pairs={{0,56},{1,449},{8,0},{9,457},{16,8},{17,465},{24,16},{25,473},{32,... | collective-permute-start | bytes 1572872 | tf_op jit(solution)/shard_map/ppermute | solution.py:23
  119.6 1.2 copy-start.1
  128.3 6.2 %collective-permute-start.13 = (bf16[256,2048]{1,0:T(8,128)(2,1)S(1)}, bf16[256,2048]{1,0:T(8,128)(2,1)S(1)}, u32[]{:S(2)}, u32[]{:S(2)}) collective-permute-start(bf16[256,2048]{1,0:T(8,128)(2,1)S(1)} %get-tuple-element.14), channel_id=1, source_target_pairs={{0,1},{1,0},{2,3},{3,2},{4,5},{5,4},{6,7},{7,6},{8,9},{9,8},{10,11... | collective-permute-start | bytes 3145736 | tf_op jit(solution)/shard_map/ppermute | solution.py:37
  169.0 6.2 %collective-permute-start.14 = (bf16[256,2048]{1,0:T(8,128)(2,1)S(1)}, bf16[256,2048]{1,0:T(8,128)(2,1)S(1)}, u32[]{:S(2)}, u32[]{:S(2)}) collective-permute-start(bf16[256,2048]{1,0:T(8,128)(2,1)S(1)} %bitcast.25), channel_id=1, source_target_pairs={{0,1},{1,0},{2,3},{3,2},{4,5},{5,4},{6,7},{7,6},{8,9},{9,8},{10,11... | collective-permute-start | bytes 3145736 | tf_op jit(solution)/shard_map/ppermute | solution.py:37
  173.3 1.9 %copy-start.2 = (bf16[512,2048]{1,0:T(8,128)(2,1)}, bf16[512,2048]{1,0:T(8,128)(2,1)S(1)}, u32[]{:S(2)}) copy-start(bf16[512,2048]{1,0:T(8,128)(2,1)S(1)} %constant_dynamic-update-slice_fusion.1) | copy-start | bytes 6291460

commit v4 on v3

--- a/solution.py
+++ b/solution.py
@@ -41,6 +41,25 @@
     n = lax.axis_size(axis)
     tiles = lax.all_to_all(jnp.broadcast_to(x, (n, *x.shape)), axis, 0, 0, tiled=True)
     return tiles.reshape(n * x.shape[0], x.shape[1])
+
+
+def copies_body(up_ref, down_ref, out_ref):
+    units = up_ref.shape[1]
+    for i in range(out_ref.shape[0]):
+        out_ref[i, :, :units] = up_ref[...]
+        out_ref[i, :, units:] = down_ref[...]
+
+
+def copies_of(up, down_t, count):
+    rows, units = up.shape
+    vmem = pl.BlockSpec(memory_space=pltpu.VMEM)
+    return pl.pallas_call(
+        copies_body,
+        in_specs=[vmem, vmem],
+        out_specs=vmem,
+        out_shape=jax.ShapeDtypeStruct((count, rows, 2 * units), up.dtype),
+        name="copies",
+    )(up, down_t)
 
 
 def scatter_x(x):
@@ -199,8 +218,7 @@
     onward = [(i, i + 1) for i in range(count - 1)]
     before = lax.ppermute(packed[:, rows - WINDOW :], SP, onward)
     after = lax.ppermute(packed[:, :WINDOW], SP, [(j, i) for i, j in onward])
-    both = jnp.concatenate([w_up, w_down.T], axis=1)
-    piece = across(jnp.broadcast_to(both, (lax.axis_size("z"), *both.shape)))
+    piece = across(copies_of(w_up, w_down.T, lax.axis_size("z")))
     w_out_other = swap(w_out)
 
     heads_all = heads_here * lax.axis_size(TP)
@@ -216,7 +234,7 @@
     up1, dn1 = along(piece, 1), along(piece, -1)
     up2, dn2 = along(up1, 1), along(dn1, -1)
     up3, dn3 = along(up2, 1), along(dn2, -1)
-    up4, dn4 = along(up3[:cut], 1), along(dn3[cut:], -1)
+    up4, dn4 = along(up2[:cut], 2), along(dn2[cut:], -2)
     pieces = [piece, dn1, dn2, dn3, up4, dn4, up3, up2, up1]
 
     att_other = swap(att_send)

time: 179 us -> 181 us (1.011)
  blocking collectives: 33.8 us -> 50.5 us
  waiting for transfers between devices: 36.5 us -> 30.3 us
  local copies, waits for them, and re-layouts: 8.99 us -> 5.67 us
  matrix products: 8.59 us -> 5.39 us
  starting transfers between devices: 70.5 us -> 67.8 us
  Pallas kernels: 13.9 us -> 16.2 us
    all_to_all x1 -> x2, blocking collectives: 16.5 us -> 33.4 us  [spread(): lax.all_to_all(jnp.broadcast_to(x, (n, *x.shape)), axis, 0, 0, tiled=True)]
    all_to_all x1, waiting for transfers between devices: 11.7 us -> 1.22 us  [shards(): lax.all_to_all(partial.astype(jnp.bfloat16).reshape(nx, share, -1), 'x',...]
    ppermute x8, waiting for transfers between devices: 16.6 us -> 23.4 us  [along(): return lax.ppermute(x, ('z', 'y', 'c'), pairs)]
    all_to_all x1 -> x0, starting transfers between devices: 3.52 us -> none  [spread(): lax.all_to_all(jnp.broadcast_to(x, (n, *x.shape)), axis, 0, 0, tiled=True)]
    all_to_all x1 -> x0, waiting for transfers between devices: 2.5 us -> none  [spread(): lax.all_to_all(jnp.broadcast_to(x, (n, *x.shape)), axis, 0, 0, tiled=True)]
    pallas_call x0 -> x1, Pallas kernels: none -> 2.03 us  [copies_of(): pl.pallas_call(copies_body, in_specs=[vmem, vmem], out_specs=vmem, out_sh...]
    dot_general x1, matrix products: 3.36 us -> 1.43 us  [shards(): jnp.dot(att_own, w_out, preferred_element_type=jnp.float32)]
  transfers between devices with their start and end apart: 18 -> 17, of which waited for: 9 -> 7; matrix products, arithmetic and copies ran while one was open for 9% -> 6% of each run, Pallas kernels for 4% -> 4%
where the time goes in v4:
time: 181 us; the launch traced here: 179 us
  starting transfers between devices  67.8 us (37%)
  blocking collectives  50.5 us (28%)
  waiting for transfers between devices  30.3 us (17%)
  Pallas kernels  16.2 us (9%)
  local copies, waits for them, and re-layouts  5.67 us (3%)
  matrix products  5.39 us (3%)
  other arithmetic  2.54 us (1%)
    ppermute x8, starting transfers between devices, along(): return lax.ppermute(x, ('z', 'y', 'c'), pairs)  34.4 us
    all_to_all x2, blocking collectives, spread(): lax.all_to_all(jnp.broadcast_to(x, (n, *x.shape)), axis, 0, 0, tiled=True)  33.4 us
    ppermute x8, waiting for transfers between devices, along(): return lax.ppermute(x, ('z', 'y', 'c'), pairs)  23.4 us
    all_to_all x1, blocking collectives, scatter_x(): lax.all_to_all(x.reshape(n, x.shape[0] // n, x.shape[1]), 'x', 0, 0, tile...  17.1 us
    ppermute x5, starting transfers between devices, swap(): return lax.ppermute(x, 'c', [(0, 1), (1, 0)])  16.3 us
    pallas_call x1, Pallas kernels, mixer(): pl.pallas_call(mixer_body, in_specs=[smem] + [vmem] * (2 + len(pieces)),...  7.8 us
    all_to_all x1, starting transfers between devices, across(): lax.all_to_all(copies, ('z', 'y', 'c'), 0, 0, tiled=True, axis_index_grou...  7.64 us
    pallas_call x1, Pallas kernels, attention(): pl.pallas_call(attention_body, in_specs=[smem] * 3 + [vmem] * 8, out_spec...  6.37 us
  transfers between devices with their start and end apart: 17, of which 7 were waited for; matrix products, arithmetic and copies ran while one was open for 6% of the time, Pallas kernels for 4%

profile of v4, /device:TPU:1, one launch (start us, length us, event | category | flops | bytes accessed | tf_op | source)
XLA Modules:
  0.0 178.8 jit_solution(8951004618258010030)
XLA Ops:
  0.0 0.0 copy-start.3
  0.0 2.0 %copies.1 = bf16[8,32,2048]{2,1,0:T(8,128)(2,1)} custom-call(bf16[32,1024]{1,0:T(8,128)(2,1)} %up_ref.1, bf16[32,1024]{1,0:T(8,128)(2,1)} %bitcast.28), custom_call_target="tpu_custom_call" | custom-call | tf_op jit(solution)/shard_map/copies/pallas_call | solution.py:56
  2.1 7.6 %all-to-all-start.2 = ((bf16[8,32,2048]{2,1,0:T(8,128)(2,1)}), bf16[8,32,2048]{2,1,0:T(8,128)(2,1)S(1)}, u32[]{:S(2)}, u32[]{:S(2)}) async-start(bf16[8,32,2048]{2,1,0:T(8,128)(2,1)} %copies.1), calls=%async_computation.2 | async-start | bytes 2097152 | tf_op jit(solution)/shard_map/all_to_all | solution.py:30
  9.7 0.0 copy-done.1
  9.7 6.1 %collective-permute-start.3 = (bf16[256,2048]{1,0:T(8,128)(2,1)S(1)}, bf16[256,2048]{1,0:T(8,128)(2,1)S(1)}, u32[]{:S(2)}, u32[]{:S(2)}) collective-permute-start(bf16[256,2048]{1,0:T(8,128)(2,1)S(1)} %copy-done.1), channel_id=1, source_target_pairs={{0,1},{1,0},{2,3},{3,2},{4,5},{5,4},{6,7},{7,6},{8,9},{9,8},{10,11... | collective-permute-start | bytes 3145736 | tf_op jit(solution)/shard_map/ppermute | solution.py:37
  15.8 0.0 copy-done.7
  15.9 1.3 collective-permute-start.1
  17.2 4.0 %collective-permute-start = (bf16[144,128]{1,0:T(8,128)(2,1)S(1)}, bf16[144,128]{1,0:T(8,128)(2,1)S(1)}, u32[]{:S(2)}, u32[]{:S(2)}) collective-permute-start(bf16[144,128]{1,0:T(8,128)(2,1)S(1)} %get-tuple-element.18), channel_id=1, source_target_pairs={{0,8},{8,16},{16,24},{24,32},{32,40},{40,48},{48,56},{56,64},{64,7... | collective-permute-start | bytes 110600 | tf_op jit(solution)/shard_map/ppermute | solution.py:219
  21.2 0.5 multiply_exponential_fusion.slope_ref
  21.7 0.7 copy.13.kg_ref
  22.4 2.3 %collective-permute-done.1.after_ref = bf16[144,128]{1,0:T(8,128)(2,1)S(1)} collective-permute-done((bf16[144,128]{1,0:T(8,128)(2,1)S(1)}, bf16[144,128]{1,0:T(8,128)(2,1)S(1)}, u32[]{:S(2)}, u32[]{:S(2)}) %collective-permute-start.1) | collective-permute-done | bytes 36896 | tf_op jit(solution)/shard_map/ppermute | solution.py:220
  24.6 0.0 collective-permute-done.before_ref
  24.7 0.6 copy-done.9
  25.3 0.0 copy-done.10
  25.3 6.4 %attend.1 = (bf16[256,256]{1,0:T(8,128)(2,1)}, bf16[256,256]{1,0:T(8,128)(2,1)}) custom-call(s32[1]{0:T(128)} %bitcast.core_ref, f32[4]{0:T(128)} %multiply_exponential_fusion.slope_ref, f32[4]{0:T(128)} %sink_ref.1, bf16[512,256]{1,0:T(8,128)(2,1)} %q_ref.1, bf16[64,512]{1,0:T(8,128)(2,1)} %bitcast.29, bf16[64,512]{1,0:T(8,128)(2,1)} %bitcast.31, ...), custom_call_target="tpu_custom_call" | custom-call | flops 2147483648 | bytes 1048576 | tf_op jit(solution)/shard_map/attend/pallas_call | solution.py:189
  31.6 2.0 %collective-permute-start.2 = (bf16[256,256]{1,0:T(8,128)(2,1)}, bf16[256,256]{1,0:T(8,128)(2,1)S(1)}, u32[]{:S(2)}, u32[]{:S(2)}) collective-permute-start(bf16[256,256]{1,0:T(8,128)(2,1)} %get-tuple-element.11), channel_id=1, source_target_pairs={{0,1},{1,0},{2,3},{3,2},{4,5},{5,4},{6,7},{7,6},{8,9},{9,8},{10,11... | collective-permute-start | bytes 393224 | tf_op jit(solution)/shard_map/ppermute | solution.py:37
  33.7 1.5 collective-permute-done.2
  35.2 0.0 collective-permute-done.3
  35.2 0.4 fusion.5
  35.7 1.4 fusion
  37.1 0.0 all-to-all-done.2
  37.1 4.1 %all-to-all-start = ((bf16[4,64,2048]{2,1,0:T(8,128)(2,1)}), bf16[4,64,2048]{2,1,0:T(8,128)(2,1)S(1)}, u32[]{:S(2)}, u32[]{:S(2)}) async-start(bf16[4,64,2048]{2,1,0:T(8,128)(2,1)} %bitcast.5), calls=%async_computation | async-start | bytes 2097152 | tf_op jit(solution)/shard_map/all_to_all | solution.py:244
  41.2 7.9 %collective-permute-start.8 = (bf16[256,2048]{1,0:T(8,128)(2,1)S(1)}, bf16[256,2048]{1,0:T(8,128)(2,1)}, u32[]{:S(2)}, u32[]{:S(2)}) collective-permute-start(bf16[256,2048]{1,0:T(8,128)(2,1)S(1)} %bitcast.20), channel_id=1, source_target_pairs={{0,8},{1,65},{8,16},{9,73},{16,24},{17,81},{24,32},{25,89},{32,40}... | collective-permute-start | bytes 3145736 | tf_op jit(solution)/shard_map/ppermute | solution.py:23
  49.2 5.6 %collective-permute-start.5 = (bf16[256,2048]{1,0:T(8,128)(2,1)S(1)}, bf16[256,2048]{1,0:T(8,128)(2,1)}, u32[]{:S(2)}, u32[]{:S(2)}) collective-permute-start(bf16[256,2048]{1,0:T(8,128)(2,1)S(1)} %bitcast.21), channel_id=1, source_target_pairs={{0,56},{1,449},{8,0},{9,457},{16,8},{17,465},{24,16},{25,473},{32,... | collective-permute-start | bytes 3145736 | tf_op jit(solution)/shard_map/ppermute | solution.py:23
  54.8 1.2 all-to-all-done
  56.0 0.2 convert_reduce_fusion.1
  56.2 1.1 fusion.1
  57.3 7.8 %collective-permute-done.8.refs_8_ = bf16[256,2048]{1,0:T(8,128)(2,1)} collective-permute-done((bf16[256,2048]{1,0:T(8,128)(2,1)S(1)}, bf16[256,2048]{1,0:T(8,128)(2,1)}, u32[]{:S(2)}, u32[]{:S(2)}) %collective-permute-start.8) | collective-permute-done | bytes 1048608 | tf_op jit(solution)/shard_map/ppermute | solution.py:23
  65.1 1.9 %collective-permute-start.9 = (bf16[256,2048]{1,0:T(8,128)(2,1)}, bf16[256,2048]{1,0:T(8,128)(2,1)S(1)}, u32[]{:S(2)}, u32[]{:S(2)}) collective-permute-start(bf16[256,2048]{1,0:T(8,128)(2,1)} %collective-permute-done.8.refs_8_), channel_id=1, source_target_pairs={{0,8},{1,65},{8,16},{9,73},{16,24},{17,81},{24,32},{25,89},{32,40}... | collective-permute-start | bytes 3145736 | tf_op jit(solution)/shard_map/ppermute | solution.py:23
  67.0 0.0 collective-permute-done.5.refs_1_
  67.1 4.6 %collective-permute-start.6 = (bf16[256,2048]{1,0:T(8,128)(2,1)}, bf16[256,2048]{1,0:T(8,128)(2,1)}, u32[]{:S(2)}, u32[]{:S(2)}) collective-permute-start(bf16[256,2048]{1,0:T(8,128)(2,1)} %collective-permute-done.5.refs_1_), channel_id=1, source_target_pairs={{0,56},{1,449},{8,0},{9,457},{16,8},{17,465},{24,16},{25,473},{32,... | collective-permute-start | bytes 3145736 | tf_op jit(solution)/shard_map/ppermute | solution.py:23
  71.7 0.1 fusion.3
  71.8 0.1 broadcast_in_dim.27
  71.9 17.5 %all_to_all.25 = bf16[4,64,2048]{2,1,0:T(8,128)(2,1)S(1)} all-to-all(bf16[4,64,2048]{2,1,0:T(8,128)(2,1)S(1)} %broadcast_in_dim.27), channel_id=1, replica_groups=mesh['z'=8,'y'=8,'x'=4,'c'=2] {'x'}, dimensions={0} | all-to-all | bytes 2097152 | tf_op jit(solution)/shard_map/all_to_all | solution.py:42
  89.4 1.9 %collective-permute-start.4 = (bf16[256,2048]{1,0:T(8,128)(2,1)S(1)}, bf16[256,2048]{1,0:T(8,128)(2,1)}, u32[]{:S(2)}, u32[]{:S(2)}) collective-permute-start(bf16[256,2048]{1,0:T(8,128)(2,1)S(1)} %bitcast.23), channel_id=1, source_target_pairs={{0,1},{1,0},{2,3},{3,2},{4,5},{5,4},{6,7},{7,6},{8,9},{9,8},{10,11... | collective-permute-start | bytes 3145736 | tf_op jit(solution)/shard_map/ppermute | solution.py:37
  91.3 0.0 collective-permute-done.9.refs_7_
  91.3 3.3 %collective-permute-start.12 = (bf16[256,2048]{1,0:T(8,128)(2,1)S(1)}, bf16[256,2048]{1,0:T(8,128)(2,1)}, u32[]{:S(2)}, u32[]{:S(2)}) collective-permute-start(bf16[256,2048]{1,0:T(8,128)(2,1)S(1)} %collective-permute-done.9.refs_7_), channel_id=1, source_target_pairs={{0,8},{1,65},{8,16},{9,73},{16,24},{17,81},{24,32},{25,89},{32,40}... | collective-permute-start | bytes 3145736 | tf_op jit(solution)/shard_map/ppermute | solution.py:23
  94.6 0.0 collective-permute-done.6.refs_2_
  94.6 3.7 %collective-permute-start.7 = (bf16[256,2048]{1,0:T(8,128)(2,1)}, bf16[256,2048]{1,0:T(8,128)(2,1)}, u32[]{:S(2)}, u32[]{:S(2)}) collective-permute-start(bf16[256,2048]{1,0:T(8,128)(2,1)} %collective-permute-done.6.refs_2_), channel_id=1, source_target_pairs={{0,56},{1,449},{8,0},{9,457},{16,8},{17,465},{24,16},{25,473},{32,... | collective-permute-start | bytes 3145736 | tf_op jit(solution)/shard_map/ppermute | solution.py:23
  98.3 0.8 slice.16
  99.1 3.6 %collective-permute-start.10 = (bf16[128,2048]{1,0:T(8,128)(2,1)}, bf16[128,2048]{1,0:T(8,128)(2,1)}, u32[]{:S(2)}, u32[]{:S(2)}) collective-permute-start(bf16[128,2048]{1,0:T(8,128)(2,1)} %slice.16), channel_id=1, source_target_pairs={{0,16},{1,129},{8,24},{9,137},{16,32},{17,145},{24,40},{25,153},{3... | collective-permute-start | bytes 1572872 | tf_op jit(solution)/shard_map/ppermute | solution.py:23
  102.7 1.9 %slice.17 = bf16[128,2048]{1,0:T(8,128)(2,1)} slice(bf16[256,2048]{1,0:T(8,128)(2,1)} %collective-permute-done.6.refs_2_), slice={[128:256], [0:2048]} | slice | bytes 1048576 | tf_op jit(solution)/shard_map/slice | solution.py:237
  104.6 3.8 %collective-permute-start.11 = (bf16[128,2048]{1,0:T(8,128)(2,1)}, bf16[128,2048]{1,0:T(8,128)(2,1)}, u32[]{:S(2)}, u32[]{:S(2)}) collective-permute-start(bf16[128,2048]{1,0:T(8,128)(2,1)} %slice.17), channel_id=1, source_target_pairs={{0,48},{1,385},{8,56},{9,393},{16,0},{17,401},{24,8},{25,409},{32,... | collective-permute-start | bytes 1572872 | tf_op jit(solution)/shard_map/ppermute | solution.py:23
  108.4 0.1 pad_add_fusion.at_ref
  108.5 0.0 collective-permute-done.4.theirs_ref
  108.5 10.9 %collective-permute-done.10.refs_4_ = bf16[128,2048]{1,0:T(8,128)(2,1)} collective-permute-done((bf16[128,2048]{1,0:T(8,128)(2,1)}, bf16[128,2048]{1,0:T(8,128)(2,1)}, u32[]{:S(2)}, u32[]{:S(2)}) %collective-permute-start.10) | collective-permute-done | bytes 524320 | tf_op jit(solution)/shard_map/ppermute | solution.py:23
  119.4 4.7 %collective-permute-done.11.refs_5_ = bf16[128,2048]{1,0:T(8,128)(2,1)} collective-permute-done((bf16[128,2048]{1,0:T(8,128)(2,1)}, bf16[128,2048]{1,0:T(8,128)(2,1)}, u32[]{:S(2)}, u32[]{:S(2)}) %collective-permute-start.11) | collective-permute-done | bytes 524320 | tf_op jit(solution)/shard_map/ppermute | solution.py:23
  124.1 0.0 collective-permute-done.12.refs_6_
  124.1 0.0 collective-permute-done.7.refs_3_
  124.1 7.8 %mixer.1 = (bf16[2048,1024]{1,0:T(8,128)(2,1)}, bf16[256,1024]{1,0:T(8,128)(2,1)S(1)}, bf16[256,2048]{1,0:T(8,128)(2,1)S(1)}) custom-call(s32[3]{0:T(128)S(1)} %pad_add_fusion.at_ref, bf16[256,2048]{1,0:T(8,128)(2,1)} %collective-permute-done.4.theirs_ref, bf16[256,2048]{1,0:T(8,128)(2,1)S(1)} %bitcast.24, bf16[256,2048]{1,0:T(8,128)(2,1)S(1)} %bitcast.22, ...), custom_call_target="tpu_custom_call" | custom-call | flops 2147483648 | bytes 8388608 | tf_op jit(solution)/shard_map/mixer/pallas_call | solution.py:111
  131.9 1.9 %collective-permute-start.13 = (bf16[256,2048]{1,0:T(8,128)(2,1)S(1)}, bf16[256,2048]{1,0:T(8,128)(2,1)S(1)}, u32[]{:S(2)}, u32[]{:S(2)}) collective-permute-start(bf16[256,2048]{1,0:T(8,128)(2,1)S(1)} %get-tuple-element.14), channel_id=1, source_target_pairs={{0,1},{1,0},{2,3},{3,2},{4,5},{5,4},{6,7},{7,6},{8,9},{9,8},{10,11... | collective-permute-start | bytes 3145736 | tf_op jit(solution)/shard_map/ppermute | solution.py:37
  133.8 3.5 %fusion.6 = f32[256,2048]{1,0:T(8,128)S(1)} fusion(bf16[256,1024]{1,0:T(8,128)(2,1)S(1)} %get-tuple-element.12, bf16[2048,1024]{1,0:T(8,128)(2,1)} %get-tuple-element.13), kind=kOutput, calls=%fused_computation.23 | convolution fusion | flops 1073741824 | bytes 6815744 | tf_op jit(solution)/shard_map/dot_general | solution.py:262
  137.4 0.0 collective-permute-done.13
  137.4 0.3 add_convert_fusion
  137.7 17.1 %all_to_all.26 = bf16[4,64,2048]{2,1,0:T(8,128)(2,1)S(1)} all-to-all(bf16[4,64,2048]{2,1,0:T(8,128)(2,1)S(1)} %bitcast.27), channel_id=1, replica_groups=mesh['z'=8,'y'=8,'x'=4,'c'=2] {'x'}, dimensions={0} | all-to-all | bytes 2097152 | tf_op jit(solution)/shard_map/all_to_all | solution.py:67
  154.8 0.2 convert_reduce_fusion
  155.0 0.1 broadcast_in_dim.28
  155.2 16.0 %all_to_all.27 = bf16[4,64,2048]{2,1,0:T(8,128)(2,1)S(1)} all-to-all(bf16[4,64,2048]{2,1,0:T(8,128)(2,1)S(1)} %broadcast_in_dim.28), channel_id=1, replica_groups=mesh['z'=8,'y'=8,'x'=4,'c'=2] {'x'}, dimensions={0} | all-to-all | bytes 2097152 | tf_op jit(solution)/shard_map/all_to_all | solution.py:42
  171.1 4.4 %collective-permute-start.14 = (bf16[256,2048]{1,0:T(8,128)(2,1)S(1)}, bf16[256,2048]{1,0:T(8,128)(2,1)S(1)}, u32[]{:S(2)}, u32[]{:S(2)}) collective-permute-start(bf16[256,2048]{1,0:T(8,128)(2,1)S(1)} %bitcast.25), channel_id=1, source_target_pairs={{0,1},{1,0},{2,3},{3,2},{4,5},{5,4},{6,7},{7,6},{8,9},{9,8},{10,11... | collective-permute-start | bytes 3145736 | tf_op jit(solution)/shard_map/ppermute | solution.py:37
  175.5 0.2 broadcast_in_dim.23
  175.8 0.1 constant_dynamic-update-slice_fusion.1
  175.9 0.0 copy-start
  175.9 1.9 %collective-permute-done.14 = bf16[256,2048]{1,0:T(8,128)(2,1)S(1)} collective-permute-done((bf16[256,2048]{1,0:T(8,128)(2,1)S(1)}, bf16[256,2048]{1,0:T(8,128)(2,1)S(1)}, u32[]{:S(2)}, u32[]{:S(2)}) %collective-permute-start.14) | collective-permute-done | bytes 1048608 | tf_op jit(solution)/shard_map/ppermute | solution.py:37
  177.8 1.0 constant_dynamic-update-slice_fusion
  (21 shorter events, 0.1 us)
Async XLA Ops:
  0.0 9.7 %copy-start.1 = (bf16[256,2048]{1,0:T(8,128)(2,1)S(1)}, bf16[256,2048]{1,0:T(8,128)(2,1)}, u32[]{:S(2)}) copy-start(bf16[256,2048]{1,0:T(8,128)(2,1)} %param.20) | copy-start | bytes 3145732
  0.0 15.8 %copy-start.7 = (s32[512]{0:T(512)S(1)}, s32[512]{0:T(512)}, u32[]{:S(2)}) copy-start(s32[512]{0:T(512)} %param.16) | copy-start | bytes 6148
  0.0 15.8 %copy-start.4 = (bf16[512,64]{0,1:T(8,128)(2,1)S(1)}, bf16[512,64]{0,1:T(8,128)(2,1)}, u32[]{:S(2)}) copy-start(bf16[512,64]{0,1:T(8,128)(2,1)} %param.15) | copy-start | bytes 196612
  0.0 15.8 %copy-start.3 = (bf16[512,64]{0,1:T(8,128)(2,1)S(1)}, bf16[512,64]{0,1:T(8,128)(2,1)}, u32[]{:S(2)}) copy-start(bf16[512,64]{0,1:T(8,128)(2,1)} %param.14) | copy-start | bytes 196612
  0.0 21.7 %copy-start.8 = (f32[64]{0:T(128)S(1)}, f32[64]{0:T(128)}, u32[]{:S(2)}) copy-start(f32[64]{0:T(128)} %param.18) | copy-start | bytes 772
  2.1 35.0 %all-to-all-start.2 = ((bf16[8,32,2048]{2,1,0:T(8,128)(2,1)}), bf16[8,32,2048]{2,1,0:T(8,128)(2,1)S(1)}, u32[]{:S(2)}, u32[]{:S(2)}) async-start(bf16[8,32,2048]{2,1,0:T(8,128)(2,1)} %copies.1), calls=%async_computation.2 | async-start | bytes 2097152 | tf_op jit(solution)/shard_map/all_to_all | solution.py:30
  9.7 25.5 %collective-permute-start.3 = (bf16[256,2048]{1,0:T(8,128)(2,1)S(1)}, bf16[256,2048]{1,0:T(8,128)(2,1)S(1)}, u32[]{:S(2)}, u32[]{:S(2)}) collective-permute-start(bf16[256,2048]{1,0:T(8,128)(2,1)S(1)} %copy-done.1), channel_id=1, source_target_pairs={{0,1},{1,0},{2,3},{3,2},{4,5},{5,4},{6,7},{7,6},{8,9},{9,8},{10,11... | collective-permute-start | bytes 3145736 | tf_op jit(solution)/shard_map/ppermute | solution.py:37
  15.9 8.8 %copy-start.5 = (bf16[16,512]{1,0:T(8,128)(2,1)}, bf16[16,512]{1,0:T(8,128)(2,1)S(1)}, u32[]{:S(2)}) copy-start(bf16[16,512]{1,0:T(8,128)(2,1)S(1)} %broadcast_in_dim.24.doc_ref) | copy-start | bytes 49156
  15.9 8.8 %collective-permute-start.1 = (bf16[144,128]{1,0:T(8,128)(2,1)S(1)}, bf16[144,128]{1,0:T(8,128)(2,1)S(1)}, u32[]{:S(2)}, u32[]{:S(2)}) collective-permute-start(bf16[144,128]{1,0:T(8,128)(2,1)S(1)} %get-tuple-element.17), channel_id=1, source_target_pairs={{8,0},{16,8},{24,16},{32,24},{40,32},{48,40},{56,48},{64,56},{72,6... | collective-permute-start | bytes 110600 | tf_op jit(solution)/shard_map/ppermute | solution.py:220
  17.2 7.5 %collective-permute-start = (bf16[144,128]{1,0:T(8,128)(2,1)S(1)}, bf16[144,128]{1,0:T(8,128)(2,1)S(1)}, u32[]{:S(2)}, u32[]{:S(2)}) collective-permute-start(bf16[144,128]{1,0:T(8,128)(2,1)S(1)} %get-tuple-element.18), channel_id=1, source_target_pairs={{0,8},{8,16},{16,24},{24,32},{32,40},{40,48},{48,56},{56,64},{64,7... | collective-permute-start | bytes 110600 | tf_op jit(solution)/shard_map/ppermute | solution.py:219
  24.6 0.6 copy-start.9
  24.6 0.6 copy-start.10
  31.6 4.0 %copy-start.2 = (bf16[256,256]{1,0:T(8,128)(2,1)S(1)}, bf16[256,256]{1,0:T(8,128)(2,1)}, u32[]{:S(2)}) copy-start(bf16[256,256]{1,0:T(8,128)(2,1)} %get-tuple-element.10) | copy-start | bytes 393220
  31.6 3.6 %collective-permute-start.2 = (bf16[256,256]{1,0:T(8,128)(2,1)}, bf16[256,256]{1,0:T(8,128)(2,1)S(1)}, u32[]{:S(2)}, u32[]{:S(2)}) collective-permute-start(bf16[256,256]{1,0:T(8,128)(2,1)} %get-tuple-element.11), channel_id=1, source_target_pairs={{0,1},{1,0},{2,3},{3,2},{4,5},{5,4},{6,7},{7,6},{8,9},{9,8},{10,11... | collective-permute-start | bytes 393224 | tf_op jit(solution)/shard_map/ppermute | solution.py:37
  37.1 34.5 %copy-start.6 = (f32[2048]{0:T(1024)S(1)}, f32[2048]{0:T(1024)}, u32[]{:S(2)}) copy-start(f32[2048]{0:T(1024)} %param.21) | copy-start | bytes 24580
  37.1 18.9 %all-to-all-start = ((bf16[4,64,2048]{2,1,0:T(8,128)(2,1)}), bf16[4,64,2048]{2,1,0:T(8,128)(2,1)S(1)}, u32[]{:S(2)}, u32[]{:S(2)}) async-start(bf16[4,64,2048]{2,1,0:T(8,128)(2,1)} %bitcast.5), calls=%async_computation | async-start | bytes 2097152 | tf_op jit(solution)/shard_map/all_to_all | solution.py:244
  41.2 23.9 %collective-permute-start.8 = (bf16[256,2048]{1,0:T(8,128)(2,1)S(1)}, bf16[256,2048]{1,0:T(8,128)(2,1)}, u32[]{:S(2)}, u32[]{:S(2)}) collective-permute-start(bf16[256,2048]{1,0:T(8,128)(2,1)S(1)} %bitcast.20), channel_id=1, source_target_pairs={{0,8},{1,65},{8,16},{9,73},{16,24},{17,81},{24,32},{25,89},{32,40}... | collective-permute-start | bytes 3145736 | tf_op jit(solution)/shard_map/ppermute | solution.py:23
  49.2 17.9 %collective-permute-start.5 = (bf16[256,2048]{1,0:T(8,128)(2,1)S(1)}, bf16[256,2048]{1,0:T(8,128)(2,1)}, u32[]{:S(2)}, u32[]{:S(2)}) collective-permute-start(bf16[256,2048]{1,0:T(8,128)(2,1)S(1)} %bitcast.21), channel_id=1, source_target_pairs={{0,56},{1,449},{8,0},{9,457},{16,8},{17,465},{24,16},{25,473},{32,... | collective-permute-start | bytes 3145736 | tf_op jit(solution)/shard_map/ppermute | solution.py:23
  65.1 26.1 %collective-permute-start.9 = (bf16[256,2048]{1,0:T(8,128)(2,1)}, bf16[256,2048]{1,0:T(8,128)(2,1)S(1)}, u32[]{:S(2)}, u32[]{:S(2)}) collective-permute-start(bf16[256,2048]{1,0:T(8,128)(2,1)} %collective-permute-done.8.refs_8_), channel_id=1, source_target_pairs={{0,8},{1,65},{8,16},{9,73},{16,24},{17,81},{24,32},{25,89},{32,40}... | collective-permute-start | bytes 3145736 | tf_op jit(solution)/shard_map/ppermute | solution.py:23
  67.1 27.6 %collective-permute-start.6 = (bf16[256,2048]{1,0:T(8,128)(2,1)}, bf16[256,2048]{1,0:T(8,128)(2,1)}, u32[]{:S(2)}, u32[]{:S(2)}) collective-permute-start(bf16[256,2048]{1,0:T(8,128)(2,1)} %collective-permute-done.5.refs_1_), channel_id=1, source_target_pairs={{0,56},{1,449},{8,0},{9,457},{16,8},{17,465},{24,16},{25,473},{32,... | collective-permute-start | bytes 3145736 | tf_op jit(solution)/shard_map/ppermute | solution.py:23
  89.4 19.1 %collective-permute-start.4 = (bf16[256,2048]{1,0:T(8,128)(2,1)S(1)}, bf16[256,2048]{1,0:T(8,128)(2,1)}, u32[]{:S(2)}, u32[]{:S(2)}) collective-permute-start(bf16[256,2048]{1,0:T(8,128)(2,1)S(1)} %bitcast.23), channel_id=1, source_target_pairs={{0,1},{1,0},{2,3},{3,2},{4,5},{5,4},{6,7},{7,6},{8,9},{9,8},{10,11... | collective-permute-start | bytes 3145736 | tf_op jit(solution)/shard_map/ppermute | solution.py:37
  91.3 32.8 %collective-permute-start.12 = (bf16[256,2048]{1,0:T(8,128)(2,1)S(1)}, bf16[256,2048]{1,0:T(8,128)(2,1)}, u32[]{:S(2)}, u32[]{:S(2)}) collective-permute-start(bf16[256,2048]{1,0:T(8,128)(2,1)S(1)} %collective-permute-done.9.refs_7_), channel_id=1, source_target_pairs={{0,8},{1,65},{8,16},{9,73},{16,24},{17,81},{24,32},{25,89},{32,40}... | collective-permute-start | bytes 3145736 | tf_op jit(solution)/shard_map/ppermute | solution.py:23
  94.6 29.5 %collective-permute-start.7 = (bf16[256,2048]{1,0:T(8,128)(2,1)}, bf16[256,2048]{1,0:T(8,128)(2,1)}, u32[]{:S(2)}, u32[]{:S(2)}) collective-permute-start(bf16[256,2048]{1,0:T(8,128)(2,1)} %collective-permute-done.6.refs_2_), channel_id=1, source_target_pairs={{0,56},{1,449},{8,0},{9,457},{16,8},{17,465},{24,16},{25,473},{32,... | collective-permute-start | bytes 3145736 | tf_op jit(solution)/shard_map/ppermute | solution.py:23
  99.1 20.3 %collective-permute-start.10 = (bf16[128,2048]{1,0:T(8,128)(2,1)}, bf16[128,2048]{1,0:T(8,128)(2,1)}, u32[]{:S(2)}, u32[]{:S(2)}) collective-permute-start(bf16[128,2048]{1,0:T(8,128)(2,1)} %slice.16), channel_id=1, source_target_pairs={{0,16},{1,129},{8,24},{9,137},{16,32},{17,145},{24,40},{25,153},{3... | collective-permute-start | bytes 1572872 | tf_op jit(solution)/shard_map/ppermute | solution.py:23
  104.6 19.5 %collective-permute-start.11 = (bf16[128,2048]{1,0:T(8,128)(2,1)}, bf16[128,2048]{1,0:T(8,128)(2,1)}, u32[]{:S(2)}, u32[]{:S(2)}) collective-permute-start(bf16[128,2048]{1,0:T(8,128)(2,1)} %slice.17), channel_id=1, source_target_pairs={{0,48},{1,385},{8,56},{9,393},{16,0},{17,401},{24,8},{25,409},{32,... | collective-permute-start | bytes 1572872 | tf_op jit(solution)/shard_map/ppermute | solution.py:23
  131.9 5.5 %collective-permute-start.13 = (bf16[256,2048]{1,0:T(8,128)(2,1)S(1)}, bf16[256,2048]{1,0:T(8,128)(2,1)S(1)}, u32[]{:S(2)}, u32[]{:S(2)}) collective-permute-start(bf16[256,2048]{1,0:T(8,128)(2,1)S(1)} %get-tuple-element.14), channel_id=1, source_target_pairs={{0,1},{1,0},{2,3},{3,2},{4,5},{5,4},{6,7},{7,6},{8,9},{9,8},{10,11... | collective-permute-start | bytes 3145736 | tf_op jit(solution)/shard_map/ppermute | solution.py:37
  171.1 6.7 %collective-permute-start.14 = (bf16[256,2048]{1,0:T(8,128)(2,1)S(1)}, bf16[256,2048]{1,0:T(8,128)(2,1)S(1)}, u32[]{:S(2)}, u32[]{:S(2)}) collective-permute-start(bf16[256,2048]{1,0:T(8,128)(2,1)S(1)} %bitcast.25), channel_id=1, source_target_pairs={{0,1},{1,0},{2,3},{3,2},{4,5},{5,4},{6,7},{7,6},{8,9},{9,8},{10,11... | collective-permute-start | bytes 3145736 | tf_op jit(solution)/shard_map/ppermute | solution.py:37
  175.9 1.9 %copy-start = (bf16[512,2048]{1,0:T(8,128)(2,1)}, bf16[512,2048]{1,0:T(8,128)(2,1)S(1)}, u32[]{:S(2)}) copy-start(bf16[512,2048]{1,0:T(8,128)(2,1)S(1)} %constant_dynamic-update-slice_fusion.1) | copy-start | bytes 6291460

commit v5 on v4

--- a/solution.py
+++ b/solution.py
@@ -57,7 +57,7 @@
         copies_body,
         in_specs=[vmem, vmem],
         out_specs=vmem,
-        out_shape=jax.ShapeDtypeStruct((count, rows, 2 * units), up.dtype),
+        out_shape=pltpu.VMEM((count, rows, 2 * units), up.dtype),
         name="copies",
     )(up, down_t)
 
@@ -73,55 +73,102 @@
     return wide * lax.rsqrt(jnp.mean(wide * wide, axis=-1, keepdims=True) + EPS) * gain
 
 
-def mixer_body(at_ref, theirs_ref, mine_ref, *refs):
-    *pieces, down_ref, act_ref, out_ref, up_ref = refs
-    count = len(pieces) - 1
+def place(at_ref, r, count, chunk, source, put):
+    index = lax.rem(at_ref[0] + r, count)
+    for j in range(count):
+        to = pl.multiple_of(j * at_ref[1] + index * at_ref[2], chunk)
+        put(pl.ds(to, chunk), source(slice(j * chunk, (j + 1) * chunk)))
+
+
+def begin_body(at_ref, theirs_ref, mine_ref, *refs):
+    *pieces, total_ref, picked_ref, down_ref, up_ref = refs
+    count = len(pieces) + 1
+    units = total_ref.shape[1]
+    block = picked_ref.shape[1]
+    chunk = block // count
+    height = mine_ref.shape[0]
+    blank = jnp.zeros((chunk, units), up_ref.dtype)
+    for r in range(count):
+        if r == count // 2:
+            place(at_ref, r, count, chunk, lambda _: blank, up_ref.__setitem__)
+            continue
+        piece = pieces[r if r < count // 2 else r - 1]
+        place(at_ref, r, count, chunk, lambda rows: piece[rows, :units], up_ref.__setitem__)
+        place(at_ref, r, count, chunk, lambda rows: piece[rows, units:], down_ref.__setitem__)
+    index = lax.rem(at_ref[0] + count // 2, count)
+    row = lax.broadcasted_iota(jnp.int32, (up_ref.shape[0], block), 0)
+    col = lax.broadcasted_iota(jnp.int32, (up_ref.shape[0], block), 1)
+    wanted = (col // chunk) * at_ref[1] + col % chunk + index * at_ref[2]
+    pick = jnp.where(row == wanted, 1.0, 0.0).astype(jnp.bfloat16)
+    for i, rows_ref in enumerate((theirs_ref, mine_ref)):
+        rows = rows_ref[...]
+        span = slice(i * height, (i + 1) * height)
+        total_ref[span] = jnp.dot(rows, up_ref[...], preferred_element_type=jnp.float32)
+        picked_ref[span] = jnp.dot(rows, pick, preferred_element_type=jnp.float32).astype(
+            jnp.bfloat16
+        )
+
+
+def begin(at, theirs, mine, pieces):
+    height, width = mine.shape
+    block, units = pieces[0].shape[0], pieces[0].shape[1] // 2
+    smem = pl.BlockSpec(memory_space=pltpu.SMEM)
+    vmem = pl.BlockSpec(memory_space=pltpu.VMEM)
+    return pl.pallas_call(
+        begin_body,
+        in_specs=[smem] + [vmem] * (2 + len(pieces)),
+        out_specs=[vmem] * 3,
+        out_shape=[
+            pltpu.VMEM((2 * height, units), jnp.float32),
+            pltpu.VMEM((2 * height, block), jnp.bfloat16),
+            pltpu.VMEM((width, units), jnp.bfloat16),
+        ],
+        scratch_shapes=[pltpu.VMEM((width, units), jnp.bfloat16)],
+        cost_estimate=pl.CostEstimate(flops=1 << 31, transcendentals=0, bytes_accessed=1 << 23),
+        compiler_params=pltpu.CompilerParams(vmem_limit_bytes=36 << 20),
+        name="begin",
+    )(at, theirs, mine, *pieces)
+
+
+def mixer_body(at_ref, total_ref, picked_ref, first_ref, second_ref, _, act_ref, out_ref, down_ref):
     units = act_ref.shape[1]
-    cut = pieces[count // 2].shape[0]
-    chunk = 2 * cut // count
-    for r in range(count):
-        index = lax.rem(at_ref[0] + r, count)
-        for j in range(count):
-            if r < count // 2:
-                source, low = pieces[r], j * chunk
-            elif r > count // 2:
-                source, low = pieces[r + 1], j * chunk
-            else:
-                source, low = pieces[r + j * chunk // cut], j * chunk % cut
-            to = pl.multiple_of(j * at_ref[1] + index * at_ref[2], chunk)
-            up_ref[pl.ds(to, chunk), :] = source[low : low + chunk, :units]
-            down_ref[pl.ds(to, chunk), :] = source[low : low + chunk, units:]
-
-    def hidden(rows):
-        wide = jnp.dot(rows, up_ref[...], preferred_element_type=jnp.float32)
-        return jnp.square(jnp.maximum(wide, 0.0)).astype(jnp.bfloat16)
-
-    first = hidden(theirs_ref[...])
-    act_ref[...] = hidden(mine_ref[...])
+    block = picked_ref.shape[1]
+    height, width = out_ref.shape
+    count = width // block
+    last = jnp.concatenate([first_ref[...], second_ref[...]], axis=0)
+    place(
+        at_ref, count // 2, count, block // count, lambda rows: last[rows, units:],
+        down_ref.__setitem__,
+    )
+    wide = total_ref[...] + jnp.dot(
+        picked_ref[...], last[:, :units], preferred_element_type=jnp.float32
+    )
+    act = jnp.square(jnp.maximum(wide, 0.0)).astype(jnp.bfloat16)
+    act_ref[...] = act[height:]
     out_ref[...] = lax.dot_general(
-        first, down_ref[...], (((1,), (1,)), ((), ())), preferred_element_type=jnp.float32
+        act[:height], down_ref[...], (((1,), (1,)), ((), ())), preferred_element_type=jnp.float32
     ).astype(out_ref.dtype)
 
 
-def mixer(at, theirs, mine, pieces):
-    height, width = mine.shape
-    units = pieces[0].shape[1] // 2
+def mixer(at, total, picked, first, second, down_t):
+    width, units = down_t.shape
+    height = total.shape[0] // 2
     smem = pl.BlockSpec(memory_space=pltpu.SMEM)
     vmem = pl.BlockSpec(memory_space=pltpu.VMEM)
     return pl.pallas_call(
         mixer_body,
-        in_specs=[smem] + [vmem] * (2 + len(pieces)),
+        in_specs=[smem] + [vmem] * 5,
         out_specs=[vmem] * 3,
         out_shape=[
-            jax.ShapeDtypeStruct((width, units), jnp.bfloat16),
-            jax.ShapeDtypeStruct((height, units), jnp.bfloat16),
-            jax.ShapeDtypeStruct((height, width), jnp.bfloat16),
+            pltpu.VMEM((height, units), jnp.bfloat16),
+            pltpu.VMEM((height, width), jnp.bfloat16),
+            pltpu.VMEM((width, units), jnp.bfloat16),
         ],
-        scratch_shapes=[pltpu.VMEM((width, units), jnp.bfloat16)],
-        cost_estimate=pl.CostEstimate(flops=1 << 31, transcendentals=0, bytes_accessed=1 << 23),
-        compiler_params=pltpu.CompilerParams(vmem_limit_bytes=40 << 20),
+        input_output_aliases={5: 2},
+        cost_estimate=pl.CostEstimate(flops=1 << 30, transcendentals=0, bytes_accessed=1 << 22),
+        compiler_params=pltpu.CompilerParams(vmem_limit_bytes=32 << 20),
         name="mixer",
-    )(at, theirs, mine, *pieces)
+    )(at, total, picked, first, second, down_t)
 
 
 def attention_body(
@@ -185,7 +232,7 @@
     head, rows = kt.shape
     smem = pl.BlockSpec(memory_space=pltpu.SMEM)
     vmem = pl.BlockSpec(memory_space=pltpu.VMEM)
-    out = jax.ShapeDtypeStruct((rows // 2, q.shape[1]), jnp.bfloat16)
+    out = pltpu.VMEM((rows // 2, q.shape[1]), jnp.bfloat16)
     return pl.pallas_call(
         attention_body,
         in_specs=[smem] * 3 + [vmem] * 8,
@@ -235,7 +282,7 @@
     up2, dn2 = along(up1, 1), along(dn1, -1)
     up3, dn3 = along(up2, 1), along(dn2, -1)
     up4, dn4 = along(up2[:cut], 2), along(dn2[cut:], -2)
-    pieces = [piece, dn1, dn2, dn3, up4, dn4, up3, up2, up1]
+    pieces = [piece, dn1, dn2, dn3, up3, up2, up1]
 
     att_other = swap(att_send)
     partial = jnp.dot(att_own, w_out, preferred_element_type=jnp.float32) + jnp.dot(
@@ -256,7 +303,8 @@
     at = jnp.stack(
         [jnp.where(core == 0, y, z), jnp.where(core == 0, block, chunk), jnp.where(core == 0, chunk, block)]
     ).astype(jnp.int32)
-    down_t, active, out = mixer(at, theirs, mine, pieces)
+    total, picked, down_t = begin(at, theirs, mine, pieces)
+    active, out, down_t = mixer(at, total, picked, up4, dn4, down_t)
     sent = swap(out)
     kept = lax.optimization_barrier(
         lax.dot_general(

time: 181 us -> 173 us (0.956)
  waiting for transfers between devices: 30.3 us -> 22.2 us
  matrix products: 5.39 us -> 3.17 us
  blocking collectives: 50.5 us -> 52.5 us
    ppermute x8, waiting for transfers between devices: 23.4 us -> 13.4 us  [along(): return lax.ppermute(x, ('z', 'y', 'c'), pairs)]
    ppermute x5, starting transfers between devices: 16.3 us -> 19.3 us  [swap(): return lax.ppermute(x, 'c', [(0, 1), (1, 0)])]
    dot_general x1, matrix products: 3.53 us -> 1.28 us  [shards(): lax.dot_general(active, down_t, (((1,), (1,)), ((), ())), preferred_eleme...]
    ppermute x8, starting transfers between devices: 34.4 us -> 32.4 us  [along(): return lax.ppermute(x, ('z', 'y', 'c'), pairs)]
    all_to_all x2, blocking collectives: 33.4 us -> 35.3 us  [spread(): lax.all_to_all(jnp.broadcast_to(x, (n, *x.shape)), axis, 0, 0, tiled=True)]
    pallas_call x1 -> x2, Pallas kernels: 7.8 us -> 8.96 us  [the longest x1 6.18 us: begin(): pl.pallas_call(begin_body, in_specs=[smem] + [vmem] * (2 + len(pieces)),...]
  transfers between devices with their start and end apart: 17 -> 17, of which waited for: 7 -> 9; matrix products, arithmetic and copies ran while one was open for 6% -> 5% of each run, Pallas kernels for 4% -> 7%
where the time goes in v5:
time: 173 us; the launch traced here: 171 us
  starting transfers between devices  68 us (39%)
  blocking collectives  52.5 us (30%)
  waiting for transfers between devices  22.2 us (13%)
  Pallas kernels  16.7 us (10%)
  local copies, waits for them, and re-layouts  5.66 us (3%)
  matrix products  3.17 us (2%)
  other arithmetic  2.59 us (1%)
    all_to_all x2, blocking collectives, spread(): lax.all_to_all(jnp.broadcast_to(x, (n, *x.shape)), axis, 0, 0, tiled=True)  35.3 us
    ppermute x8, starting transfers between devices, along(): return lax.ppermute(x, ('z', 'y', 'c'), pairs)  32.4 us
    ppermute x5, starting transfers between devices, swap(): return lax.ppermute(x, 'c', [(0, 1), (1, 0)])  19.3 us
    all_to_all x1, blocking collectives, scatter_x(): lax.all_to_all(x.reshape(n, x.shape[0] // n, x.shape[1]), 'x', 0, 0, tile...  17.2 us
    ppermute x8, waiting for transfers between devices, along(): return lax.ppermute(x, ('z', 'y', 'c'), pairs)  13.4 us
    all_to_all x1, starting transfers between devices, across(): lax.all_to_all(copies, ('z', 'y', 'c'), 0, 0, tiled=True, axis_index_grou...  7.64 us
    pallas_call x1, Pallas kernels, begin(): pl.pallas_call(begin_body, in_specs=[smem] + [vmem] * (2 + len(pieces)),...  6.18 us
    pallas_call x1, Pallas kernels, attention(): pl.pallas_call(attention_body, in_specs=[smem] * 3 + [vmem] * 8, out_spec...  5.71 us
  transfers between devices with their start and end apart: 17, of which 9 were waited for; matrix products, arithmetic and copies ran while one was open for 5% of the time, Pallas kernels for 7%

profile of v5, /device:TPU:1, one launch (start us, length us, event | category | flops | bytes accessed | tf_op | source)
XLA Modules:
  0.0 171.2 jit_solution(1774451214929473932)
XLA Ops:
  0.0 0.0 copy-start.3
  0.0 2.0 %copies.1 = bf16[8,32,2048]{2,1,0:T(8,128)(2,1)} custom-call(bf16[32,1024]{1,0:T(8,128)(2,1)} %up_ref.1, bf16[32,1024]{1,0:T(8,128)(2,1)} %bitcast.28), custom_call_target="tpu_custom_call" | custom-call | tf_op jit(solution)/shard_map/copies/pallas_call | solution.py:56
  2.1 7.6 %all-to-all-start.2 = ((bf16[8,32,2048]{2,1,0:T(8,128)(2,1)}), bf16[8,32,2048]{2,1,0:T(8,128)(2,1)S(1)}, u32[]{:S(2)}, u32[]{:S(2)}) async-start(bf16[8,32,2048]{2,1,0:T(8,128)(2,1)} %copies.1), calls=%async_computation.2 | async-start | bytes 2097152 | tf_op jit(solution)/shard_map/all_to_all | solution.py:30
  9.7 0.0 copy-done.1
  9.7 6.1 %collective-permute-start.3 = (bf16[256,2048]{1,0:T(8,128)(2,1)S(1)}, bf16[256,2048]{1,0:T(8,128)(2,1)S(1)}, u32[]{:S(2)}, u32[]{:S(2)}) collective-permute-start(bf16[256,2048]{1,0:T(8,128)(2,1)S(1)} %copy-done.1), channel_id=1, source_target_pairs={{0,1},{1,0},{2,3},{3,2},{4,5},{5,4},{6,7},{7,6},{8,9},{9,8},{10,11... | collective-permute-start | bytes 3145736 | tf_op jit(solution)/shard_map/ppermute | solution.py:37
  15.9 3.2 %collective-permute-start = (bf16[144,128]{1,0:T(8,128)(2,1)S(1)}, bf16[144,128]{1,0:T(8,128)(2,1)S(1)}, u32[]{:S(2)}, u32[]{:S(2)}) collective-permute-start(bf16[144,128]{1,0:T(8,128)(2,1)S(1)} %get-tuple-element.24), channel_id=1, source_target_pairs={{0,8},{8,16},{16,24},{24,32},{32,40},{40,48},{48,56},{56,64},{64,7... | collective-permute-start | bytes 110600 | tf_op jit(solution)/shard_map/ppermute | solution.py:266
  19.1 1.3 collective-permute-start.1
  20.4 0.6 multiply_exponential_fusion.slope_ref
  21.0 0.7 copy.14.kg_ref
  21.7 0.0 collective-permute-done.before_ref
  21.7 2.6 %collective-permute-done.1.after_ref = bf16[144,128]{1,0:T(8,128)(2,1)S(1)} collective-permute-done((bf16[144,128]{1,0:T(8,128)(2,1)S(1)}, bf16[144,128]{1,0:T(8,128)(2,1)S(1)}, u32[]{:S(2)}, u32[]{:S(2)}) %collective-permute-start.1) | collective-permute-done | bytes 36896 | tf_op jit(solution)/shard_map/ppermute | solution.py:267
  24.2 0.0 copy-done.4
  24.3 0.6 copy-done.9
  24.9 5.7 %attend.1 = (bf16[256,256]{1,0:T(8,128)(2,1)S(1)}, bf16[256,256]{1,0:T(8,128)(2,1)S(1)}) custom-call(s32[1]{0:T(128)} %bitcast.core_ref, f32[4]{0:T(128)} %multiply_exponential_fusion.slope_ref, f32[4]{0:T(128)} %sink_ref.1, bf16[512,256]{1,0:T(8,128)(2,1)} %q_ref.1, bf16[64,512]{1,0:T(8,128)(2,1)} %bitcast.29, bf16[64,512]{1,0:T(8,128)(2,1)} %bitcast.31, ...), custom_call_target="tpu_custom_call" | custom-call | flops 2147483648 | bytes 1048576 | tf_op jit(solution)/shard_map/attend/pallas_call | solution.py:236
  30.6 2.9 %collective-permute-start.2 = (bf16[256,256]{1,0:T(8,128)(2,1)S(1)}, bf16[256,256]{1,0:T(8,128)(2,1)S(1)}, u32[]{:S(2)}, u32[]{:S(2)}) collective-permute-start(bf16[256,256]{1,0:T(8,128)(2,1)S(1)} %get-tuple-element.14), channel_id=1, source_target_pairs={{0,1},{1,0},{2,3},{3,2},{4,5},{5,4},{6,7},{7,6},{8,9},{9,8},{10,11... | collective-permute-start | bytes 393224 | tf_op jit(solution)/shard_map/ppermute | solution.py:37
  33.5 1.0 collective-permute-done.2
  34.4 0.0 collective-permute-done.3
  34.4 0.4 fusion.5
  34.9 1.5 fusion
  36.3 0.0 all-to-all-done.2
  36.3 4.1 %all-to-all-start = ((bf16[4,64,2048]{2,1,0:T(8,128)(2,1)}), bf16[4,64,2048]{2,1,0:T(8,128)(2,1)S(1)}, u32[]{:S(2)}, u32[]{:S(2)}) async-start(bf16[4,64,2048]{2,1,0:T(8,128)(2,1)} %bitcast.5), calls=%async_computation | async-start | bytes 2097152 | tf_op jit(solution)/shard_map/all_to_all | solution.py:291
  40.5 4.1 %collective-permute-start.8 = (bf16[256,2048]{1,0:T(8,128)(2,1)S(1)}, bf16[256,2048]{1,0:T(8,128)(2,1)}, u32[]{:S(2)}, u32[]{:S(2)}) collective-permute-start(bf16[256,2048]{1,0:T(8,128)(2,1)S(1)} %bitcast.20), channel_id=1, source_target_pairs={{0,8},{1,65},{8,16},{9,73},{16,24},{17,81},{24,32},{25,89},{32,40}... | collective-permute-start | bytes 3145736 | tf_op jit(solution)/shard_map/ppermute | solution.py:23
  44.6 8.0 %collective-permute-start.5 = (bf16[256,2048]{1,0:T(8,128)(2,1)S(1)}, bf16[256,2048]{1,0:T(8,128)(2,1)}, u32[]{:S(2)}, u32[]{:S(2)}) collective-permute-start(bf16[256,2048]{1,0:T(8,128)(2,1)S(1)} %bitcast.21), channel_id=1, source_target_pairs={{0,56},{1,449},{8,0},{9,457},{16,8},{17,465},{24,16},{25,473},{32,... | collective-permute-start | bytes 3145736 | tf_op jit(solution)/shard_map/ppermute | solution.py:23
  52.6 2.5 %all-to-all-done = bf16[4,64,2048]{2,1,0:T(8,128)(2,1)S(1)} async-done(((bf16[4,64,2048]{2,1,0:T(8,128)(2,1)}), bf16[4,64,2048]{2,1,0:T(8,128)(2,1)S(1)}, u32[]{:S(2)}, u32[]{:S(2)}) %all-to-all-start) | async-done | bytes 1048608 | tf_op jit(solution)/shard_map/all_to_all | solution.py:291
  55.0 0.2 convert_reduce_fusion.1
  55.2 1.1 fusion.1
  56.4 6.6 %collective-permute-done.8.refs_6_ = bf16[256,2048]{1,0:T(8,128)(2,1)} collective-permute-done((bf16[256,2048]{1,0:T(8,128)(2,1)S(1)}, bf16[256,2048]{1,0:T(8,128)(2,1)}, u32[]{:S(2)}, u32[]{:S(2)}) %collective-permute-start.8) | collective-permute-done | bytes 1048608 | tf_op jit(solution)/shard_map/ppermute | solution.py:23
  62.9 1.9 %collective-permute-start.9 = (bf16[256,2048]{1,0:T(8,128)(2,1)}, bf16[256,2048]{1,0:T(8,128)(2,1)S(1)}, u32[]{:S(2)}, u32[]{:S(2)}) collective-permute-start(bf16[256,2048]{1,0:T(8,128)(2,1)} %collective-permute-done.8.refs_6_), channel_id=1, source_target_pairs={{0,8},{1,65},{8,16},{9,73},{16,24},{17,81},{24,32},{25,89},{32,40}... | collective-permute-start | bytes 3145736 | tf_op jit(solution)/shard_map/ppermute | solution.py:23
  64.8 0.0 collective-permute-done.5.refs_1_
  64.8 4.6 %collective-permute-start.6 = (bf16[256,2048]{1,0:T(8,128)(2,1)}, bf16[256,2048]{1,0:T(8,128)(2,1)}, u32[]{:S(2)}, u32[]{:S(2)}) collective-permute-start(bf16[256,2048]{1,0:T(8,128)(2,1)} %collective-permute-done.5.refs_1_), channel_id=1, source_target_pairs={{0,56},{1,449},{8,0},{9,457},{16,8},{17,465},{24,16},{25,473},{32,... | collective-permute-start | bytes 3145736 | tf_op jit(solution)/shard_map/ppermute | solution.py:23
  69.4 0.1 fusion.3
  69.6 0.1 broadcast_in_dim.27
  69.7 18.9 %all_to_all.25 = bf16[4,64,2048]{2,1,0:T(8,128)(2,1)S(1)} all-to-all(bf16[4,64,2048]{2,1,0:T(8,128)(2,1)S(1)} %broadcast_in_dim.27), channel_id=1, replica_groups=mesh['z'=8,'y'=8,'x'=4,'c'=2] {'x'}, dimensions={0} | all-to-all | bytes 2097152 | tf_op jit(solution)/shard_map/all_to_all | solution.py:42
  88.6 3.1 %collective-permute-start.4 = (bf16[256,2048]{1,0:T(8,128)(2,1)S(1)}, bf16[256,2048]{1,0:T(8,128)(2,1)}, u32[]{:S(2)}, u32[]{:S(2)}) collective-permute-start(bf16[256,2048]{1,0:T(8,128)(2,1)S(1)} %bitcast.23), channel_id=1, source_target_pairs={{0,1},{1,0},{2,3},{3,2},{4,5},{5,4},{6,7},{7,6},{8,9},{9,8},{10,11... | collective-permute-start | bytes 3145736 | tf_op jit(solution)/shard_map/ppermute | solution.py:37
  91.7 0.0 collective-permute-done.9.refs_5_
  91.7 1.9 %collective-permute-start.10 = (bf16[256,2048]{1,0:T(8,128)(2,1)S(1)}, bf16[256,2048]{1,0:T(8,128)(2,1)}, u32[]{:S(2)}, u32[]{:S(2)}) collective-permute-start(bf16[256,2048]{1,0:T(8,128)(2,1)S(1)} %collective-permute-done.9.refs_5_), channel_id=1, source_target_pairs={{0,8},{1,65},{8,16},{9,73},{16,24},{17,81},{24,32},{25,89},{32,40}... | collective-permute-start | bytes 3145736 | tf_op jit(solution)/shard_map/ppermute | solution.py:23
  93.6 0.0 collective-permute-done.6.refs_2_
  93.6 4.6 %collective-permute-start.7 = (bf16[256,2048]{1,0:T(8,128)(2,1)}, bf16[256,2048]{1,0:T(8,128)(2,1)}, u32[]{:S(2)}, u32[]{:S(2)}) collective-permute-start(bf16[256,2048]{1,0:T(8,128)(2,1)} %collective-permute-done.6.refs_2_), channel_id=1, source_target_pairs={{0,56},{1,449},{8,0},{9,457},{16,8},{17,465},{24,16},{25,473},{32,... | collective-permute-start | bytes 3145736 | tf_op jit(solution)/shard_map/ppermute | solution.py:23
  98.2 0.8 slice.16
  99.0 1.9 %collective-permute-start.11 = (bf16[128,2048]{1,0:T(8,128)(2,1)}, bf16[128,2048]{1,0:T(8,128)(2,1)}, u32[]{:S(2)}, u32[]{:S(2)}) collective-permute-start(bf16[128,2048]{1,0:T(8,128)(2,1)} %slice.16), channel_id=1, source_target_pairs={{0,16},{1,129},{8,24},{9,137},{16,32},{17,145},{24,40},{25,153},{3... | collective-permute-start | bytes 1572872 | tf_op jit(solution)/shard_map/ppermute | solution.py:23
  101.0 1.9 %slice.17 = bf16[128,2048]{1,0:T(8,128)(2,1)} slice(bf16[256,2048]{1,0:T(8,128)(2,1)} %collective-permute-done.6.refs_2_), slice={[128:256], [0:2048]} | slice | bytes 1048576 | tf_op jit(solution)/shard_map/slice | solution.py:284
  102.8 5.5 %collective-permute-start.12 = (bf16[128,2048]{1,0:T(8,128)(2,1)}, bf16[128,2048]{1,0:T(8,128)(2,1)}, u32[]{:S(2)}, u32[]{:S(2)}) collective-permute-start(bf16[128,2048]{1,0:T(8,128)(2,1)} %slice.17), channel_id=1, source_target_pairs={{0,48},{1,385},{8,56},{9,393},{16,0},{17,401},{24,8},{25,409},{32,... | collective-permute-start | bytes 1572872 | tf_op jit(solution)/shard_map/ppermute | solution.py:23
  108.3 0.1 pad_add_fusion.at_ref
  108.4 0.0 collective-permute-done.4.theirs_ref
  108.4 0.9 collective-permute-done.10.refs_4_
  109.3 1.1 collective-permute-done.7.refs_3_
  110.4 6.2 %begin.1 = (f32[512,1024]{1,0:T(8,128)S(1)}, bf16[512,256]{1,0:T(8,128)(2,1)S(1)}, bf16[2048,1024]{1,0:T(8,128)(2,1)S(1)}) custom-call(s32[3]{0:T(128)S(1)} %pad_add_fusion.at_ref, bf16[256,2048]{1,0:T(8,128)(2,1)} %collective-permute-done.4.theirs_ref, bf16[256,2048]{1,0:T(8,128)(2,1)S(1)} %bitcast.24, bf16[256,2048]{1,0:T(8,128)(2,1)S(1)} %bitcast.22, ...), custom_call_target="tpu_custom_call" | custom-call | flops 2147483648 | bytes 8388608 | tf_op jit(solution)/shard_map/begin/pallas_call | solution.py:117
  116.6 0.0 collective-permute-done.11.first_ref
  116.6 4.9 %collective-permute-done.12.second_ref = bf16[128,2048]{1,0:T(8,128)(2,1)} collective-permute-done((bf16[128,2048]{1,0:T(8,128)(2,1)}, bf16[128,2048]{1,0:T(8,128)(2,1)}, u32[]{:S(2)}, u32[]{:S(2)}) %collective-permute-start.12) | collective-permute-done | bytes 524320 | tf_op jit(solution)/shard_map/ppermute | solution.py:23
  121.5 2.8 %mixer.1 = (bf16[256,1024]{1,0:T(8,128)(2,1)S(1)}, bf16[256,2048]{1,0:T(8,128)(2,1)S(1)}, bf16[2048,1024]{1,0:T(8,128)(2,1)S(1)}) custom-call(s32[3]{0:T(128)S(1)} %pad_add_fusion.at_ref, f32[512,1024]{1,0:T(8,128)S(1)} %get-tuple-element.15.total_ref, bf16[512,256]{1,0:T(8,128)(2,1)S(1)} %get-tuple-element.16.picked_ref, ...), custom_call_target="tpu_custom_call", output_to_operand_aliasing={{2}: (5, {})} | custom-call | flops 1073741824 | bytes 4194304 | tf_op jit(solution)/shard_map/mixer/pallas_call | solution.py:158
  124.3 3.2 %collective-permute-start.13 = (bf16[256,2048]{1,0:T(8,128)(2,1)S(1)}, bf16[256,2048]{1,0:T(8,128)(2,1)S(1)}, u32[]{:S(2)}, u32[]{:S(2)}) collective-permute-start(bf16[256,2048]{1,0:T(8,128)(2,1)S(1)} %get-tuple-element.20), channel_id=1, source_target_pairs={{0,1},{1,0},{2,3},{3,2},{4,5},{5,4},{6,7},{7,6},{8,9},{9,8},{10,11... | collective-permute-start | bytes 3145736 | tf_op jit(solution)/shard_map/ppermute | solution.py:37
  127.5 1.3 fusion.6
  128.8 0.8 collective-permute-done.13
  129.6 0.3 add_convert_fusion
  129.9 17.2 %all_to_all.26 = bf16[4,64,2048]{2,1,0:T(8,128)(2,1)S(1)} all-to-all(bf16[4,64,2048]{2,1,0:T(8,128)(2,1)S(1)} %bitcast.27), channel_id=1, replica_groups=mesh['z'=8,'y'=8,'x'=4,'c'=2] {'x'}, dimensions={0} | all-to-all | bytes 2097152 | tf_op jit(solution)/shard_map/all_to_all | solution.py:67
  147.2 0.2 convert_reduce_fusion
  147.4 0.1 broadcast_in_dim.28
  147.5 16.4 %all_to_all.27 = bf16[4,64,2048]{2,1,0:T(8,128)(2,1)S(1)} all-to-all(bf16[4,64,2048]{2,1,0:T(8,128)(2,1)S(1)} %broadcast_in_dim.28), channel_id=1, replica_groups=mesh['z'=8,'y'=8,'x'=4,'c'=2] {'x'}, dimensions={0} | all-to-all | bytes 2097152 | tf_op jit(solution)/shard_map/all_to_all | solution.py:42
  163.9 4.0 %collective-permute-start.14 = (bf16[256,2048]{1,0:T(8,128)(2,1)S(1)}, bf16[256,2048]{1,0:T(8,128)(2,1)S(1)}, u32[]{:S(2)}, u32[]{:S(2)}) collective-permute-start(bf16[256,2048]{1,0:T(8,128)(2,1)S(1)} %bitcast.25), channel_id=1, source_target_pairs={{0,1},{1,0},{2,3},{3,2},{4,5},{5,4},{6,7},{7,6},{8,9},{9,8},{10,11... | collective-permute-start | bytes 3145736 | tf_op jit(solution)/shard_map/ppermute | solution.py:37
  167.9 0.2 broadcast_in_dim.23
  168.1 0.1 constant_dynamic-update-slice_fusion.1
  168.2 0.0 copy-start
  168.2 1.9 %collective-permute-done.14 = bf16[256,2048]{1,0:T(8,128)(2,1)S(1)} collective-permute-done((bf16[256,2048]{1,0:T(8,128)(2,1)S(1)}, bf16[256,2048]{1,0:T(8,128)(2,1)S(1)}, u32[]{:S(2)}, u32[]{:S(2)}) %collective-permute-start.14) | collective-permute-done | bytes 1048608 | tf_op jit(solution)/shard_map/ppermute | solution.py:37
  170.1 1.0 constant_dynamic-update-slice_fusion
  (20 shorter events, 0.1 us)
Async XLA Ops:
  0.0 9.7 %copy-start.1 = (bf16[256,2048]{1,0:T(8,128)(2,1)S(1)}, bf16[256,2048]{1,0:T(8,128)(2,1)}, u32[]{:S(2)}) copy-start(bf16[256,2048]{1,0:T(8,128)(2,1)} %param.20) | copy-start | bytes 3145732
  0.0 15.8 %copy-start.6 = (s32[512]{0:T(512)S(1)}, s32[512]{0:T(512)}, u32[]{:S(2)}) copy-start(s32[512]{0:T(512)} %param.16) | copy-start | bytes 6148
  0.0 15.8 %copy-start.2 = (bf16[512,64]{0,1:T(8,128)(2,1)S(1)}, bf16[512,64]{0,1:T(8,128)(2,1)}, u32[]{:S(2)}) copy-start(bf16[512,64]{0,1:T(8,128)(2,1)} %param.14) | copy-start | bytes 196612
  0.0 15.8 %copy-start.3 = (bf16[512,64]{0,1:T(8,128)(2,1)S(1)}, bf16[512,64]{0,1:T(8,128)(2,1)}, u32[]{:S(2)}) copy-start(bf16[512,64]{0,1:T(8,128)(2,1)} %param.15) | copy-start | bytes 196612
  0.0 20.9 %copy-start.7 = (f32[64]{0:T(128)S(1)}, f32[64]{0:T(128)}, u32[]{:S(2)}) copy-start(f32[64]{0:T(128)} %param.18) | copy-start | bytes 772
  2.1 34.3 %all-to-all-start.2 = ((bf16[8,32,2048]{2,1,0:T(8,128)(2,1)}), bf16[8,32,2048]{2,1,0:T(8,128)(2,1)S(1)}, u32[]{:S(2)}, u32[]{:S(2)}) async-start(bf16[8,32,2048]{2,1,0:T(8,128)(2,1)} %copies.1), calls=%async_computation.2 | async-start | bytes 2097152 | tf_op jit(solution)/shard_map/all_to_all | solution.py:30
  9.7 24.7 %collective-permute-start.3 = (bf16[256,2048]{1,0:T(8,128)(2,1)S(1)}, bf16[256,2048]{1,0:T(8,128)(2,1)S(1)}, u32[]{:S(2)}, u32[]{:S(2)}) collective-permute-start(bf16[256,2048]{1,0:T(8,128)(2,1)S(1)} %copy-done.1), channel_id=1, source_target_pairs={{0,1},{1,0},{2,3},{3,2},{4,5},{5,4},{6,7},{7,6},{8,9},{9,8},{10,11... | collective-permute-start | bytes 3145736 | tf_op jit(solution)/shard_map/ppermute | solution.py:37
  15.8 8.4 %copy-start.4 = (bf16[16,512]{1,0:T(8,128)(2,1)}, bf16[16,512]{1,0:T(8,128)(2,1)S(1)}, u32[]{:S(2)}) copy-start(bf16[16,512]{1,0:T(8,128)(2,1)S(1)} %broadcast_in_dim.24.doc_ref) | copy-start | bytes 49156
  15.9 5.8 %collective-permute-start = (bf16[144,128]{1,0:T(8,128)(2,1)S(1)}, bf16[144,128]{1,0:T(8,128)(2,1)S(1)}, u32[]{:S(2)}, u32[]{:S(2)}) collective-permute-start(bf16[144,128]{1,0:T(8,128)(2,1)S(1)} %get-tuple-element.24), channel_id=1, source_target_pairs={{0,8},{8,16},{16,24},{24,32},{32,40},{40,48},{48,56},{56,64},{64,7... | collective-permute-start | bytes 110600 | tf_op jit(solution)/shard_map/ppermute | solution.py:266
  19.1 5.2 %collective-permute-start.1 = (bf16[144,128]{1,0:T(8,128)(2,1)S(1)}, bf16[144,128]{1,0:T(8,128)(2,1)S(1)}, u32[]{:S(2)}, u32[]{:S(2)}) collective-permute-start(bf16[144,128]{1,0:T(8,128)(2,1)S(1)} %get-tuple-element.23), channel_id=1, source_target_pairs={{8,0},{16,8},{24,16},{32,24},{40,32},{48,40},{56,48},{64,56},{72,6... | collective-permute-start | bytes 110600 | tf_op jit(solution)/shard_map/ppermute | solution.py:267
  21.7 2.6 %copy-start.8 = (bf16[144,128]{1,0:T(8,128)(2,1)}, bf16[144,128]{1,0:T(8,128)(2,1)S(1)}, u32[]{:S(2)}) copy-start(bf16[144,128]{1,0:T(8,128)(2,1)S(1)} %collective-permute-done.before_ref) | copy-start | bytes 110596
  24.2 0.6 copy-start.9
  30.6 3.9 %collective-permute-start.2 = (bf16[256,256]{1,0:T(8,128)(2,1)S(1)}, bf16[256,256]{1,0:T(8,128)(2,1)S(1)}, u32[]{:S(2)}, u32[]{:S(2)}) collective-permute-start(bf16[256,256]{1,0:T(8,128)(2,1)S(1)} %get-tuple-element.14), channel_id=1, source_target_pairs={{0,1},{1,0},{2,3},{3,2},{4,5},{5,4},{6,7},{7,6},{8,9},{9,8},{10,11... | collective-permute-start | bytes 393224 | tf_op jit(solution)/shard_map/ppermute | solution.py:37
  36.3 33.1 %copy-start.5 = (f32[2048]{0:T(1024)S(1)}, f32[2048]{0:T(1024)}, u32[]{:S(2)}) copy-start(f32[2048]{0:T(1024)} %param.21) | copy-start | bytes 24580
  36.3 18.7 %all-to-all-start = ((bf16[4,64,2048]{2,1,0:T(8,128)(2,1)}), bf16[4,64,2048]{2,1,0:T(8,128)(2,1)S(1)}, u32[]{:S(2)}, u32[]{:S(2)}) async-start(bf16[4,64,2048]{2,1,0:T(8,128)(2,1)} %bitcast.5), calls=%async_computation | async-start | bytes 2097152 | tf_op jit(solution)/shard_map/all_to_all | solution.py:291
  40.5 22.4 %collective-permute-start.8 = (bf16[256,2048]{1,0:T(8,128)(2,1)S(1)}, bf16[256,2048]{1,0:T(8,128)(2,1)}, u32[]{:S(2)}, u32[]{:S(2)}) collective-permute-start(bf16[256,2048]{1,0:T(8,128)(2,1)S(1)} %bitcast.20), channel_id=1, source_target_pairs={{0,8},{1,65},{8,16},{9,73},{16,24},{17,81},{24,32},{25,89},{32,40}... | collective-permute-start | bytes 3145736 | tf_op jit(solution)/shard_map/ppermute | solution.py:23
  44.6 20.3 %collective-permute-start.5 = (bf16[256,2048]{1,0:T(8,128)(2,1)S(1)}, bf16[256,2048]{1,0:T(8,128)(2,1)}, u32[]{:S(2)}, u32[]{:S(2)}) collective-permute-start(bf16[256,2048]{1,0:T(8,128)(2,1)S(1)} %bitcast.21), channel_id=1, source_target_pairs={{0,56},{1,449},{8,0},{9,457},{16,8},{17,465},{24,16},{25,473},{32,... | collective-permute-start | bytes 3145736 | tf_op jit(solution)/shard_map/ppermute | solution.py:23
  62.9 28.8 %collective-permute-start.9 = (bf16[256,2048]{1,0:T(8,128)(2,1)}, bf16[256,2048]{1,0:T(8,128)(2,1)S(1)}, u32[]{:S(2)}, u32[]{:S(2)}) collective-permute-start(bf16[256,2048]{1,0:T(8,128)(2,1)} %collective-permute-done.8.refs_6_), channel_id=1, source_target_pairs={{0,8},{1,65},{8,16},{9,73},{16,24},{17,81},{24,32},{25,89},{32,40}... | collective-permute-start | bytes 3145736 | tf_op jit(solution)/shard_map/ppermute | solution.py:23
  64.8 28.8 %collective-permute-start.6 = (bf16[256,2048]{1,0:T(8,128)(2,1)}, bf16[256,2048]{1,0:T(8,128)(2,1)}, u32[]{:S(2)}, u32[]{:S(2)}) collective-permute-start(bf16[256,2048]{1,0:T(8,128)(2,1)} %collective-permute-done.5.refs_1_), channel_id=1, source_target_pairs={{0,56},{1,449},{8,0},{9,457},{16,8},{17,465},{24,16},{25,473},{32,... | collective-permute-start | bytes 3145736 | tf_op jit(solution)/shard_map/ppermute | solution.py:23
  88.6 19.8 %collective-permute-start.4 = (bf16[256,2048]{1,0:T(8,128)(2,1)S(1)}, bf16[256,2048]{1,0:T(8,128)(2,1)}, u32[]{:S(2)}, u32[]{:S(2)}) collective-permute-start(bf16[256,2048]{1,0:T(8,128)(2,1)S(1)} %bitcast.23), channel_id=1, source_target_pairs={{0,1},{1,0},{2,3},{3,2},{4,5},{5,4},{6,7},{7,6},{8,9},{9,8},{10,11... | collective-permute-start | bytes 3145736 | tf_op jit(solution)/shard_map/ppermute | solution.py:37
  91.7 17.6 %collective-permute-start.10 = (bf16[256,2048]{1,0:T(8,128)(2,1)S(1)}, bf16[256,2048]{1,0:T(8,128)(2,1)}, u32[]{:S(2)}, u32[]{:S(2)}) collective-permute-start(bf16[256,2048]{1,0:T(8,128)(2,1)S(1)} %collective-permute-done.9.refs_5_), channel_id=1, source_target_pairs={{0,8},{1,65},{8,16},{9,73},{16,24},{17,81},{24,32},{25,89},{32,40}... | collective-permute-start | bytes 3145736 | tf_op jit(solution)/shard_map/ppermute | solution.py:23
  93.6 16.8 %collective-permute-start.7 = (bf16[256,2048]{1,0:T(8,128)(2,1)}, bf16[256,2048]{1,0:T(8,128)(2,1)}, u32[]{:S(2)}, u32[]{:S(2)}) collective-permute-start(bf16[256,2048]{1,0:T(8,128)(2,1)} %collective-permute-done.6.refs_2_), channel_id=1, source_target_pairs={{0,56},{1,449},{8,0},{9,457},{16,8},{17,465},{24,16},{25,473},{32,... | collective-permute-start | bytes 3145736 | tf_op jit(solution)/shard_map/ppermute | solution.py:23
  99.0 17.6 %collective-permute-start.11 = (bf16[128,2048]{1,0:T(8,128)(2,1)}, bf16[128,2048]{1,0:T(8,128)(2,1)}, u32[]{:S(2)}, u32[]{:S(2)}) collective-permute-start(bf16[128,2048]{1,0:T(8,128)(2,1)} %slice.16), channel_id=1, source_target_pairs={{0,16},{1,129},{8,24},{9,137},{16,32},{17,145},{24,40},{25,153},{3... | collective-permute-start | bytes 1572872 | tf_op jit(solution)/shard_map/ppermute | solution.py:23
  102.8 18.6 %collective-permute-start.12 = (bf16[128,2048]{1,0:T(8,128)(2,1)}, bf16[128,2048]{1,0:T(8,128)(2,1)}, u32[]{:S(2)}, u32[]{:S(2)}) collective-permute-start(bf16[128,2048]{1,0:T(8,128)(2,1)} %slice.17), channel_id=1, source_target_pairs={{0,48},{1,385},{8,56},{9,393},{16,0},{17,401},{24,8},{25,409},{32,... | collective-permute-start | bytes 1572872 | tf_op jit(solution)/shard_map/ppermute | solution.py:23
  124.3 5.3 %collective-permute-start.13 = (bf16[256,2048]{1,0:T(8,128)(2,1)S(1)}, bf16[256,2048]{1,0:T(8,128)(2,1)S(1)}, u32[]{:S(2)}, u32[]{:S(2)}) collective-permute-start(bf16[256,2048]{1,0:T(8,128)(2,1)S(1)} %get-tuple-element.20), channel_id=1, source_target_pairs={{0,1},{1,0},{2,3},{3,2},{4,5},{5,4},{6,7},{7,6},{8,9},{9,8},{10,11... | collective-permute-start | bytes 3145736 | tf_op jit(solution)/shard_map/ppermute | solution.py:37
  163.9 6.3 %collective-permute-start.14 = (bf16[256,2048]{1,0:T(8,128)(2,1)S(1)}, bf16[256,2048]{1,0:T(8,128)(2,1)S(1)}, u32[]{:S(2)}, u32[]{:S(2)}) collective-permute-start(bf16[256,2048]{1,0:T(8,128)(2,1)S(1)} %bitcast.25), channel_id=1, source_target_pairs={{0,1},{1,0},{2,3},{3,2},{4,5},{5,4},{6,7},{7,6},{8,9},{9,8},{10,11... | collective-permute-start | bytes 3145736 | tf_op jit(solution)/shard_map/ppermute | solution.py:37
  168.2 1.9 %copy-start = (bf16[512,2048]{1,0:T(8,128)(2,1)}, bf16[512,2048]{1,0:T(8,128)(2,1)S(1)}, u32[]{:S(2)}) copy-start(bf16[512,2048]{1,0:T(8,128)(2,1)S(1)} %constant_dynamic-update-slice_fusion.1) | copy-start | bytes 6291460

commit v6 on v5

--- a/solution.py
+++ b/solution.py
@@ -171,21 +171,11 @@
     )(at, total, picked, first, second, down_t)
 
 
-def attention_body(
-    core_ref, slope_ref, sink_ref, q_ref, kt_ref, vt_ref, doc_ref, before_ref, after_ref,
-    qg_ref, kg_ref, other_ref, own_ref, kn_ref, vn_ref, dk_ref
-):
-    head = kt_ref.shape[0]
+def attend_blocks(inner, core_ref, slope_ref, sink_ref, q_ref, key_blocks, qg_ref, kg_ref, put, kn_ref, vn_ref, dk_ref):
+    head = kn_ref.shape[1]
     heads = q_ref.shape[1] // head
-    kg = kg_ref[...]
-    for j in range(6):
-        if j == 0:
-            kt, vt, doc = before_ref[:head, :], before_ref[head : 2 * head, :], before_ref[2 * head : 2 * head + 8, :]
-        elif j == 5:
-            kt, vt, doc = after_ref[:head, :], after_ref[head : 2 * head, :], after_ref[2 * head : 2 * head + 8, :]
-        else:
-            lanes = slice((j - 1) * WINDOW, j * WINDOW)
-            kt, vt, doc = kt_ref[:, lanes], vt_ref[:, lanes], doc_ref[:8, lanes]
+    kg = jnp.broadcast_to(kg_ref[...], (WINDOW, head)).T
+    for j, (kt, vt, doc) in key_blocks:
         wide = kt.astype(jnp.float32)
         scale = lax.rsqrt(jnp.mean(wide * wide, axis=0, keepdims=True) + EPS)
         kn_ref[j] = (wide * scale * kg).astype(jnp.bfloat16)
@@ -199,53 +189,90 @@
     core = core_ref[0]
     for half in range(2):
         side = 1 - core if half == 0 else core
-        for j in range(2):
-            block = 2 * side + j
-            q = q_ref[pl.ds(pl.multiple_of(block * WINDOW, WINDOW), WINDOW), :]
-            keys = jnp.concatenate([kn_ref[block], kn_ref[block + 1], kn_ref[block + 2]], axis=1)
-            vals = jnp.concatenate([vn_ref[block], vn_ref[block + 1], vn_ref[block + 2]], axis=1)
-            doc_k = jnp.concatenate(
-                [jnp.broadcast_to(dk_ref[block + i][:1], (WINDOW, WINDOW)) for i in range(3)], axis=1
+        block = 1 + side if inner else 3 * side
+        q = q_ref[pl.ds(pl.multiple_of(block * WINDOW, WINDOW), WINDOW), :]
+        keys = jnp.concatenate([kn_ref[block], kn_ref[block + 1], kn_ref[block + 2]], axis=1)
+        vals = jnp.concatenate([vn_ref[block], vn_ref[block + 1], vn_ref[block + 2]], axis=1)
+        doc_k = jnp.concatenate(
+            [jnp.broadcast_to(dk_ref[block + i][:1], (WINDOW, WINDOW)) for i in range(3)], axis=1
+        )
+        doc_q = jnp.broadcast_to(dk_ref[block + 1][:1], (WINDOW, WINDOW)).T
+        allowed = near & (doc_k == jnp.concatenate([doc_q] * 3, axis=1))
+        outs = []
+        for h in range(heads):
+            wide = q[:, h * head : (h + 1) * head].astype(jnp.float32)
+            scale = lax.rsqrt(jnp.mean(wide * wide, axis=-1, keepdims=True) + EPS)
+            qn = (wide * scale * qg_ref[...]).astype(jnp.bfloat16)
+            s = jnp.dot(qn, keys, preferred_element_type=jnp.float32) * head ** (-0.5)
+            s = jnp.where(allowed, s - slope_ref[h] * far, jnp.float32(-1e30))
+            top = jnp.maximum(jnp.max(s, axis=-1, keepdims=True), sink_ref[h])
+            p = jnp.exp(s - top)
+            denom = jnp.sum(p, axis=-1, keepdims=True) + jnp.exp(sink_ref[h] - top)
+            mixed = lax.dot_general(
+                p.astype(jnp.bfloat16), vals, (((1,), (1,)), ((), ())),
+                preferred_element_type=jnp.float32,
             )
-            doc_q = jnp.broadcast_to(dk_ref[block + 1][:1], (WINDOW, WINDOW)).T
-            allowed = near & (doc_k == jnp.concatenate([doc_q] * 3, axis=1))
-            outs = []
-            for h in range(heads):
-                wide = q[:, h * head : (h + 1) * head].astype(jnp.float32)
-                scale = lax.rsqrt(jnp.mean(wide * wide, axis=-1, keepdims=True) + EPS)
-                qn = (wide * scale * qg_ref[...]).astype(jnp.bfloat16)
-                s = jnp.dot(qn, keys, preferred_element_type=jnp.float32) * head ** (-0.5)
-                s = jnp.where(allowed, s - slope_ref[h] * far, jnp.float32(-1e30))
-                top = jnp.maximum(jnp.max(s, axis=-1, keepdims=True), sink_ref[h])
-                p = jnp.exp(s - top)
-                denom = jnp.sum(p, axis=-1, keepdims=True) + jnp.exp(sink_ref[h] - top)
-                mixed = lax.dot_general(
-                    p.astype(jnp.bfloat16), vals, (((1,), (1,)), ((), ())),
-                    preferred_element_type=jnp.float32,
-                )
-                outs.append((mixed / denom).astype(jnp.bfloat16))
-            target = other_ref if half == 0 else own_ref
-            target[j * WINDOW : (j + 1) * WINDOW, :] = jnp.concatenate(outs, axis=1)
-
-
-def attention(core, slopes, sink, q, kt, vt, doc, before, after, q_gain, k_gain):
-    head, rows = kt.shape
+            outs.append((mixed / denom).astype(jnp.bfloat16))
+        put(half, side, jnp.concatenate(outs, axis=1))
+
+
+def own_blocks(kt_ref, vt_ref, doc_ref):
+    found = []
+    for j in range(1, 5):
+        lanes = slice((j - 1) * WINDOW, j * WINDOW)
+        found.append((j, (kt_ref[:, lanes], vt_ref[:, lanes], doc_ref[:8, lanes])))
+    return found
+
+
+def inner_body(
+    core_ref, slope_ref, sink_ref, q_ref, kt_ref, vt_ref, doc_ref, qg_ref, kg_ref,
+    out_ref, kn_ref, vn_ref, dk_ref
+):
+    def put(half, side, value):
+        out_ref[half] = value
+
+    attend_blocks(
+        True, core_ref, slope_ref, sink_ref, q_ref, own_blocks(kt_ref, vt_ref, doc_ref),
+        qg_ref, kg_ref, put, kn_ref, vn_ref, dk_ref,
+    )
+
+
+def outer_body(
+    core_ref, slope_ref, sink_ref, q_ref, kt_ref, vt_ref, doc_ref, qg_ref, kg_ref,
+    before_ref, after_ref, inner_ref, other_ref, own_ref, kn_ref, vn_ref, dk_ref
+):
+    head = kt_ref.shape[0]
+
+    def put(half, side, value):
+        target = other_ref if half == 0 else own_ref
+        target[pl.ds(pl.multiple_of(side * WINDOW, WINDOW), WINDOW), :] = value
+        target[pl.ds(pl.multiple_of((1 - side) * WINDOW, WINDOW), WINDOW), :] = inner_ref[half]
+
+    blocks = own_blocks(kt_ref, vt_ref, doc_ref)
+    for j, ref in ((0, before_ref), (5, after_ref)):
+        blocks.append((j, (ref[:head, :], ref[head : 2 * head, :], ref[2 * head : 2 * head + 8, :])))
+    attend_blocks(
+        False, core_ref, slope_ref, sink_ref, q_ref, blocks, qg_ref, kg_ref, put, kn_ref, vn_ref, dk_ref
+    )
+
+
+def attention(body, out_shape, core, slopes, sink, q, kt, vt, doc, q_gain, k_gain, *more):
+    head = kt.shape[0]
     smem = pl.BlockSpec(memory_space=pltpu.SMEM)
     vmem = pl.BlockSpec(memory_space=pltpu.VMEM)
-    out = pltpu.VMEM((rows // 2, q.shape[1]), jnp.bfloat16)
     return pl.pallas_call(
-        attention_body,
-        in_specs=[smem] * 3 + [vmem] * 8,
-        out_specs=[vmem, vmem],
-        out_shape=[out, out],
+        body,
+        in_specs=[smem] * 3 + [vmem] * (6 + len(more)),
+        out_specs=[vmem] * len(out_shape),
+        out_shape=out_shape,
         scratch_shapes=[
             pltpu.VMEM((6, head, WINDOW), jnp.bfloat16),
             pltpu.VMEM((6, head, WINDOW), jnp.bfloat16),
             pltpu.VMEM((6, 8, WINDOW), jnp.float32),
         ],
-        cost_estimate=pl.CostEstimate(flops=1 << 31, transcendentals=1 << 20, bytes_accessed=1 << 20),
-        name="attend",
-    )(core, slopes, sink, q, kt, vt, doc, before, after, q_gain, k_gain)
+        cost_estimate=pl.CostEstimate(flops=1 << 30, transcendentals=1 << 19, bytes_accessed=1 << 20),
+        compiler_params=pltpu.CompilerParams(vmem_limit_bytes=12 << 20),
+    )(core, slopes, sink, q, kt, vt, doc, q_gain, k_gain, *more)
 
 
 def shards(
@@ -273,9 +300,16 @@
     slopes = jnp.exp2(
         -8.0 * (first_head + jnp.arange(heads_here, dtype=jnp.float32) + 1.0) / heads_all
     )
+    shared = (
+        core.astype(jnp.int32).reshape(1), slopes, sink, queries, kt, vt, doc,
+        q_gain[None, :], k_gain[None, :],
+    )
+    width = queries.shape[1]
+    (inner,) = attention(
+        inner_body, [pltpu.VMEM((2, WINDOW, width), jnp.bfloat16)], *shared
+    )
     att_send, att_own = attention(
-        core.astype(jnp.int32).reshape(1), slopes, sink, queries, kt, vt, doc, before, after,
-        q_gain[None, :], k_gain[:, None],
+        outer_body, [pltpu.VMEM((half, width), jnp.bfloat16)] * 2, *shared, before, after, inner
     )
     cut = piece.shape[0] // 2
     up1, dn1 = along(piece, 1), along(piece, -1)

time: 173 us -> 172 us (level)
  waiting for transfers between devices: 22.2 us -> 20.3 us
    ppermute x1, waiting for transfers between devices: 2.58 us -> 0.73 us  [shards(): after = lax.ppermute(packed[:, :WINDOW], SP, [(j, i) for i, j in onward])]
    pallas_call x1 -> x2, Pallas kernels: 5.71 us -> 6.15 us  [attention(): pl.pallas_call(body, in_specs=[smem] * 3 + [vmem] * (6 + len(more)), out_...]
where the time goes in v6:
time: 172 us; the launch traced here: 170 us
  starting transfers between devices  68.9 us (40%)
  blocking collectives  52.5 us (31%)
  waiting for transfers between devices  20.3 us (12%)
  Pallas kernels  17.1 us (10%)
  matrix products  4.38 us (3%)
  local copies, waits for them, and re-layouts  4.35 us (3%)
  other arithmetic  2.05 us (1%)
    all_to_all x2, blocking collectives, spread(): lax.all_to_all(jnp.broadcast_to(x, (n, *x.shape)), axis, 0, 0, tiled=True)  35.3 us
    ppermute x8, starting transfers between devices, along(): return lax.ppermute(x, ('z', 'y', 'c'), pairs)  32.4 us
    ppermute x5, starting transfers between devices, swap(): return lax.ppermute(x, 'c', [(0, 1), (1, 0)])  20.2 us
    all_to_all x1, blocking collectives, scatter_x(): lax.all_to_all(x.reshape(n, x.shape[0] // n, x.shape[1]), 'x', 0, 0, tile...  17.2 us
    ppermute x8, waiting for transfers between devices, along(): return lax.ppermute(x, ('z', 'y', 'c'), pairs)  13.5 us
    all_to_all x1, starting transfers between devices, across(): lax.all_to_all(copies, ('z', 'y', 'c'), 0, 0, tiled=True, axis_index_grou...  7.64 us
    pallas_call x1, Pallas kernels, begin(): pl.pallas_call(begin_body, in_specs=[smem] + [vmem] * (2 + len(pieces)),...  6.18 us
    pallas_call x2, Pallas kernels, attention(): pl.pallas_call(body, in_specs=[smem] * 3 + [vmem] * (6 + len(more)), out_...  6.15 us
  transfers between devices with their start and end apart: 17, of which 9 were waited for; matrix products, arithmetic and copies ran while one was open for 5% of the time, Pallas kernels for 7%

profile of v6, /device:TPU:1, one launch (start us, length us, event | category | flops | bytes accessed | tf_op | source)
XLA Modules:
  0.0 170.1 jit_solution(14098806394633134752)
XLA Ops:
  0.0 2.0 %copies.1 = bf16[8,32,2048]{2,1,0:T(8,128)(2,1)} custom-call(bf16[32,1024]{1,0:T(8,128)(2,1)} %up_ref.1, bf16[32,1024]{1,0:T(8,128)(2,1)} %bitcast.38), custom_call_target="tpu_custom_call" | custom-call | tf_op jit(solution)/shard_map/copies/pallas_call | solution.py:56
  2.1 7.6 %all-to-all-start.2 = ((bf16[8,32,2048]{2,1,0:T(8,128)(2,1)}), bf16[8,32,2048]{2,1,0:T(8,128)(2,1)S(1)}, u32[]{:S(2)}, u32[]{:S(2)}) async-start(bf16[8,32,2048]{2,1,0:T(8,128)(2,1)} %copies.1), calls=%async_computation.2 | async-start | bytes 2097152 | tf_op jit(solution)/shard_map/all_to_all | solution.py:30
  9.7 6.1 %collective-permute-start.3 = (bf16[256,2048]{1,0:T(8,128)(2,1)}, bf16[256,2048]{1,0:T(8,128)(2,1)S(1)}, u32[]{:S(2)}, u32[]{:S(2)}) collective-permute-start(bf16[256,2048]{1,0:T(8,128)(2,1)} %param.20), channel_id=1, source_target_pairs={{0,1},{1,0},{2,3},{3,2},{4,5},{5,4},{6,7},{7,6},{8,9},{9,8},{10,11... | collective-permute-start | bytes 3145736 | tf_op jit(solution)/shard_map/ppermute | solution.py:37
  15.9 3.2 %collective-permute-start = (bf16[144,128]{1,0:T(8,128)(2,1)S(1)}, bf16[144,128]{1,0:T(8,128)(2,1)S(1)}, u32[]{:S(2)}, u32[]{:S(2)}) collective-permute-start(bf16[144,128]{1,0:T(8,128)(2,1)S(1)} %get-tuple-element.24), channel_id=1, source_target_pairs={{0,8},{8,16},{16,24},{24,32},{32,40},{40,48},{48,56},{56,64},{64,7... | collective-permute-start | bytes 110600 | tf_op jit(solution)/shard_map/ppermute | solution.py:293
  19.1 1.3 collective-permute-start.1
  20.4 0.0 copy-done.4
  20.4 0.0 copy-done.5
  20.4 0.0 copy-done.2
  20.4 0.0 copy-done.3
  20.4 3.1 %shard_map.118.inner_ref = bf16[2,128,256]{2,1,0:T(8,128)(2,1)S(1)} custom-call(s32[1]{0:T(128)} %bitcast.core_ref, f32[4]{0:T(128)S(1)} %multiply_exponential_fusion.slope_ref, f32[4]{0:T(128)S(1)} %copy-done.3, bf16[512,256]{1,0:T(8,128)(2,1)S(1)} %copy-done.2, bf16[64,512]{1,0:T(8,128)(2,1)S(1)} %bitcast.26, bf16[64,512]{1,0:T(8,128)(2,1)S(1)} %bitcast.29, ...), custom_call_target="tpu_custom_call" | custom-call | flops 1073741824 | bytes 1048576 | tf_op jit(solution)/shard_map/pallas_call | solution.py:263
  23.5 0.0 collective-permute-done.before_ref
  23.5 0.7 collective-permute-done.1.after_ref
  24.3 3.1 %shard_map.119 = (bf16[256,256]{1,0:T(8,128)(2,1)S(1)}, bf16[256,256]{1,0:T(8,128)(2,1)S(1)}) custom-call(s32[1]{0:T(128)} %bitcast.core_ref, f32[4]{0:T(128)S(1)} %multiply_exponential_fusion.slope_ref, f32[4]{0:T(128)S(1)} %copy-done.3, bf16[512,256]{1,0:T(8,128)(2,1)S(1)} %copy-done.2, bf16[64,512]{1,0:T(8,128)(2,1)S(1)} %bitcast.27, ...), custom_call_target="tpu_custom_call" | custom-call | flops 1073741824 | bytes 1048576 | tf_op jit(solution)/shard_map/pallas_call | solution.py:263
  27.3 2.9 %collective-permute-start.2 = (bf16[256,256]{1,0:T(8,128)(2,1)S(1)}, bf16[256,256]{1,0:T(8,128)(2,1)S(1)}, u32[]{:S(2)}, u32[]{:S(2)}) collective-permute-start(bf16[256,256]{1,0:T(8,128)(2,1)S(1)} %get-tuple-element.14), channel_id=1, source_target_pairs={{0,1},{1,0},{2,3},{3,2},{4,5},{5,4},{6,7},{7,6},{8,9},{9,8},{10,11... | collective-permute-start | bytes 393224 | tf_op jit(solution)/shard_map/ppermute | solution.py:37
  30.2 1.0 collective-permute-done.2
  31.2 0.0 collective-permute-done.3
  31.2 0.4 fusion.5
  31.6 2.7 %fusion = bf16[256,2048]{1,0:T(8,128)(2,1)} fusion(f32[256,2048]{1,0:T(8,128)S(1)} %fusion.5, bf16[256,256]{1,0:T(8,128)(2,1)S(1)} %get-tuple-element.13, bf16[256,2048]{1,0:T(8,128)(2,1)} %param.20), kind=kOutput, calls=%fused_computation.1 | convolution fusion | flops 269484032 | bytes 4325376 | tf_op jit(solution)/shard_map/dot_general | solution.py:322
  34.3 0.0 all-to-all-done.2
  34.3 4.1 %all-to-all-start = ((bf16[4,64,2048]{2,1,0:T(8,128)(2,1)}), bf16[4,64,2048]{2,1,0:T(8,128)(2,1)S(1)}, u32[]{:S(2)}, u32[]{:S(2)}) async-start(bf16[4,64,2048]{2,1,0:T(8,128)(2,1)} %bitcast.5), calls=%async_computation | async-start | bytes 2097152 | tf_op jit(solution)/shard_map/all_to_all | solution.py:325
  38.4 5.4 %collective-permute-start.8 = (bf16[256,2048]{1,0:T(8,128)(2,1)S(1)}, bf16[256,2048]{1,0:T(8,128)(2,1)}, u32[]{:S(2)}, u32[]{:S(2)}) collective-permute-start(bf16[256,2048]{1,0:T(8,128)(2,1)S(1)} %bitcast.20), channel_id=1, source_target_pairs={{0,8},{1,65},{8,16},{9,73},{16,24},{17,81},{24,32},{25,89},{32,40}... | collective-permute-start | bytes 3145736 | tf_op jit(solution)/shard_map/ppermute | solution.py:23
  43.9 6.6 %collective-permute-start.5 = (bf16[256,2048]{1,0:T(8,128)(2,1)S(1)}, bf16[256,2048]{1,0:T(8,128)(2,1)}, u32[]{:S(2)}, u32[]{:S(2)}) collective-permute-start(bf16[256,2048]{1,0:T(8,128)(2,1)S(1)} %bitcast.21), channel_id=1, source_target_pairs={{0,56},{1,449},{8,0},{9,457},{16,8},{17,465},{24,16},{25,473},{32,... | collective-permute-start | bytes 3145736 | tf_op jit(solution)/shard_map/ppermute | solution.py:23
  50.5 2.5 %all-to-all-done = bf16[4,64,2048]{2,1,0:T(8,128)(2,1)S(1)} async-done(((bf16[4,64,2048]{2,1,0:T(8,128)(2,1)}), bf16[4,64,2048]{2,1,0:T(8,128)(2,1)S(1)}, u32[]{:S(2)}, u32[]{:S(2)}) %all-to-all-start) | async-done | bytes 1048608 | tf_op jit(solution)/shard_map/all_to_all | solution.py:325
  53.0 0.2 convert_reduce_fusion.1
  53.1 1.1 fusion.1
  54.3 6.6 %collective-permute-done.8.refs_6_ = bf16[256,2048]{1,0:T(8,128)(2,1)} collective-permute-done((bf16[256,2048]{1,0:T(8,128)(2,1)S(1)}, bf16[256,2048]{1,0:T(8,128)(2,1)}, u32[]{:S(2)}, u32[]{:S(2)}) %collective-permute-start.8) | collective-permute-done | bytes 1048608 | tf_op jit(solution)/shard_map/ppermute | solution.py:23
  60.9 1.9 %collective-permute-start.9 = (bf16[256,2048]{1,0:T(8,128)(2,1)}, bf16[256,2048]{1,0:T(8,128)(2,1)S(1)}, u32[]{:S(2)}, u32[]{:S(2)}) collective-permute-start(bf16[256,2048]{1,0:T(8,128)(2,1)} %collective-permute-done.8.refs_6_), channel_id=1, source_target_pairs={{0,8},{1,65},{8,16},{9,73},{16,24},{17,81},{24,32},{25,89},{32,40}... | collective-permute-start | bytes 3145736 | tf_op jit(solution)/shard_map/ppermute | solution.py:23
  62.8 0.0 collective-permute-done.5.refs_1_
  62.8 4.6 %collective-permute-start.6 = (bf16[256,2048]{1,0:T(8,128)(2,1)}, bf16[256,2048]{1,0:T(8,128)(2,1)}, u32[]{:S(2)}, u32[]{:S(2)}) collective-permute-start(bf16[256,2048]{1,0:T(8,128)(2,1)} %collective-permute-done.5.refs_1_), channel_id=1, source_target_pairs={{0,56},{1,449},{8,0},{9,457},{16,8},{17,465},{24,16},{25,473},{32,... | collective-permute-start | bytes 3145736 | tf_op jit(solution)/shard_map/ppermute | solution.py:23
  67.4 0.0 copy-done.7
  67.4 0.1 fusion.3
  67.5 0.1 broadcast_in_dim.27
  67.6 18.9 %all_to_all.25 = bf16[4,64,2048]{2,1,0:T(8,128)(2,1)S(1)} all-to-all(bf16[4,64,2048]{2,1,0:T(8,128)(2,1)S(1)} %broadcast_in_dim.27), channel_id=1, replica_groups=mesh['z'=8,'y'=8,'x'=4,'c'=2] {'x'}, dimensions={0} | all-to-all | bytes 2097152 | tf_op jit(solution)/shard_map/all_to_all | solution.py:42
  86.6 3.1 %collective-permute-start.4 = (bf16[256,2048]{1,0:T(8,128)(2,1)S(1)}, bf16[256,2048]{1,0:T(8,128)(2,1)}, u32[]{:S(2)}, u32[]{:S(2)}) collective-permute-start(bf16[256,2048]{1,0:T(8,128)(2,1)S(1)} %bitcast.23), channel_id=1, source_target_pairs={{0,1},{1,0},{2,3},{3,2},{4,5},{5,4},{6,7},{7,6},{8,9},{9,8},{10,11... | collective-permute-start | bytes 3145736 | tf_op jit(solution)/shard_map/ppermute | solution.py:37
  89.6 0.0 collective-permute-done.9.refs_5_
  89.7 1.9 %collective-permute-start.10 = (bf16[256,2048]{1,0:T(8,128)(2,1)S(1)}, bf16[256,2048]{1,0:T(8,128)(2,1)}, u32[]{:S(2)}, u32[]{:S(2)}) collective-permute-start(bf16[256,2048]{1,0:T(8,128)(2,1)S(1)} %collective-permute-done.9.refs_5_), channel_id=1, source_target_pairs={{0,8},{1,65},{8,16},{9,73},{16,24},{17,81},{24,32},{25,89},{32,40}... | collective-permute-start | bytes 3145736 | tf_op jit(solution)/shard_map/ppermute | solution.py:23
  91.6 0.0 collective-permute-done.6.refs_2_
  91.6 4.6 %collective-permute-start.7 = (bf16[256,2048]{1,0:T(8,128)(2,1)}, bf16[256,2048]{1,0:T(8,128)(2,1)}, u32[]{:S(2)}, u32[]{:S(2)}) collective-permute-start(bf16[256,2048]{1,0:T(8,128)(2,1)} %collective-permute-done.6.refs_2_), channel_id=1, source_target_pairs={{0,56},{1,449},{8,0},{9,457},{16,8},{17,465},{24,16},{25,473},{32,... | collective-permute-start | bytes 3145736 | tf_op jit(solution)/shard_map/ppermute | solution.py:23
  96.2 0.8 slice.16
  97.0 1.9 %collective-permute-start.11 = (bf16[128,2048]{1,0:T(8,128)(2,1)}, bf16[128,2048]{1,0:T(8,128)(2,1)}, u32[]{:S(2)}, u32[]{:S(2)}) collective-permute-start(bf16[128,2048]{1,0:T(8,128)(2,1)} %slice.16), channel_id=1, source_target_pairs={{0,16},{1,129},{8,24},{9,137},{16,32},{17,145},{24,40},{25,153},{3... | collective-permute-start | bytes 1572872 | tf_op jit(solution)/shard_map/ppermute | solution.py:23
  98.9 1.9 %slice.17 = bf16[128,2048]{1,0:T(8,128)(2,1)} slice(bf16[256,2048]{1,0:T(8,128)(2,1)} %collective-permute-done.6.refs_2_), slice={[128:256], [0:2048]} | slice | bytes 1048576 | tf_op jit(solution)/shard_map/slice | solution.py:318
  100.8 5.5 %collective-permute-start.12 = (bf16[128,2048]{1,0:T(8,128)(2,1)}, bf16[128,2048]{1,0:T(8,128)(2,1)}, u32[]{:S(2)}, u32[]{:S(2)}) collective-permute-start(bf16[128,2048]{1,0:T(8,128)(2,1)} %slice.17), channel_id=1, source_target_pairs={{0,48},{1,385},{8,56},{9,393},{16,0},{17,401},{24,8},{25,409},{32,... | collective-permute-start | bytes 1572872 | tf_op jit(solution)/shard_map/ppermute | solution.py:23
  106.3 0.1 pad_add_fusion.at_ref
  106.4 0.0 collective-permute-done.4.theirs_ref
  106.4 0.9 collective-permute-done.10.refs_4_
  107.3 1.2 collective-permute-done.7.refs_3_
  108.5 6.2 %begin.1 = (f32[512,1024]{1,0:T(8,128)S(1)}, bf16[512,256]{1,0:T(8,128)(2,1)S(1)}, bf16[2048,1024]{1,0:T(8,128)(2,1)S(1)}) custom-call(s32[3]{0:T(128)S(1)} %pad_add_fusion.at_ref, bf16[256,2048]{1,0:T(8,128)(2,1)} %collective-permute-done.4.theirs_ref, bf16[256,2048]{1,0:T(8,128)(2,1)S(1)} %bitcast.24, bf16[256,2048]{1,0:T(8,128)(2,1)S(1)} %bitcast.22, ...), custom_call_target="tpu_custom_call" | custom-call | flops 2147483648 | bytes 8388608 | tf_op jit(solution)/shard_map/begin/pallas_call | solution.py:117
  114.6 0.0 collective-permute-done.11.first_ref
  114.7 4.8 %collective-permute-done.12.second_ref = bf16[128,2048]{1,0:T(8,128)(2,1)} collective-permute-done((bf16[128,2048]{1,0:T(8,128)(2,1)}, bf16[128,2048]{1,0:T(8,128)(2,1)}, u32[]{:S(2)}, u32[]{:S(2)}) %collective-permute-start.12) | collective-permute-done | bytes 524320 | tf_op jit(solution)/shard_map/ppermute | solution.py:23
  119.4 2.8 %mixer.1 = (bf16[256,1024]{1,0:T(8,128)(2,1)S(1)}, bf16[256,2048]{1,0:T(8,128)(2,1)S(1)}, bf16[2048,1024]{1,0:T(8,128)(2,1)S(1)}) custom-call(s32[3]{0:T(128)S(1)} %pad_add_fusion.at_ref, f32[512,1024]{1,0:T(8,128)S(1)} %get-tuple-element.15.total_ref, bf16[512,256]{1,0:T(8,128)(2,1)S(1)} %get-tuple-element.16.picked_ref, ...), custom_call_target="tpu_custom_call", output_to_operand_aliasing={{2}: (5, {})} | custom-call | flops 1073741824 | bytes 4194304 | tf_op jit(solution)/shard_map/mixer/pallas_call | solution.py:158
  122.2 4.2 %collective-permute-start.13 = (bf16[256,2048]{1,0:T(8,128)(2,1)S(1)}, bf16[256,2048]{1,0:T(8,128)(2,1)S(1)}, u32[]{:S(2)}, u32[]{:S(2)}) collective-permute-start(bf16[256,2048]{1,0:T(8,128)(2,1)S(1)} %get-tuple-element.20), channel_id=1, source_target_pairs={{0,1},{1,0},{2,3},{3,2},{4,5},{5,4},{6,7},{7,6},{8,9},{9,8},{10,11... | collective-permute-start | bytes 3145736 | tf_op jit(solution)/shard_map/ppermute | solution.py:37
  126.4 1.3 fusion.6
  127.7 0.8 collective-permute-done.13
  128.5 0.3 add_convert_fusion
  128.8 17.2 %all_to_all.26 = bf16[4,64,2048]{2,1,0:T(8,128)(2,1)S(1)} all-to-all(bf16[4,64,2048]{2,1,0:T(8,128)(2,1)S(1)} %bitcast.37), channel_id=1, replica_groups=mesh['z'=8,'y'=8,'x'=4,'c'=2] {'x'}, dimensions={0} | all-to-all | bytes 2097152 | tf_op jit(solution)/shard_map/all_to_all | solution.py:67
  146.1 0.2 convert_reduce_fusion
  146.3 0.1 broadcast_in_dim.28
  146.4 16.4 %all_to_all.27 = bf16[4,64,2048]{2,1,0:T(8,128)(2,1)S(1)} all-to-all(bf16[4,64,2048]{2,1,0:T(8,128)(2,1)S(1)} %broadcast_in_dim.28), channel_id=1, replica_groups=mesh['z'=8,'y'=8,'x'=4,'c'=2] {'x'}, dimensions={0} | all-to-all | bytes 2097152 | tf_op jit(solution)/shard_map/all_to_all | solution.py:42
  162.8 4.0 %collective-permute-start.14 = (bf16[256,2048]{1,0:T(8,128)(2,1)S(1)}, bf16[256,2048]{1,0:T(8,128)(2,1)S(1)}, u32[]{:S(2)}, u32[]{:S(2)}) collective-permute-start(bf16[256,2048]{1,0:T(8,128)(2,1)S(1)} %bitcast.35), channel_id=1, source_target_pairs={{0,1},{1,0},{2,3},{3,2},{4,5},{5,4},{6,7},{7,6},{8,9},{9,8},{10,11... | collective-permute-start | bytes 3145736 | tf_op jit(solution)/shard_map/ppermute | solution.py:37
  166.8 0.2 broadcast_in_dim.23
  167.1 0.1 constant_dynamic-update-slice_fusion.1
  167.2 0.0 copy-start.6
  167.2 1.9 %collective-permute-done.14 = bf16[256,2048]{1,0:T(8,128)(2,1)S(1)} collective-permute-done((bf16[256,2048]{1,0:T(8,128)(2,1)S(1)}, bf16[256,2048]{1,0:T(8,128)(2,1)S(1)}, u32[]{:S(2)}, u32[]{:S(2)}) %collective-permute-start.14) | collective-permute-done | bytes 1048608 | tf_op jit(solution)/shard_map/ppermute | solution.py:37
  169.1 1.0 constant_dynamic-update-slice_fusion
  (18 shorter events, 0.1 us)
Async XLA Ops:
  0.0 15.8 %copy-start.8 = (s32[512]{0:T(512)S(1)}, s32[512]{0:T(512)}, u32[]{:S(2)}) copy-start(s32[512]{0:T(512)} %param.16) | copy-start | bytes 6148
  0.0 15.8 %copy-start = (bf16[512,64]{0,1:T(8,128)(2,1)S(1)}, bf16[512,64]{0,1:T(8,128)(2,1)}, u32[]{:S(2)}) copy-start(bf16[512,64]{0,1:T(8,128)(2,1)} %param.14) | copy-start | bytes 196612
  0.0 15.8 %copy-start.1 = (bf16[512,64]{0,1:T(8,128)(2,1)S(1)}, bf16[512,64]{0,1:T(8,128)(2,1)}, u32[]{:S(2)}) copy-start(bf16[512,64]{0,1:T(8,128)(2,1)} %param.15) | copy-start | bytes 196612
  0.0 20.4 %copy-start.4 = (f32[64]{0:T(128)S(1)}, f32[64]{0:T(128)}, u32[]{:S(2)}) copy-start(f32[64]{0:T(128)} %param.17) | copy-start | bytes 772
  0.0 20.4 %copy-start.5 = (f32[64]{0:T(128)S(1)}, f32[64]{0:T(128)}, u32[]{:S(2)}) copy-start(f32[64]{0:T(128)} %param.18) | copy-start | bytes 772
  0.0 20.4 %copy-start.2 = (bf16[512,256]{1,0:T(8,128)(2,1)S(1)}, bf16[512,256]{1,0:T(8,128)(2,1)}, u32[]{:S(2)}) copy-start(bf16[512,256]{1,0:T(8,128)(2,1)} %q_ref.3) | copy-start | bytes 786436
  0.0 20.4 %copy-start.3 = (f32[4]{0:T(128)S(1)}, f32[4]{0:T(128)}, u32[]{:S(2)}) copy-start(f32[4]{0:T(128)} %sink_ref.3) | copy-start | bytes 52
  2.1 32.2 %all-to-all-start.2 = ((bf16[8,32,2048]{2,1,0:T(8,128)(2,1)}), bf16[8,32,2048]{2,1,0:T(8,128)(2,1)S(1)}, u32[]{:S(2)}, u32[]{:S(2)}) async-start(bf16[8,32,2048]{2,1,0:T(8,128)(2,1)} %copies.1), calls=%async_computation.2 | async-start | bytes 2097152 | tf_op jit(solution)/shard_map/all_to_all | solution.py:30
  9.7 21.5 %collective-permute-start.3 = (bf16[256,2048]{1,0:T(8,128)(2,1)}, bf16[256,2048]{1,0:T(8,128)(2,1)S(1)}, u32[]{:S(2)}, u32[]{:S(2)}) collective-permute-start(bf16[256,2048]{1,0:T(8,128)(2,1)} %param.20), channel_id=1, source_target_pairs={{0,1},{1,0},{2,3},{3,2},{4,5},{5,4},{6,7},{7,6},{8,9},{9,8},{10,11... | collective-permute-start | bytes 3145736 | tf_op jit(solution)/shard_map/ppermute | solution.py:37
  15.9 7.7 %collective-permute-start = (bf16[144,128]{1,0:T(8,128)(2,1)S(1)}, bf16[144,128]{1,0:T(8,128)(2,1)S(1)}, u32[]{:S(2)}, u32[]{:S(2)}) collective-permute-start(bf16[144,128]{1,0:T(8,128)(2,1)S(1)} %get-tuple-element.24), channel_id=1, source_target_pairs={{0,8},{8,16},{16,24},{24,32},{32,40},{40,48},{48,56},{56,64},{64,7... | collective-permute-start | bytes 110600 | tf_op jit(solution)/shard_map/ppermute | solution.py:293
  19.1 5.2 %collective-permute-start.1 = (bf16[144,128]{1,0:T(8,128)(2,1)S(1)}, bf16[144,128]{1,0:T(8,128)(2,1)S(1)}, u32[]{:S(2)}, u32[]{:S(2)}) collective-permute-start(bf16[144,128]{1,0:T(8,128)(2,1)S(1)} %get-tuple-element.23), channel_id=1, source_target_pairs={{8,0},{16,8},{24,16},{32,24},{40,32},{48,40},{56,48},{64,56},{72,6... | collective-permute-start | bytes 110600 | tf_op jit(solution)/shard_map/ppermute | solution.py:294
  27.3 3.8 %collective-permute-start.2 = (bf16[256,256]{1,0:T(8,128)(2,1)S(1)}, bf16[256,256]{1,0:T(8,128)(2,1)S(1)}, u32[]{:S(2)}, u32[]{:S(2)}) collective-permute-start(bf16[256,256]{1,0:T(8,128)(2,1)S(1)} %get-tuple-element.14), channel_id=1, source_target_pairs={{0,1},{1,0},{2,3},{3,2},{4,5},{5,4},{6,7},{7,6},{8,9},{9,8},{10,11... | collective-permute-start | bytes 393224 | tf_op jit(solution)/shard_map/ppermute | solution.py:37
  34.3 33.1 %copy-start.7 = (f32[2048]{0:T(1024)S(1)}, f32[2048]{0:T(1024)}, u32[]{:S(2)}) copy-start(f32[2048]{0:T(1024)} %param.21) | copy-start | bytes 24580
  34.3 18.7 %all-to-all-start = ((bf16[4,64,2048]{2,1,0:T(8,128)(2,1)}), bf16[4,64,2048]{2,1,0:T(8,128)(2,1)S(1)}, u32[]{:S(2)}, u32[]{:S(2)}) async-start(bf16[4,64,2048]{2,1,0:T(8,128)(2,1)} %bitcast.5), calls=%async_computation | async-start | bytes 2097152 | tf_op jit(solution)/shard_map/all_to_all | solution.py:325
  38.4 22.4 %collective-permute-start.8 = (bf16[256,2048]{1,0:T(8,128)(2,1)S(1)}, bf16[256,2048]{1,0:T(8,128)(2,1)}, u32[]{:S(2)}, u32[]{:S(2)}) collective-permute-start(bf16[256,2048]{1,0:T(8,128)(2,1)S(1)} %bitcast.20), channel_id=1, source_target_pairs={{0,8},{1,65},{8,16},{9,73},{16,24},{17,81},{24,32},{25,89},{32,40}... | collective-permute-start | bytes 3145736 | tf_op jit(solution)/shard_map/ppermute | solution.py:23
  43.9 18.9 %collective-permute-start.5 = (bf16[256,2048]{1,0:T(8,128)(2,1)S(1)}, bf16[256,2048]{1,0:T(8,128)(2,1)}, u32[]{:S(2)}, u32[]{:S(2)}) collective-permute-start(bf16[256,2048]{1,0:T(8,128)(2,1)S(1)} %bitcast.21), channel_id=1, source_target_pairs={{0,56},{1,449},{8,0},{9,457},{16,8},{17,465},{24,16},{25,473},{32,... | collective-permute-start | bytes 3145736 | tf_op jit(solution)/shard_map/ppermute | solution.py:23
  60.9 28.8 %collective-permute-start.9 = (bf16[256,2048]{1,0:T(8,128)(2,1)}, bf16[256,2048]{1,0:T(8,128)(2,1)S(1)}, u32[]{:S(2)}, u32[]{:S(2)}) collective-permute-start(bf16[256,2048]{1,0:T(8,128)(2,1)} %collective-permute-done.8.refs_6_), channel_id=1, source_target_pairs={{0,8},{1,65},{8,16},{9,73},{16,24},{17,81},{24,32},{25,89},{32,40}... | collective-permute-start | bytes 3145736 | tf_op jit(solution)/shard_map/ppermute | solution.py:23
  62.8 28.8 %collective-permute-start.6 = (bf16[256,2048]{1,0:T(8,128)(2,1)}, bf16[256,2048]{1,0:T(8,128)(2,1)}, u32[]{:S(2)}, u32[]{:S(2)}) collective-permute-start(bf16[256,2048]{1,0:T(8,128)(2,1)} %collective-permute-done.5.refs_1_), channel_id=1, source_target_pairs={{0,56},{1,449},{8,0},{9,457},{16,8},{17,465},{24,16},{25,473},{32,... | collective-permute-start | bytes 3145736 | tf_op jit(solution)/shard_map/ppermute | solution.py:23
  86.6 19.8 %collective-permute-start.4 = (bf16[256,2048]{1,0:T(8,128)(2,1)S(1)}, bf16[256,2048]{1,0:T(8,128)(2,1)}, u32[]{:S(2)}, u32[]{:S(2)}) collective-permute-start(bf16[256,2048]{1,0:T(8,128)(2,1)S(1)} %bitcast.23), channel_id=1, source_target_pairs={{0,1},{1,0},{2,3},{3,2},{4,5},{5,4},{6,7},{7,6},{8,9},{9,8},{10,11... | collective-permute-start | bytes 3145736 | tf_op jit(solution)/shard_map/ppermute | solution.py:37
  89.7 17.6 %collective-permute-start.10 = (bf16[256,2048]{1,0:T(8,128)(2,1)S(1)}, bf16[256,2048]{1,0:T(8,128)(2,1)}, u32[]{:S(2)}, u32[]{:S(2)}) collective-permute-start(bf16[256,2048]{1,0:T(8,128)(2,1)S(1)} %collective-permute-done.9.refs_5_), channel_id=1, source_target_pairs={{0,8},{1,65},{8,16},{9,73},{16,24},{17,81},{24,32},{25,89},{32,40}... | collective-permute-start | bytes 3145736 | tf_op jit(solution)/shard_map/ppermute | solution.py:23
  91.6 16.9 %collective-permute-start.7 = (bf16[256,2048]{1,0:T(8,128)(2,1)}, bf16[256,2048]{1,0:T(8,128)(2,1)}, u32[]{:S(2)}, u32[]{:S(2)}) collective-permute-start(bf16[256,2048]{1,0:T(8,128)(2,1)} %collective-permute-done.6.refs_2_), channel_id=1, source_target_pairs={{0,56},{1,449},{8,0},{9,457},{16,8},{17,465},{24,16},{25,473},{32,... | collective-permute-start | bytes 3145736 | tf_op jit(solution)/shard_map/ppermute | solution.py:23
  97.0 17.6 %collective-permute-start.11 = (bf16[128,2048]{1,0:T(8,128)(2,1)}, bf16[128,2048]{1,0:T(8,128)(2,1)}, u32[]{:S(2)}, u32[]{:S(2)}) collective-permute-start(bf16[128,2048]{1,0:T(8,128)(2,1)} %slice.16), channel_id=1, source_target_pairs={{0,16},{1,129},{8,24},{9,137},{16,32},{17,145},{24,40},{25,153},{3... | collective-permute-start | bytes 1572872 | tf_op jit(solution)/shard_map/ppermute | solution.py:23
  100.8 18.6 %collective-permute-start.12 = (bf16[128,2048]{1,0:T(8,128)(2,1)}, bf16[128,2048]{1,0:T(8,128)(2,1)}, u32[]{:S(2)}, u32[]{:S(2)}) collective-permute-start(bf16[128,2048]{1,0:T(8,128)(2,1)} %slice.17), channel_id=1, source_target_pairs={{0,48},{1,385},{8,56},{9,393},{16,0},{17,401},{24,8},{25,409},{32,... | collective-permute-start | bytes 1572872 | tf_op jit(solution)/shard_map/ppermute | solution.py:23
  122.2 6.3 %collective-permute-start.13 = (bf16[256,2048]{1,0:T(8,128)(2,1)S(1)}, bf16[256,2048]{1,0:T(8,128)(2,1)S(1)}, u32[]{:S(2)}, u32[]{:S(2)}) collective-permute-start(bf16[256,2048]{1,0:T(8,128)(2,1)S(1)} %get-tuple-element.20), channel_id=1, source_target_pairs={{0,1},{1,0},{2,3},{3,2},{4,5},{5,4},{6,7},{7,6},{8,9},{9,8},{10,11... | collective-permute-start | bytes 3145736 | tf_op jit(solution)/shard_map/ppermute | solution.py:37
  162.8 6.3 %collective-permute-start.14 = (bf16[256,2048]{1,0:T(8,128)(2,1)S(1)}, bf16[256,2048]{1,0:T(8,128)(2,1)S(1)}, u32[]{:S(2)}, u32[]{:S(2)}) collective-permute-start(bf16[256,2048]{1,0:T(8,128)(2,1)S(1)} %bitcast.35), channel_id=1, source_target_pairs={{0,1},{1,0},{2,3},{3,2},{4,5},{5,4},{6,7},{7,6},{8,9},{9,8},{10,11... | collective-permute-start | bytes 3145736 | tf_op jit(solution)/shard_map/ppermute | solution.py:37
  167.2 1.9 %copy-start.6 = (bf16[512,2048]{1,0:T(8,128)(2,1)}, bf16[512,2048]{1,0:T(8,128)(2,1)S(1)}, u32[]{:S(2)}) copy-start(bf16[512,2048]{1,0:T(8,128)(2,1)S(1)} %constant_dynamic-update-slice_fusion.1) | copy-start | bytes 6291460
